TPU v7x, 32 devices: a whole 2x2x4 slice. The times are simulated.
32 devices in a mesh: kv: 8 (over z, x), tp: 4 (over y, core).
Axes of the slice: x: 2, y: 2, z: 4, core: 2. Of those that a mesh axis runs over, the one named last changes fastest.
Arguments:
- tokens: bfloat16 [128, 2048], P(None, 'kv'), may hold values from -16 to 16
- norm_gain: bfloat16 [2048], P('kv'), may hold values from 0.099609375 to 1.8984375
- w_query: bfloat16 [2048, 1024], P('kv', 'tp'), may hold values from -0.125 to 0.125
- w_key: bfloat16 [2048, 1024], P('kv', 'tp'), may hold values from -0.125 to 0.125
- w_value: bfloat16 [2048, 2048], P('kv', 'tp'), may hold values from -0.125 to 0.125
- w_gate: bfloat16 [2048, 2048], P('kv', 'tp'), may hold values from -0.125 to 0.125
- w_decay: bfloat16 [2048, 1024], P('kv', 'tp'), may hold values from -0.5 to 0.5
- log_decay: float32 [128, 1024], P('kv', 'tp'), may hold values from -1.5 to 0
- state: float32 [128, 8, 128, 256], P('kv', 'tp'), may hold values from -6 to 6
- out_gain: float32 [256], replicated, may hold values from 0.1 to 1.9
- w_out: bfloat16 [2048, 2048], P('tp', 'kv'), may hold values from -0.125 to 0.125
- mixer_gain: bfloat16 [2048], P('kv'), may hold values from 0.099609375 to 1.8984375
- w_ffgate: bfloat16 [2048, 6144], P('kv', 'tp'), may hold values from -0.125 to 0.125
- w_ffup: bfloat16 [2048, 6144], P('kv', 'tp'), may hold values from -0.125 to 0.125
- w_down: bfloat16 [6144, 2048], P('tp', 'kv'), may hold values from -0.078125 to 0.078125
Outputs:
- result: bfloat16 [128, 2048], P(None, 'kv')
- new_state: float32 [128, 8, 128, 256], P('kv', 'tp')
All inputs are finite; a program needn't handle non-finite values.
Results may differ from a plain program's by a relative error of at most 0.028.
Values may be sent and summed in bfloat16 or wider, within the bound.
No kernel may reach another device: no remote copies, remote signals or barrier semaphores. Data moves between devices by JAX's collectives and lax.ppermute only.
A program may use at most 64 MiB of HBM per device.

v0:
```python
import jax
import jax.numpy as jnp
from jax import lax
from jax.sharding import PartitionSpec as P

D = 2048
DK = 128
DV = 256


eps = 1e-06
gate_norm = 16.0


def prepare(resid, gain):
    wide = resid.astype(jnp.float32)
    scaled = (wide * gain.astype(jnp.float32)).astype(jnp.bfloat16)
    return (scaled, jnp.sum(wide * wide, axis=1))


def project(scaled, weights):
    return jnp.concatenate(
        [jnp.dot(scaled, weight, preferred_element_type=jnp.float32) for weight in weights], axis=1
    )


def activate(terms, sums, width):
    terms = terms * lax.rsqrt(sums / D + eps)[:, None]
    return (jax.nn.silu(terms[:, :width]) * terms[:, width:]).astype(jnp.bfloat16)


def body(
    tokens,
    norm_gain,
    w_query,
    w_key,
    w_value,
    w_gate,
    w_decay,
    log_decay,
    state,
    out_gain,
    w_out,
    mixer_gain,
    w_ffgate,
    w_ffup,
    w_down,
):
    seq_dev = state.shape[0]
    heads = state.shape[1]
    key_width = w_query.shape[1]
    value_width = w_value.shape[1]
    scaled, squares = prepare(tokens, norm_gain)
    attn_weights = (w_query, w_key, w_value, w_gate, w_decay)
    sums_all = lax.psum(squares, "kv")
    terms = lax.psum_scatter(
        project(scaled, attn_weights).astype(jnp.bfloat16), "kv", scatter_dimension=0, tiled=True
    ).astype(jnp.float32)
    sums = lax.dynamic_slice_in_dim(sums_all, lax.axis_index("kv") * seq_dev, seq_dev, 0)
    terms = terms * lax.rsqrt(sums / D + eps)[:, None]
    query = terms[:, :key_width].reshape(seq_dev, heads, DK) * DK ** (-0.5)
    keys = terms[:, key_width : 2 * key_width].reshape(seq_dev, heads, DK)
    values = terms[:, 2 * key_width : 2 * key_width + value_width].reshape(seq_dev, heads, DV)
    gate = terms[:, 2 * key_width + value_width : 2 * key_width + 2 * value_width]
    decay_pre = terms[:, 2 * key_width + 2 * value_width :]
    log_a = jax.nn.log_sigmoid(decay_pre) / gate_norm + log_decay
    new_state = (
        state * jnp.exp(log_a).reshape(seq_dev, heads, DK)[..., None]
        + keys[..., None] * values[:, :, None, :]
    )
    attended = jnp.einsum("bhk,bhkv->bhv", query, new_state, precision=lax.Precision.HIGHEST)
    normed = (
        attended * lax.rsqrt(jnp.mean(attended * attended, axis=2, keepdims=True) + eps) * out_gain
    )
    mixed = (normed.reshape(seq_dev, value_width) * jax.nn.silu(gate)).astype(jnp.bfloat16)
    partial_out = jnp.dot(
        lax.all_gather(mixed, "kv", axis=0, tiled=True), w_out, preferred_element_type=jnp.float32
    )
    attn_sum = lax.psum(partial_out.astype(jnp.bfloat16), "tp").astype(jnp.float32)
    middle = (tokens.astype(jnp.float32) + attn_sum).astype(jnp.bfloat16)
    scaled2, squares2 = prepare(middle, mixer_gain)
    ff_weights = (w_ffgate, w_ffup)
    width = w_ffgate.shape[1]
    terms2, sums2 = (
        lax.psum(project(scaled2, ff_weights).astype(jnp.bfloat16), "kv").astype(jnp.float32),
        lax.psum(squares2.astype(jnp.bfloat16), "kv").astype(jnp.float32),
    )
    hidden = activate(terms2, sums2, width)
    partial_down = jnp.dot(hidden, w_down, preferred_element_type=jnp.float32)
    down_total = lax.psum(partial_down.astype(jnp.bfloat16), "tp").astype(jnp.float32)
    result = (middle.astype(jnp.float32) + down_total).astype(jnp.bfloat16)
    return (result, new_state)


def solution(mesh):
    return jax.shard_map(
        body,
        mesh=mesh,
        in_specs=(
            P(None, "kv"),
            P("kv"),
            P("kv", "tp"),
            P("kv", "tp"),
            P("kv", "tp"),
            P("kv", "tp"),
            P("kv", "tp"),
            P("kv", "tp"),
            P("kv", "tp", None, None),
            P(),
            P("tp", "kv"),
            P("kv"),
            P("kv", "tp"),
            P("kv", "tp"),
            P("tp", "kv"),
        ),
        out_specs=(P(None, "kv"), P("kv", "tp", None, None)),
        check_vma=False,
    )
```

profile of v0, /device:TPU:0, one launch (start us, length us, event | category | flops | bytes accessed | tf_op | source)
XLA Modules:
  0.0 271.0 jit_solution(2558215234920750995)
XLA Ops:
  7.2 0.0 copy-start
  7.2 0.0 reduce-scatter.2.cloned.1.call-start
  7.2 0.7 convert_element_type.59
  7.9 1.1 fusion.4
  9.1 1.1 fusion.3
  10.2 1.2 fusion.1
  11.4 1.2 fusion
  12.5 1.1 fusion.2
  13.6 0.0 copy-start.4
  13.7 0.8 copy-done.4
  14.4 0.0 reduce-scatter.2.cloned.1.call-update
  14.4 0.0 all-reduce.4.cloned.1.call-start
  14.5 0.9 fusion.8
  15.4 23.1 %psum.35 = f32[128]{0:T(128)S(1)} all-reduce(f32[128]{0:T(128)S(1)} %fusion.8), channel_id=1, replica_groups=mesh['kv'=8,'tp'=4] {'kv'}, use_global_device_ids=true, to_apply=%region_2.0 | all-reduce | flops 128 | bytes 1024 | tf_op jit(solution)/shard_map/psum | solution.py:55
  38.6 0.1 add_rsqrt_fusion.2
  38.7 41.1 %reduce-scatter.2.cloned.1.call-done = bf16[16,1792]{1,0:T(8,128)(2,1)} async-done(((bf16[128,1792]{1,0:T(8,128)(2,1)}), bf16[16,1792]{1,0:T(8,128)(2,1)}) %reduce-scatter.2.cloned.1.call-update) | async-done | bytes 57360 | tf_op jit(solution)/shard_map/reduce_scatter | solution.py:56
  79.8 0.9 convert_multiply_fusion.5
  80.7 0.7 fusion.25
  81.5 2.9 %multiply_add_fusion = f32[16,2,128,256]{3,2,1,0:T(8,128)S(1)} fusion(f32[16,2,128,256]{3,2,1,0:T(8,128)} %param.23, f32[16,2,256]{2,1,0:T(2,128)S(1)} %mul.124, f32[16,2,128]{2,1,0:T(2,128)S(1)} %mul.122, f32[16,2,128]{2,1,0:T(2,128)S(1)} %mul.119), kind=kLoop, calls=%fused_computation | loop fusion | flops 3145728 | bytes 8454144 | tf_op jit(solution)/shard_map/add | solution.py:68
  84.4 0.0 copy-start.1
  84.4 0.0 copy-start.6
  84.4 0.0 copy-start.5
  84.4 0.0 copy-start.8
  84.4 0.0 copy-start.2
  84.4 0.0 copy-start.3
  84.4 1.9 copy-done.1
  86.4 2.1 fusion.28
  88.5 0.0 copy-start.7
  88.5 0.1 fusion.15
  88.6 0.0 copy-done.6
  88.6 0.1 fusion.16
  88.7 30.5 %all_gather.3 = bf16[128,512]{1,0:T(8,128)(2,1)S(1)} all-gather(bf16[16,512]{1,0:T(8,128)(2,1)S(1)} %multiply_convert_fusion), channel_id=1, replica_groups=mesh['kv'=8,'tp'=4] {'kv'}, dimensions={0}, use_global_device_ids=true | all-gather | bytes 147456 | tf_op jit(solution)/shard_map/all_gather | solution.py:77
  119.3 0.0 copy-done.5
  119.3 0.8 convolution_convert_fusion.5
  120.1 0.0 all-reduce.4.cloned.1.call-update
  120.1 0.0 all-reduce.6.cloned.1.call-start
  120.2 0.0 copy-done.8
  120.2 30.7 %all-reduce.4.cloned.1.call-done = bf16[128,256]{1,0:T(8,128)(2,1)} async-done(((bf16[128,256]{1,0:T(8,128)(2,1)}), bf16[128,256]{1,0:T(8,128)(2,1)}) %all-reduce.4.cloned.1.call-update) | async-done | bytes 65552 | tf_op jit(solution)/shard_map/psum | solution.py:79
  150.9 0.0 copy-done.2
  150.9 0.9 fusion.11
  151.9 0.0 copy-done
  151.9 0.3 convolution_convert_fusion
  152.2 0.0 copy-done.3
  152.2 0.3 convolution_convert_fusion.1
  152.4 1.0 pad_maximum_fusion
  153.4 0.0 all-reduce.6.cloned.1.call-update
  153.5 0.0 all-reduce.8.cloned.1.call-start
  153.5 21.6 %psum.38 = bf16[128]{0:T(256)(128)(2,1)S(1)} all-reduce(bf16[128]{0:T(256)(128)(2,1)S(1)} %get-tuple-element.2), channel_id=1, replica_groups=mesh['kv'=8,'tp'=4] {'kv'}, use_global_device_ids=true, to_apply=%region_7.8 | all-reduce | flops 128 | bytes 512 | tf_op jit(solution)/shard_map/psum | solution.py:86
  175.2 54.4 %all-reduce.6.cloned.1.call-done = bf16[128,3072]{1,0:T(8,128)(2,1)} async-done(((bf16[128,3072]{1,0:T(8,128)(2,1)}), bf16[128,3072]{1,0:T(8,128)(2,1)}) %all-reduce.6.cloned.1.call-update) | async-done | bytes 786448 | tf_op jit(solution)/shard_map/psum | solution.py:85
  229.5 1.3 convert_multiply_fusion
  230.9 0.0 copy-done.7
  230.9 1.0 convolution_convert_fusion.4
  231.9 0.0 all-reduce.8.cloned.1.call-update
  231.9 31.1 %all-reduce.8.cloned.1.call-done = bf16[128,256]{1,0:T(8,128)(2,1)} async-done(((bf16[128,256]{1,0:T(8,128)(2,1)}), bf16[128,256]{1,0:T(8,128)(2,1)}) %all-reduce.8.cloned.1.call-update) | async-done | bytes 65552 | tf_op jit(solution)/shard_map/psum | solution.py:90
  263.0 1.5 fusion.12
  (10 shorter events, 0.1 us)
Async XLA Ops:
  7.2 144.7 %copy-start = (bf16[256,1536]{1,0:T(8,128)(2,1)S(1)}, bf16[256,1536]{1,0:T(8,128)(2,1)}, u32[]{:S(2)}) copy-start(bf16[256,1536]{1,0:T(8,128)(2,1)} %param.28) | copy-start | bytes 2359300
  7.2 72.6 %reduce-scatter.2.cloned.1.call-start = ((), (), s32[]{:S(2)}) async-start(), calls=%async_computation.1 | async-start | bytes 516096 | tf_op jit(solution)/shard_map/reduce_scatter | solution.py:56
  13.6 0.8 copy-start.4
  14.4 136.5 %all-reduce.4.cloned.1.call-start = ((), (), s32[]{:S(2)}) async-start(), calls=%async_computation.2 | async-start | bytes 131072 | tf_op jit(solution)/shard_map/psum | solution.py:79
  84.4 2.0 copy-start.1
  84.4 4.2 %copy-start.6 = (f32[256]{0:T(256)S(1)}, f32[256]{0:T(256)}, u32[]{:S(2)}) copy-start(f32[256]{0:T(256)} %param.24) | copy-start | bytes 3076
  84.4 34.9 %copy-start.5 = (bf16[512,256]{1,0:T(8,128)(2,1)S(1)}, bf16[512,256]{1,0:T(8,128)(2,1)}, u32[]{:S(2)}) copy-start(bf16[512,256]{1,0:T(8,128)(2,1)} %param.25) | copy-start | bytes 786436
  84.4 35.8 %copy-start.8 = (bf16[256]{0:T(256)(128)(2,1)S(1)}, bf16[256]{0:T(256)(128)(2,1)}, u32[]{:S(2)}) copy-start(bf16[256]{0:T(256)(128)(2,1)} %param.26) | copy-start | bytes 1540
  84.4 66.5 %copy-start.2 = (bf16[128,256]{1,0:T(8,128)(2,1)S(1)}, bf16[128,256]{1,0:T(8,128)(2,1)}, u32[]{:S(2)}) copy-start(bf16[128,256]{1,0:T(8,128)(2,1)} %param.15) | copy-start | bytes 196612
  84.4 67.7 %copy-start.3 = (bf16[256,1536]{1,0:T(8,128)(2,1)S(1)}, bf16[256,1536]{1,0:T(8,128)(2,1)}, u32[]{:S(2)}) copy-start(bf16[256,1536]{1,0:T(8,128)(2,1)} %param.27) | copy-start | bytes 2359300
  88.5 142.4 %copy-start.7 = (bf16[1536,256]{1,0:T(8,128)(2,1)S(1)}, bf16[1536,256]{1,0:T(8,128)(2,1)}, u32[]{:S(2)}) copy-start(bf16[1536,256]{1,0:T(8,128)(2,1)} %param.29) | copy-start | bytes 2359300
  120.1 109.4 %all-reduce.6.cloned.1.call-start = ((), (), s32[]{:S(2)}) async-start(), calls=%async_computation.3 | async-start | bytes 1572864 | tf_op jit(solution)/shard_map/psum | solution.py:85
  153.5 109.5 %all-reduce.8.cloned.1.call-start = ((), (), s32[]{:S(2)}) async-start(), calls=%async_computation.4 | async-start | bytes 131072 | tf_op jit(solution)/shard_map/psum | solution.py:90
Sparse Core Ops, SparseCore 0:
  14.6 65.1 reduce-scatter.1
  120.2 30.6 all-reduce.3
  154.3 75.1 all-reduce.5
  232.3 30.6 all-reduce.7
where the time goes:
time: 272 us; the launch traced here: 271 us
  waiting for transfers between devices  157 us (58%)
  blocking collectives  75.3 us (28%)
  between operations  14 us (5%)
  other arithmetic  11.2 us (4%)
  matrix products  10.1 us (4%)
  local copies, waits for them, and re-layouts  2.83 us (1%)
    psum x1, waiting for transfers between devices, body(): lax.psum(project(scaled2, ff_weights).astype(jnp.bfloat16), 'kv')  54.4 us
    reduce_scatter x1, waiting for transfers between devices, body(): lax.psum_scatter(project(scaled, attn_weights).astype(jnp.bfloat16), 'kv'...  41.1 us
    psum x1, waiting for transfers between devices, body(): lax.psum(partial_down.astype(jnp.bfloat16), 'tp').astype(jnp.float32)  31.1 us
    psum x1, waiting for transfers between devices, body(): lax.psum(partial_out.astype(jnp.bfloat16), 'tp').astype(jnp.float32)  30.7 us
    all_gather x1, blocking collectives, body(): lax.all_gather(mixed, 'kv', axis=0, tiled=True)  30.5 us
    psum x1, blocking collectives, body(): sums_all = lax.psum(squares, 'kv')  23.1 us
    psum x1, blocking collectives, body(): lax.psum(squares2.astype(jnp.bfloat16), 'kv').astype(jnp.float32)  21.6 us
    dot_general x7, matrix products, project(): jnp.dot(scaled, weight, preferred_element_type=jnp.float32)  6.19 us
  transfers between devices with their start and end apart: 4, of which 4 were waited for; matrix products, arithmetic and copies ran while one was open for 0% of the time, Pallas kernels for 0%

commit v1 on v0

v1 whole, which is shorter than its diff:
```python
import functools

import jax
import jax.numpy as jnp
from jax import lax
from jax.experimental import pallas as pl
from jax.experimental.pallas import tpu as pltpu
from jax.sharding import PartitionSpec as P


D = 2048
DK = 128
DV = 256
LANES = 128
STEPS = 8


eps = 1e-06
gate_norm = 16.0


def swap_blocks(array, me, count):
    rows = array.shape[0] // count
    half = 1
    while half < count:
        view = array.reshape(count // (2 * half), 2, half * rows, array.shape[1])
        flipped = jnp.concatenate([view[:, 1:], view[:, :1]], axis=1)
        array = jnp.where((me // half) % 2 == 1, flipped, view).reshape(array.shape)
        half *= 2
    return array


def send_xor(array, sizes, masks):
    if len(sizes) == 1:
        (axis,) = sizes
        pairs = [(i, i ^ masks[0]) for i in range(sizes[axis])]
        return lax.ppermute(array, axis, pairs)
    (first, outer), (second, inner) = sizes.items()
    pairs = [
        (i * inner + j, (i ^ masks[0]) * inner + (j ^ masks[1]))
        for i in range(outer)
        for j in range(inner)
    ]
    return lax.ppermute(array, (first, second), pairs)


def wide(array):
    return array.astype(jnp.float32)


def dot(left, right):
    return jnp.dot(left, right, preferred_element_type=jnp.float32)


def split_squares(squares):
    head = squares.astype(jnp.bfloat16)
    rest = (squares - head.astype(jnp.float32)).astype(jnp.bfloat16)
    lane = lax.broadcasted_iota(jnp.int32, (squares.shape[0], LANES), 1)
    return jnp.where(lane < LANES // 2, head, rest)


def joined_squares(block):
    return block[:, :1] + block[:, LANES // 2 : LANES // 2 + 1]


VMEM = pl.BlockSpec(memory_space=pltpu.VMEM)
HBM = pl.BlockSpec(memory_space=pltpu.HBM)


def call(kernel, outs, *args, specs=None, out_specs=None, scratch=(), grant=8 << 20):
    return pl.pallas_call(
        kernel,
        out_shape=outs,
        in_specs=specs or [VMEM] * len(args),
        out_specs=out_specs or jax.tree.map(lambda _: VMEM, outs),
        scratch_shapes=list(scratch),
        compiler_params=pltpu.CompilerParams(vmem_limit_bytes=grant),
    )(*args)


def in_hbm(*arrays):
    return [pltpu.with_memory_space_constraint(array, pltpu.HBM) for array in arrays]


def shape(dims, dtype=jnp.bfloat16):
    return jax.ShapeDtypeStruct(dims, dtype)


def row(ref):
    return wide(ref[...])[None]


def block_of(ref, me, m, rows):
    return ref[pl.ds(pl.multiple_of((me ^ m) * rows, rows), rows), :]


def project_kernel(count, rows, *refs):
    loaded, (ffgate, ffup, down) = refs[:8], refs[8:11]
    pieces, (gate_out, up_out, down_out, pair_out) = refs[11 : 11 + count], refs[11 + count : 15 + count]
    staged, sems = refs[15 + count : 23 + count], refs[23 + count]
    me = lax.axis_index("kv")
    other = 1 - lax.rem(me, 2)
    half = ffgate.shape[1] // 2
    start = pl.multiple_of(other * half, half)
    loads = [pltpu.make_async_copy(w, s, sems.at[j]) for j, (w, s) in enumerate(zip(loaded, staged))]
    for load in loads:
        load.start()
    moves = [
        pltpu.make_async_copy(ffgate.at[:, pl.ds(start, half)], gate_out, sems.at[8]),
        pltpu.make_async_copy(ffup.at[:, pl.ds(start, half)], up_out, sems.at[9]),
        pltpu.make_async_copy(down.at[pl.ds(start, half)], down_out, sems.at[10]),
    ]
    for move in moves:
        move.start()
    tokens, norm_gain, mixer_gain = staged[:3]
    for load in loads[:3]:
        load.wait()
    total = tokens.shape[0]
    pair_out[:total] = tokens[...]
    pair_out[total:] = jnp.broadcast_to(row(mixer_gain), (rows, tokens.shape[1])).astype(jnp.bfloat16)
    mine = jnp.concatenate([block_of(tokens, me, m, rows) for m in range(count)], axis=0)
    mine = wide(mine)
    scaled = (mine * row(norm_gain)).astype(jnp.bfloat16)
    squares = split_squares(jnp.sum(mine * mine, axis=1, keepdims=True))
    at = 0
    for load, weight in zip(loads[3:], staged[3:]):
        load.wait()
        width = weight.shape[1]
        terms = dot(scaled, weight[...]).astype(jnp.bfloat16)
        for m in range(count):
            pieces[m][:, at : at + width] = terms[m * rows : (m + 1) * rows]
        at += width
    for m in range(count):
        pieces[m][:, at:] = squares[m * rows : (m + 1) * rows]
    for move in moves:
        move.wait()


def attend_kernel(count, key_width, steps, *refs):
    pieces, (log_decay_in, state_in, out_gain_in) = refs[:count], refs[count : count + 3]
    mixed_out, keep_out, key_out, value_out = refs[count + 3 : count + 7]
    log_decay, state, out_gain, attended, sems = refs[count + 7 :]
    rows, heads = state.shape[:2]
    some = rows // steps
    loads = [
        pltpu.make_async_copy(log_decay_in, log_decay, sems.at[0]),
        pltpu.make_async_copy(out_gain_in, out_gain, sems.at[1]),
    ] + [
        pltpu.make_async_copy(
            state_in.at[pl.ds(i * some, some)], state.at[pl.ds(i * some, some)], sems.at[2 + i]
        )
        for i in range(steps)
    ]
    for load in loads:
        load.start()
    terms = wide(pieces[0][...])
    for piece in pieces[1:]:
        terms = terms + wide(piece[...])
    inv = lax.rsqrt(joined_squares(terms[:, -LANES:]) / D + eps)
    terms = terms * inv
    value_width = heads * DV
    query = terms[:, :key_width] * DK ** (-0.5)
    keys = terms[:, key_width : 2 * key_width]
    values = terms[:, 2 * key_width : 2 * key_width + value_width]
    gate = terms[:, 2 * key_width + value_width : 2 * key_width + 2 * value_width]
    decay_pre = terms[:, 2 * key_width + 2 * value_width : 3 * key_width + 2 * value_width]
    log_sigmoid = jnp.minimum(decay_pre, 0.0) - jnp.log1p(jnp.exp(-jnp.abs(decay_pre)))
    key_out[...] = keys
    value_out[...] = values
    for load in loads[:2]:
        load.wait()
    keep = jnp.exp(log_sigmoid / gate_norm + log_decay[...])
    keep_out[...] = keep
    kept = query * keep
    columns = [kept[:, h * DK : (h + 1) * DK].T for h in range(heads)]
    for i in range(steps):
        loads[2 + i].wait()
        for b in range(i * some, (i + 1) * some):
            for h in range(heads):
                attended[b : b + 1, h * DV : (h + 1) * DV] = jnp.sum(
                    columns[h][:, b : b + 1] * state[b, h], axis=0, keepdims=True
                )
    for h in range(heads):
        lanes = slice(h * DK, (h + 1) * DK)
        outs = slice(h * DV, (h + 1) * DV)
        scores = jnp.sum(query[:, lanes] * keys[:, lanes], axis=1, keepdims=True)
        full = attended[:, outs] + scores * values[:, outs]
        scale = lax.rsqrt(jnp.mean(full * full, axis=1, keepdims=True) + eps)
        normed = full * scale * row(out_gain)
        mixed_out[:, outs] = (normed * jax.nn.silu(gate[:, outs])).astype(jnp.bfloat16)


def rows_kernel(count, *refs):
    blocks, (first, second, out) = refs[:count], refs[count:]
    left = jnp.concatenate([block[...] for block in blocks], axis=0)
    depth, model = second.shape
    start = lax.rem(lax.axis_index("kv"), 2) * depth if first.shape[0] > depth else 0
    kept = first[pl.ds(pl.multiple_of(start, depth), depth)] if first.shape[0] > depth else first[...]
    out[:, :model] = dot(left, kept).astype(jnp.bfloat16)
    out[:, model:] = dot(left, second[...]).astype(jnp.bfloat16)


def middle_kernel(n_even, n_odd, *refs):
    evens, odds = refs[:n_even], refs[n_even : n_even + n_odd]
    tokens, pair, mixer_gain, ffgate, ffup, gate_pair, up_pair = refs[n_even + n_odd :][:7]
    middle_out, *pieces = refs[n_even + n_odd + 7 :]
    me = lax.axis_index("kv")
    batch, model = tokens.shape
    half = gate_pair.shape[1]
    count = 2 * len(pieces)
    rows = batch // count
    even = sum(wide(ref[...]) for ref in evens)
    odd = sum(wide(ref[...]) for ref in odds)

    def stream(stay, first, second):
        blocks = []
        for m in range(count):
            source = first if m % 2 == 0 else second
            blocks.append(
                wide(block_of(stay, me, m, rows)) + source[m // 2 * rows : (m // 2 + 1) * rows]
            )
        return wide(jnp.concatenate(blocks, axis=0).astype(jnp.bfloat16))

    own = stream(tokens, even[:, :model], odd[:, model:])
    other = stream(pair, even[:, model:], odd[:, :model])
    middle_out[...] = own.astype(jnp.bfloat16)
    own2 = (own * row(mixer_gain)).astype(jnp.bfloat16)
    other2 = (other * wide(pair[batch : batch + 1])).astype(jnp.bfloat16)
    squares = jnp.sum(own * own, axis=1, keepdims=True) + jnp.sum(other * other, axis=1, keepdims=True)
    squares = split_squares(squares)
    kept = pl.ds(pl.multiple_of(lax.rem(me, 2) * half, half), half)
    gate = (dot(own2, ffgate[:, kept]) + dot(other2, gate_pair[...])).astype(jnp.bfloat16)
    upper = (dot(own2, ffup[:, kept]) + dot(other2, up_pair[...])).astype(jnp.bfloat16)
    for i, piece in enumerate(pieces):
        part = slice(2 * i * rows, 2 * (i + 1) * rows)
        piece[:, :half] = gate[part]
        piece[:, half : 2 * half] = upper[part]
        piece[:, 2 * half :] = squares[part]


def hidden_kernel(count, *refs):
    pieces, out = refs[:count], refs[count]
    half = out.shape[1]
    terms = sum(wide(piece[...]) for piece in pieces)
    inv = lax.rsqrt(joined_squares(terms[:, 2 * half :]) / D + eps)
    hidden = jax.nn.silu(terms[:, :half] * inv) * (terms[:, half : 2 * half] * inv)
    out[...] = hidden.astype(jnp.bfloat16)


def body(
    tokens,
    norm_gain,
    w_query,
    w_key,
    w_value,
    w_gate,
    w_decay,
    log_decay,
    state,
    out_gain,
    w_out,
    mixer_gain,
    w_ffgate,
    w_ffup,
    w_down,
):
    n_kv = lax.axis_size("kv")
    n_tp = lax.axis_size("tp")
    kv, tp, both = {"kv": n_kv}, {"tp": n_tp}, {"kv": n_kv, "tp": n_tp}
    me = lax.axis_index("kv")
    rows = state.shape[0]
    heads = state.shape[1]
    key_width = w_query.shape[1]
    value_width = w_value.shape[1]
    model = tokens.shape[1]
    half = w_ffgate.shape[1] // 2

    batch = tokens.shape[0]
    attn_weights = (w_query, w_key, w_value, w_gate, w_decay)
    total_width = sum(w.shape[1] for w in attn_weights) + LANES
    loaded = (tokens, norm_gain, mixer_gain) + attn_weights
    made = call(
        functools.partial(project_kernel, n_kv, rows),
        [shape((rows, total_width))] * n_kv
        + [shape((model, half))] * 2
        + [shape((half, model)), shape((batch + rows, model))],
        *in_hbm(*loaded, w_ffgate, w_ffup, w_down),
        specs=[HBM] * 11,
        out_specs=[VMEM] * (n_kv + 4),
        scratch=[pltpu.VMEM(w.shape, w.dtype) for w in loaded]
        + [pltpu.SemaphoreType.DMA((11,))],
    )
    pieces, (gate_sent, up_sent, down_sent, pair_sent) = made[:n_kv], made[n_kv:]
    gate_pair = send_xor(gate_sent, kv, (1,))
    order = [m for m in range(2, n_kv, 2)][::-1] + [m for m in range(1, n_kv, 2)][::-1]
    came = {}
    for m in order:
        came[m] = send_xor(pieces[m], kv, (m,))
    out_pair = send_xor(w_out, kv, (1,))
    up_pair = send_xor(up_sent, kv, (1,))
    pair = send_xor(pair_sent, kv, (1,))
    down_pair = send_xor(down_sent, kv, (1,))

    mixed, keep, keys, values = call(
        functools.partial(attend_kernel, n_kv, key_width, STEPS),
        [shape((rows, value_width))]
        + [shape((rows, w), jnp.float32) for w in (key_width, key_width, value_width)],
        pieces[0],
        *[came[m] for m in order],
        *in_hbm(log_decay, state, out_gain),
        specs=[VMEM] * n_kv + [HBM] * 3,
        scratch=[
            pltpu.VMEM(log_decay.shape, jnp.float32),
            pltpu.VMEM(state.shape, jnp.float32),
            pltpu.VMEM(out_gain.shape, jnp.float32),
            pltpu.VMEM((rows, value_width), jnp.float32),
            pltpu.SemaphoreType.DMA((2 + STEPS,)),
        ],
        grant=12 << 20,
    )

    evens = list(range(2, n_kv, 2))
    blocks = {}
    for m in evens[::-1]:
        blocks[m] = send_xor(mixed, kv, (m,))
    new_state = (
        state * keep.reshape(rows, heads, DK)[..., None]
        + keys.reshape(rows, heads, DK)[..., None]
        * values.reshape(rows, heads, DV)[:, :, None, :]
    )
    chip = call(
        functools.partial(rows_kernel, n_kv // 2),
        shape((n_kv // 2 * rows, 2 * model)),
        mixed,
        *[blocks[m] for m in evens],
        w_out,
        out_pair,
    )
    chip_core = send_xor(chip, tp, (1,))
    sent = (wide(chip) + wide(chip_core)).astype(jnp.bfloat16)
    even, odd = [chip, chip_core], []
    for m in range(0, n_tp, 2)[::-1]:
        odd.append(send_xor(sent, both, (1, m)))
        if m:
            even.append(send_xor(sent, both, (0, m)))

    middle, *parts = call(
        functools.partial(middle_kernel, len(even), len(odd)),
        [shape((batch, model))] + [shape((2 * rows, 2 * half + LANES))] * (n_kv // 2),
        *even,
        *odd,
        tokens,
        pair,
        mixer_gain,
        w_ffgate,
        w_ffup,
        gate_pair,
        up_pair,
    )
    terms2 = [parts[0]]
    for m in evens[::-1]:
        terms2.append(send_xor(parts[m // 2], kv, (m,)))
    hidden = call(functools.partial(hidden_kernel, n_kv // 2), shape((2 * rows, half)), *terms2)

    blocks = {}
    for m in evens[::-1]:
        blocks[m] = send_xor(hidden, kv, (m,))
    down = call(
        functools.partial(rows_kernel, n_kv // 2),
        shape((batch, 2 * model)),
        hidden,
        *[blocks[m] for m in evens],
        w_down,
        down_pair,
    )
    down = wide(down) + wide(send_xor(down, tp, (1,)))
    own, other = down[:, :model], down[:, model:].astype(jnp.bfloat16)
    sent = own.astype(jnp.bfloat16)
    crossed = 0.0
    for m in range(0, n_tp, 2)[::-1]:
        crossed = crossed + wide(send_xor(other, both, (1, m)))
        if m:
            own = own + wide(send_xor(sent, both, (0, m)))
    crossed = crossed.reshape(n_kv // 2, 2, rows, model)
    crossed = jnp.concatenate([crossed[:, 1:], crossed[:, :1]], axis=1).reshape(own.shape)
    result = (wide(middle) + own + crossed).astype(jnp.bfloat16)
    return (swap_blocks(result, me, n_kv), new_state)


def solution(mesh):
    return jax.shard_map(
        body,
        mesh=mesh,
        in_specs=(
            P(None, "kv"),
            P("kv"),
            P("kv", "tp"),
            P("kv", "tp"),
            P("kv", "tp"),
            P("kv", "tp"),
            P("kv", "tp"),
            P("kv", "tp"),
            P("kv", "tp", None, None),
            P(),
            P("tp", "kv"),
            P("kv"),
            P("kv", "tp"),
            P("kv", "tp"),
            P("tp", "kv"),
        ),
        out_specs=(P(None, "kv"), P("kv", "tp", None, None)),
        check_vma=False,
    )
```

time: 272 us -> 102 us (0.38)
  waiting for transfers between devices: 157 us -> 51 us
  blocking collectives: 75.3 us -> 0 us
  starting transfers between devices: 0.16 us -> 38.7 us
  between operations: 14 us -> 0.97 us
  matrix products: 10.1 us -> 0 us
  other arithmetic: 11.2 us -> 5.04 us
  Pallas kernels: 0 us -> 5.66 us
    psum x3 -> x0, waiting for transfers between devices: 116 us -> none  [the longest x1 54.4 us: body(): lax.psum(project(scaled2, ff_weights).astype(jnp.bfloat16), 'kv')]
    ppermute x0 -> x29, waiting for transfers between devices: none -> 51 us  [the longest x23 36.1 us: send_xor(): return lax.ppermute(array, axis, pairs)]
    psum x2 -> x0, blocking collectives: 44.8 us -> none  [the longest x1 23.1 us: body(): sums_all = lax.psum(squares, 'kv')]
    reduce_scatter x1 -> x0, waiting for transfers between devices: 41.1 us -> none  [body(): lax.psum_scatter(project(scaled, attn_weights).astype(jnp.bfloat16), 'kv'...]
    ppermute x0 -> x29, starting transfers between devices: none -> 38.7 us  [the longest x23 32 us: send_xor(): return lax.ppermute(array, axis, pairs)]
    all_gather x1 -> x0, blocking collectives: 30.5 us -> none  [body(): lax.all_gather(mixed, 'kv', axis=0, tiled=True)]
    dot_general x10 -> x0, matrix products: 10.1 us -> none  [the longest x7 6.19 us: project(): jnp.dot(scaled, weight, preferred_element_type=jnp.float32)]
    pallas_call x0 -> x6, Pallas kernels: none -> 5.66 us  [call(): pl.pallas_call(kernel, out_shape=outs, in_specs=specs or [VMEM] * len(arg...]
  transfers between devices with their start and end apart: 4 -> 29, of which waited for: 4 -> 16; matrix products, arithmetic and copies ran while one was open for 0% -> 4% of each run, Pallas kernels for 0% -> 5%
where the time goes in v1:
time: 102 us
  waiting for transfers between devices  51 us (50%)
  starting transfers between devices  38.7 us (38%)
  Pallas kernels  5.66 us (6%)
  other arithmetic  5.04 us (5%)
    ppermute x23, waiting for transfers between devices, send_xor(): return lax.ppermute(array, axis, pairs)  36.1 us
    ppermute x23, starting transfers between devices, send_xor(): return lax.ppermute(array, axis, pairs)  32 us
    ppermute x6, waiting for transfers between devices, send_xor(): return lax.ppermute(array, (first, second), pairs)  14.9 us
    ppermute x6, starting transfers between devices, send_xor(): return lax.ppermute(array, (first, second), pairs)  6.69 us
    pallas_call x6, Pallas kernels, call(): pl.pallas_call(kernel, out_shape=outs, in_specs=specs or [VMEM] * len(arg...  5.66 us
    add x1, other arithmetic, body(): state * keep.reshape(rows, heads, DK)[..., None]  4.21 us
  transfers between devices with their start and end apart: 29, of which 16 were waited for; matrix products, arithmetic and copies ran while one was open for 4% of the time, Pallas kernels for 5%

profile of v1, /device:TPU:0, one launch (start us, length us, event | category | flops | bytes accessed | tf_op | source)
XLA Modules:
  0.0 101.6 jit_solution(6679674946403414070)
XLA Ops:
  0.7 3.0 %collective-permute-start.10 = (bf16[512,256]{1,0:T(8,128)(2,1)}, bf16[512,256]{1,0:T(8,128)(2,1)S(1)}, u32[]{:S(2)}, u32[]{:S(2)}) collective-permute-start(bf16[512,256]{1,0:T(8,128)(2,1)} %refs_4_.4), channel_id=1, source_target_pairs={{0,4},{4,0},{8,12},{12,8},{16,20},{20,16},{24,28},{28,24},{1,5},{5... | collective-permute-start | bytes 786440 | tf_op jit(solution)/shard_map/ppermute | solution.py:37
  3.7 2.0 %shard_map.158 = (bf16[16,1920]{1,0:T(8,128)(2,1)S(1)}, bf16[16,1920]{1,0:T(8,128)(2,1)S(1)}, bf16[16,1920]{1,0:T(8,128)(2,1)S(1)}, bf16[16,1920]{1,0:T(8,128)(2...) custom-call(bf16[128,256]{1,0:T(8,128)(2,1)} %refs_5_.3, ...), custom_call_target="tpu_custom_call" | custom-call | tf_op jit(solution)/shard_map/pallas_call | solution.py:71
  5.7 3.7 %collective-permute-start = (bf16[16,1920]{1,0:T(8,128)(2,1)S(1)}, bf16[16,1920]{1,0:T(8,128)(2,1)S(1)}, u32[]{:S(2)}, u32[]{:S(2)}) collective-permute-start(bf16[16,1920]{1,0:T(8,128)(2,1)S(1)} %get-tuple-element.24), channel_id=1, source_target_pairs={{0,24},{4,28},{8,16},{12,20},{16,8},{20,12},{24,0},{28,4},{1,25},{... | collective-permute-start | bytes 184328 | tf_op jit(solution)/shard_map/ppermute | solution.py:37
  9.4 0.0 collective-permute-start.1
  9.4 0.8 collective-permute-start.2
  10.2 3.6 %collective-permute-start.3 = (bf16[16,1920]{1,0:T(8,128)(2,1)S(1)}, bf16[16,1920]{1,0:T(8,128)(2,1)S(1)}, u32[]{:S(2)}, u32[]{:S(2)}) collective-permute-start(bf16[16,1920]{1,0:T(8,128)(2,1)S(1)} %get-tuple-element.27), channel_id=1, source_target_pairs={{0,28},{4,24},{8,20},{12,16},{16,12},{20,8},{24,4},{28,0},{1,29},{... | collective-permute-start | bytes 184328 | tf_op jit(solution)/shard_map/ppermute | solution.py:37
  13.7 0.0 collective-permute-done.refs_1_
  13.7 1.4 %collective-permute-start.4 = (bf16[16,1920]{1,0:T(8,128)(2,1)S(1)}, bf16[16,1920]{1,0:T(8,128)(2,1)S(1)}, u32[]{:S(2)}, u32[]{:S(2)}) collective-permute-start(bf16[16,1920]{1,0:T(8,128)(2,1)S(1)} %get-tuple-element.28), channel_id=1, source_target_pairs={{0,20},{4,16},{8,28},{12,24},{16,4},{20,0},{24,12},{28,8},{1,21},{... | collective-permute-start | bytes 184328 | tf_op jit(solution)/shard_map/ppermute | solution.py:37
  15.1 1.0 collective-permute-done.1.refs_2_
  16.1 1.5 %collective-permute-start.5 = (bf16[16,1920]{1,0:T(8,128)(2,1)S(1)}, bf16[16,1920]{1,0:T(8,128)(2,1)S(1)}, u32[]{:S(2)}, u32[]{:S(2)}) collective-permute-start(bf16[16,1920]{1,0:T(8,128)(2,1)S(1)} %get-tuple-element.29), channel_id=1, source_target_pairs={{0,12},{4,8},{8,4},{12,0},{16,28},{20,24},{24,20},{28,16},{1,13},{... | collective-permute-start | bytes 184328 | tf_op jit(solution)/shard_map/ppermute | solution.py:37
  17.6 0.0 collective-permute-done.2.refs_3_
  17.6 0.5 collective-permute-start.6
  18.1 0.0 collective-permute-done.3.refs_4_
  18.1 1.7 %collective-permute-done.4.refs_5_ = bf16[16,1920]{1,0:T(8,128)(2,1)S(1)} collective-permute-done((bf16[16,1920]{1,0:T(8,128)(2,1)S(1)}, bf16[16,1920]{1,0:T(8,128)(2,1)S(1)}, u32[]{:S(2)}, u32[]{:S(2)}) %collective-permute-start.4) | collective-permute-done | bytes 61472 | tf_op jit(solution)/shard_map/ppermute | solution.py:37
  19.8 1.4 %collective-permute-done.5.refs_6_ = bf16[16,1920]{1,0:T(8,128)(2,1)S(1)} collective-permute-done((bf16[16,1920]{1,0:T(8,128)(2,1)S(1)}, bf16[16,1920]{1,0:T(8,128)(2,1)S(1)}, u32[]{:S(2)}, u32[]{:S(2)}) %collective-permute-start.5) | collective-permute-done | bytes 61472 | tf_op jit(solution)/shard_map/ppermute | solution.py:37
  21.2 0.7 collective-permute-done.6.refs_7_
  21.8 2.6 %shard_map.159 = (bf16[16,512]{1,0:T(8,128)(2,1)S(1)}, f32[16,256]{1,0:T(8,128)S(1)}, f32[16,256]{1,0:T(8,128)S(1)}, f32[16,512]{1,0:T(8,128)S(1)}) custom-call(bf16[16,1920]{1,0:T(8,128)(2,1)S(1)} %get-tuple-element.23.refs_0_, bf16[16,1920]{1,0:T(8,128)(2,1)S(1)} %collective-permute-done.refs_1_, bf16[16,1920]{1,0:T(8,128)(2,1)S(1)} %collective-permute-done.1.refs_2_, ...), custom_call_target="tpu_custom_call" | custom-call | tf_op jit(solution)/shard_map/pallas_call | solution.py:71
  24.5 3.5 %collective-permute-start.9 = (bf16[16,512]{1,0:T(8,128)(2,1)S(1)}, bf16[16,512]{1,0:T(8,128)(2,1)S(1)}, u32[]{:S(2)}, u32[]{:S(2)}) collective-permute-start(bf16[16,512]{1,0:T(8,128)(2,1)S(1)} %get-tuple-element.31.refs_0_), channel_id=1, source_target_pairs={{0,24},{4,28},{8,16},{12,20},{16,8},{20,12},{24,0},{28,4},{1,25},{... | collective-permute-start | bytes 49160 | tf_op jit(solution)/shard_map/ppermute | solution.py:37
  28.0 0.0 collective-permute-start.8
  28.0 0.9 collective-permute-start.7
  28.9 1.1 %collective-permute-done.9.refs_3_ = bf16[16,512]{1,0:T(8,128)(2,1)S(1)} collective-permute-done((bf16[16,512]{1,0:T(8,128)(2,1)S(1)}, bf16[16,512]{1,0:T(8,128)(2,1)S(1)}, u32[]{:S(2)}, u32[]{:S(2)}) %collective-permute-start.9) | collective-permute-done | bytes 16416 | tf_op jit(solution)/shard_map/ppermute | solution.py:37
  30.1 2.5 %collective-permute-done.8.refs_2_ = bf16[16,512]{1,0:T(8,128)(2,1)S(1)} collective-permute-done((bf16[16,512]{1,0:T(8,128)(2,1)S(1)}, bf16[16,512]{1,0:T(8,128)(2,1)S(1)}, u32[]{:S(2)}, u32[]{:S(2)}) %collective-permute-start.8) | collective-permute-done | bytes 16416 | tf_op jit(solution)/shard_map/ppermute | solution.py:37
  32.6 0.0 collective-permute-done.7.refs_1_
  32.6 0.0 collective-permute-done.10.refs_5_
  32.6 0.2 shard_map.160.refs_0_
  32.8 0.1 collective-permute-start.11
  32.9 0.4 collective-permute-start.16
  33.3 1.7 %collective-permute-start.17 = (bf16[256,768]{1,0:T(8,128)(2,1)S(1)}, bf16[256,768]{1,0:T(8,128)(2,1)S(1)}, u32[]{:S(2)}, u32[]{:S(2)}) collective-permute-start(bf16[256,768]{1,0:T(8,128)(2,1)S(1)} %get-tuple-element.34), channel_id=1, source_target_pairs={{0,4},{4,0},{8,12},{12,8},{16,20},{20,16},{24,28},{28,24},{1,5},{5... | collective-permute-start | bytes 1179656 | tf_op jit(solution)/shard_map/ppermute | solution.py:37
  35.0 0.3 collective-permute-start.15
  35.3 1.7 %collective-permute-start.24 = (bf16[768,256]{1,0:T(8,128)(2,1)S(1)}, bf16[768,256]{1,0:T(8,128)(2,1)S(1)}, u32[]{:S(2)}, u32[]{:S(2)}) collective-permute-start(bf16[768,256]{1,0:T(8,128)(2,1)S(1)} %get-tuple-element.40), channel_id=1, source_target_pairs={{0,4},{4,0},{8,12},{12,8},{16,20},{20,16},{24,28},{28,24},{1,5},{5... | collective-permute-start | bytes 1179656 | tf_op jit(solution)/shard_map/ppermute | solution.py:37
  37.0 0.0 collective-permute-done.11.refs_1_
  37.1 0.4 collective-permute-start.14
  37.4 17.6 %collective-permute-done.15.refs_6_ = bf16[144,256]{1,0:T(8,128)(2,1)S(1)} collective-permute-done((bf16[144,256]{1,0:T(8,128)(2,1)S(1)}, bf16[144,256]{1,0:T(8,128)(2,1)S(1)}, u32[]{:S(2)}, u32[]{:S(2)}) %collective-permute-start.15) | collective-permute-done | bytes 73760 | tf_op jit(solution)/shard_map/ppermute | solution.py:37
  55.0 1.3 %collective-permute-start.13 = (bf16[64,512]{1,0:T(8,128)(2,1)S(1)}, bf16[64,512]{1,0:T(8,128)(2,1)S(1)}, u32[]{:S(2)}, u32[]{:S(2)}) collective-permute-start(bf16[64,512]{1,0:T(8,128)(2,1)S(1)} %add_convert_fusion), channel_id=1, source_target_pairs={{0,6},{1,7},{2,4},{3,5},{4,2},{5,3},{6,0},{7,1},{8,14},{9,15},{10,... | collective-permute-start | bytes 196616 | tf_op jit(solution)/shard_map/ppermute | solution.py:44
  56.2 8.6 %collective-permute-done.14.refs_4_ = bf16[64,512]{1,0:T(8,128)(2,1)S(1)} collective-permute-done((bf16[64,512]{1,0:T(8,128)(2,1)S(1)}, bf16[64,512]{1,0:T(8,128)(2,1)S(1)}, u32[]{:S(2)}, u32[]{:S(2)}) %collective-permute-start.14) | collective-permute-done | bytes 65568 | tf_op jit(solution)/shard_map/ppermute | solution.py:44
  64.8 1.5 %collective-permute-start.12 = (bf16[64,512]{1,0:T(8,128)(2,1)S(1)}, bf16[64,512]{1,0:T(8,128)(2,1)S(1)}, u32[]{:S(2)}, u32[]{:S(2)}) collective-permute-start(bf16[64,512]{1,0:T(8,128)(2,1)S(1)} %add_convert_fusion), channel_id=1, source_target_pairs={{0,2},{1,3},{2,0},{3,1},{4,6},{5,7},{6,4},{7,5},{8,10},{9,11},{10,... | collective-permute-start | bytes 196616 | tf_op jit(solution)/shard_map/ppermute | solution.py:44
  66.3 0.3 collective-permute-done.13.refs_3_
  66.6 2.4 %collective-permute-done.12.refs_2_ = bf16[64,512]{1,0:T(8,128)(2,1)S(1)} collective-permute-done((bf16[64,512]{1,0:T(8,128)(2,1)S(1)}, bf16[64,512]{1,0:T(8,128)(2,1)S(1)}, u32[]{:S(2)}, u32[]{:S(2)}) %collective-permute-start.12) | collective-permute-done | bytes 65568 | tf_op jit(solution)/shard_map/ppermute | solution.py:44
  69.1 0.0 collective-permute-done.16.refs_10_
  69.1 0.0 collective-permute-done.17.refs_11_
  69.1 0.4 shard_map.161
  69.5 1.5 %collective-permute-start.18 = (bf16[32,1664]{1,0:T(8,128)(2,1)S(1)}, bf16[32,1664]{1,0:T(8,128)(2,1)S(1)}, u32[]{:S(2)}, u32[]{:S(2)}) collective-permute-start(bf16[32,1664]{1,0:T(8,128)(2,1)S(1)} %get-tuple-element.37), channel_id=1, source_target_pairs={{0,24},{4,28},{8,16},{12,20},{16,8},{20,12},{24,0},{28,4},{1,25},{... | collective-permute-start | bytes 319496 | tf_op jit(solution)/shard_map/ppermute | solution.py:37
  71.0 0.6 collective-permute-start.19
  71.7 2.3 %collective-permute-start.20 = (bf16[32,1664]{1,0:T(8,128)(2,1)S(1)}, bf16[32,1664]{1,0:T(8,128)(2,1)S(1)}, u32[]{:S(2)}, u32[]{:S(2)}) collective-permute-start(bf16[32,1664]{1,0:T(8,128)(2,1)S(1)} %get-tuple-element.39), channel_id=1, source_target_pairs={{0,8},{4,12},{8,0},{12,4},{16,24},{20,28},{24,16},{28,20},{1,9},{5... | collective-permute-start | bytes 319496 | tf_op jit(solution)/shard_map/ppermute | solution.py:37
  74.0 2.8 %collective-permute-done.18.refs_1_ = bf16[32,1664]{1,0:T(8,128)(2,1)S(1)} collective-permute-done((bf16[32,1664]{1,0:T(8,128)(2,1)S(1)}, bf16[32,1664]{1,0:T(8,128)(2,1)S(1)}, u32[]{:S(2)}, u32[]{:S(2)}) %collective-permute-start.18) | collective-permute-done | bytes 106528 | tf_op jit(solution)/shard_map/ppermute | solution.py:37
  76.8 3.3 %collective-permute-done.19.refs_2_ = bf16[32,1664]{1,0:T(8,128)(2,1)S(1)} collective-permute-done((bf16[32,1664]{1,0:T(8,128)(2,1)S(1)}, bf16[32,1664]{1,0:T(8,128)(2,1)S(1)}, u32[]{:S(2)}, u32[]{:S(2)}) %collective-permute-start.19) | collective-permute-done | bytes 106528 | tf_op jit(solution)/shard_map/ppermute | solution.py:37
  80.0 0.0 collective-permute-done.20.refs_3_
  80.0 0.2 shard_map.162.refs_0_
  80.2 2.3 %collective-permute-start.23 = (bf16[32,768]{1,0:T(8,128)(2,1)S(1)}, bf16[32,768]{1,0:T(8,128)(2,1)S(1)}, u32[]{:S(2)}, u32[]{:S(2)}) collective-permute-start(bf16[32,768]{1,0:T(8,128)(2,1)S(1)} %shard_map.162.refs_0_), channel_id=1, source_target_pairs={{0,24},{4,28},{8,16},{12,20},{16,8},{20,12},{24,0},{28,4},{1,25},{... | collective-permute-start | bytes 147464 | tf_op jit(solution)/shard_map/ppermute | solution.py:37
  82.5 0.0 collective-permute-start.22
  82.6 2.1 %collective-permute-start.21 = (bf16[32,768]{1,0:T(8,128)(2,1)S(1)}, bf16[32,768]{1,0:T(8,128)(2,1)S(1)}, u32[]{:S(2)}, u32[]{:S(2)}) collective-permute-start(bf16[32,768]{1,0:T(8,128)(2,1)S(1)} %shard_map.162.refs_0_), channel_id=1, source_target_pairs={{0,8},{4,12},{8,0},{12,4},{16,24},{20,28},{24,16},{28,20},{1,9},{5... | collective-permute-start | bytes 147464 | tf_op jit(solution)/shard_map/ppermute | solution.py:37
  84.7 0.0 collective-permute-done.24.refs_5_
  84.7 1.6 %collective-permute-done.23.refs_3_ = bf16[32,768]{1,0:T(8,128)(2,1)S(1)} collective-permute-done((bf16[32,768]{1,0:T(8,128)(2,1)S(1)}, bf16[32,768]{1,0:T(8,128)(2,1)S(1)}, u32[]{:S(2)}, u32[]{:S(2)}) %collective-permute-start.23) | collective-permute-done | bytes 49184 | tf_op jit(solution)/shard_map/ppermute | solution.py:37
  86.3 1.3 %collective-permute-done.22.refs_2_ = bf16[32,768]{1,0:T(8,128)(2,1)S(1)} collective-permute-done((bf16[32,768]{1,0:T(8,128)(2,1)S(1)}, bf16[32,768]{1,0:T(8,128)(2,1)S(1)}, u32[]{:S(2)}, u32[]{:S(2)}) %collective-permute-start.22) | collective-permute-done | bytes 49184 | tf_op jit(solution)/shard_map/ppermute | solution.py:37
  87.5 0.0 collective-permute-done.21.refs_1_
  87.5 0.3 shard_map.163
  87.8 0.1 collective-permute-start.25
  88.0 1.2 %collective-permute-done.25 = bf16[128,512]{1,0:T(8,128)(2,1)S(1)} collective-permute-done((bf16[128,512]{1,0:T(8,128)(2,1)S(1)}, bf16[128,512]{1,0:T(8,128)(2,1)S(1)}, u32[]{:S(2)}, u32[]{:S(2)}) %collective-permute-start.25) | collective-permute-done | bytes 131104 | tf_op jit(solution)/shard_map/ppermute | solution.py:37
  89.3 1.8 %collective-permute-start.27 = (bf16[128,256]{1,0:T(8,128)(2,1)S(1)}, bf16[128,256]{1,0:T(8,128)(2,1)S(1)}, u32[]{:S(2)}, u32[]{:S(2)}) collective-permute-start(bf16[128,256]{1,0:T(8,128)(2,1)S(1)} %get-tuple-element.45), channel_id=1, source_target_pairs={{0,6},{1,7},{2,4},{3,5},{4,2},{5,3},{6,0},{7,1},{8,14},{9,15},{10,... | collective-permute-start | bytes 196616 | tf_op jit(solution)/shard_map/ppermute | solution.py:44
  91.1 1.2 %collective-permute-start.28 = (bf16[128,256]{1,0:T(8,128)(2,1)S(1)}, bf16[128,256]{1,0:T(8,128)(2,1)S(1)}, u32[]{:S(2)}, u32[]{:S(2)}) collective-permute-start(bf16[128,256]{1,0:T(8,128)(2,1)S(1)} %get-tuple-element.45), channel_id=1, source_target_pairs={{0,4},{1,5},{2,6},{3,7},{4,0},{5,1},{6,2},{7,3},{8,12},{9,13},{10,... | collective-permute-start | bytes 196616 | tf_op jit(solution)/shard_map/ppermute | solution.py:44
  92.2 4.2 %multiply_add_fusion = f32[16,2,128,256]{3,2,1,0:T(8,128)} fusion(f32[16,2,128,256]{3,2,1,0:T(8,128)} %refs_9_.4, f32[16,2,256]{2,1,0:T(2,128)S(1)} %mul.32, f32[16,2,128]{2,1,0:T(2,128)S(1)} %mul.30, f32[16,2,128]{2,1,0:T(2,128)S(1)} %mul.27), kind=kLoop, calls=%fused_computation | loop fusion | flops 3145728 | bytes 8454144 | tf_op jit(solution)/shard_map/add | solution.py:327
  96.4 0.6 collective-permute-start.26
  97.1 3.6 %collective-permute-done.26 = bf16[128,256]{1,0:T(8,128)(2,1)S(1)} collective-permute-done((bf16[128,256]{1,0:T(8,128)(2,1)S(1)}, bf16[128,256]{1,0:T(8,128)(2,1)S(1)}, u32[]{:S(2)}, u32[]{:S(2)}) %collective-permute-start.26) | collective-permute-done | bytes 65568 | tf_op jit(solution)/shard_map/ppermute | solution.py:44
  100.9 0.7 fusion.2
  (32 shorter events, 0.3 us)
Async XLA Ops:
  0.6 32.0 %copy-start.4 = (bf16[512,256]{1,0:T(8,128)(2,1)S(1)}, bf16[512,256]{1,0:T(8,128)(2,1)}, u32[]{:S(2)}) copy-start(bf16[512,256]{1,0:T(8,128)(2,1)} %refs_4_.4) | copy-start | bytes 786436
  0.6 68.4 %copy-start.2 = (bf16[256,1536]{1,0:T(8,128)(2,1)S(1)}, bf16[256,1536]{1,0:T(8,128)(2,1)}, u32[]{:S(2)}) copy-start(bf16[256,1536]{1,0:T(8,128)(2,1)} %refs_9_.5) | copy-start | bytes 2359300
  0.7 68.4 %copy-start.1 = (bf16[256,1536]{1,0:T(8,128)(2,1)S(1)}, bf16[256,1536]{1,0:T(8,128)(2,1)}, u32[]{:S(2)}) copy-start(bf16[256,1536]{1,0:T(8,128)(2,1)} %refs_8_.5) | copy-start | bytes 2359300
  0.7 68.4 %copy-start.5 = (bf16[256]{0:T(256)(128)(2,1)S(1)}, bf16[256]{0:T(256)(128)(2,1)}, u32[]{:S(2)}) copy-start(bf16[256]{0:T(256)(128)(2,1)} %refs_7_.3) | copy-start | bytes 1540
  0.7 68.4 %copy-start.3 = (bf16[128,256]{1,0:T(8,128)(2,1)S(1)}, bf16[128,256]{1,0:T(8,128)(2,1)}, u32[]{:S(2)}) copy-start(bf16[128,256]{1,0:T(8,128)(2,1)} %refs_5_.3) | copy-start | bytes 196612
  0.7 31.9 %collective-permute-start.10 = (bf16[512,256]{1,0:T(8,128)(2,1)}, bf16[512,256]{1,0:T(8,128)(2,1)S(1)}, u32[]{:S(2)}, u32[]{:S(2)}) collective-permute-start(bf16[512,256]{1,0:T(8,128)(2,1)} %refs_4_.4), channel_id=1, source_target_pairs={{0,4},{4,0},{8,12},{12,8},{16,20},{20,16},{24,28},{28,24},{1,5},{5... | collective-permute-start | bytes 786440 | tf_op jit(solution)/shard_map/ppermute | solution.py:37
  5.7 8.0 %collective-permute-start = (bf16[16,1920]{1,0:T(8,128)(2,1)S(1)}, bf16[16,1920]{1,0:T(8,128)(2,1)S(1)}, u32[]{:S(2)}, u32[]{:S(2)}) collective-permute-start(bf16[16,1920]{1,0:T(8,128)(2,1)S(1)} %get-tuple-element.24), channel_id=1, source_target_pairs={{0,24},{4,28},{8,16},{12,20},{16,8},{20,12},{24,0},{28,4},{1,25},{... | collective-permute-start | bytes 184328 | tf_op jit(solution)/shard_map/ppermute | solution.py:37
  9.4 6.7 %collective-permute-start.1 = (bf16[16,1920]{1,0:T(8,128)(2,1)S(1)}, bf16[16,1920]{1,0:T(8,128)(2,1)S(1)}, u32[]{:S(2)}, u32[]{:S(2)}) collective-permute-start(bf16[16,1920]{1,0:T(8,128)(2,1)S(1)} %get-tuple-element.25), channel_id=1, source_target_pairs={{0,16},{4,20},{8,24},{12,28},{16,0},{20,4},{24,8},{28,12},{1,17},{... | collective-permute-start | bytes 184328 | tf_op jit(solution)/shard_map/ppermute | solution.py:37
  9.4 8.2 %collective-permute-start.2 = (bf16[16,1920]{1,0:T(8,128)(2,1)S(1)}, bf16[16,1920]{1,0:T(8,128)(2,1)S(1)}, u32[]{:S(2)}, u32[]{:S(2)}) collective-permute-start(bf16[16,1920]{1,0:T(8,128)(2,1)S(1)} %get-tuple-element.26), channel_id=1, source_target_pairs={{0,8},{4,12},{8,0},{12,4},{16,24},{20,28},{24,16},{28,20},{1,9},{5... | collective-permute-start | bytes 184328 | tf_op jit(solution)/shard_map/ppermute | solution.py:37
  10.2 7.9 %collective-permute-start.3 = (bf16[16,1920]{1,0:T(8,128)(2,1)S(1)}, bf16[16,1920]{1,0:T(8,128)(2,1)S(1)}, u32[]{:S(2)}, u32[]{:S(2)}) collective-permute-start(bf16[16,1920]{1,0:T(8,128)(2,1)S(1)} %get-tuple-element.27), channel_id=1, source_target_pairs={{0,28},{4,24},{8,20},{12,16},{16,12},{20,8},{24,4},{28,0},{1,29},{... | collective-permute-start | bytes 184328 | tf_op jit(solution)/shard_map/ppermute | solution.py:37
  13.7 6.1 %collective-permute-start.4 = (bf16[16,1920]{1,0:T(8,128)(2,1)S(1)}, bf16[16,1920]{1,0:T(8,128)(2,1)S(1)}, u32[]{:S(2)}, u32[]{:S(2)}) collective-permute-start(bf16[16,1920]{1,0:T(8,128)(2,1)S(1)} %get-tuple-element.28), channel_id=1, source_target_pairs={{0,20},{4,16},{8,28},{12,24},{16,4},{20,0},{24,12},{28,8},{1,21},{... | collective-permute-start | bytes 184328 | tf_op jit(solution)/shard_map/ppermute | solution.py:37
  16.1 5.1 %collective-permute-start.5 = (bf16[16,1920]{1,0:T(8,128)(2,1)S(1)}, bf16[16,1920]{1,0:T(8,128)(2,1)S(1)}, u32[]{:S(2)}, u32[]{:S(2)}) collective-permute-start(bf16[16,1920]{1,0:T(8,128)(2,1)S(1)} %get-tuple-element.29), channel_id=1, source_target_pairs={{0,12},{4,8},{8,4},{12,0},{16,28},{20,24},{24,20},{28,16},{1,13},{... | collective-permute-start | bytes 184328 | tf_op jit(solution)/shard_map/ppermute | solution.py:37
  17.6 4.3 %collective-permute-start.6 = (bf16[16,1920]{1,0:T(8,128)(2,1)S(1)}, bf16[16,1920]{1,0:T(8,128)(2,1)S(1)}, u32[]{:S(2)}, u32[]{:S(2)}) collective-permute-start(bf16[16,1920]{1,0:T(8,128)(2,1)S(1)} %get-tuple-element.30), channel_id=1, source_target_pairs={{0,4},{4,0},{8,12},{12,8},{16,20},{20,16},{24,28},{28,24},{1,5},{5... | collective-permute-start | bytes 184328 | tf_op jit(solution)/shard_map/ppermute | solution.py:37
  21.8 65.7 %copy-start = (bf16[1536,256]{1,0:T(8,128)(2,1)S(1)}, bf16[1536,256]{1,0:T(8,128)(2,1)}, u32[]{:S(2)}) copy-start(bf16[1536,256]{1,0:T(8,128)(2,1)} %refs_4_.5) | copy-start | bytes 2359300
  24.5 5.6 %collective-permute-start.9 = (bf16[16,512]{1,0:T(8,128)(2,1)S(1)}, bf16[16,512]{1,0:T(8,128)(2,1)S(1)}, u32[]{:S(2)}, u32[]{:S(2)}) collective-permute-start(bf16[16,512]{1,0:T(8,128)(2,1)S(1)} %get-tuple-element.31.refs_0_), channel_id=1, source_target_pairs={{0,24},{4,28},{8,16},{12,20},{16,8},{20,12},{24,0},{28,4},{1,25},{... | collective-permute-start | bytes 49160 | tf_op jit(solution)/shard_map/ppermute | solution.py:37
  28.0 4.6 %collective-permute-start.8 = (bf16[16,512]{1,0:T(8,128)(2,1)S(1)}, bf16[16,512]{1,0:T(8,128)(2,1)S(1)}, u32[]{:S(2)}, u32[]{:S(2)}) collective-permute-start(bf16[16,512]{1,0:T(8,128)(2,1)S(1)} %get-tuple-element.31.refs_0_), channel_id=1, source_target_pairs={{0,16},{4,20},{8,24},{12,28},{16,0},{20,4},{24,8},{28,12},{1,17},{... | collective-permute-start | bytes 49160 | tf_op jit(solution)/shard_map/ppermute | solution.py:37
  28.0 4.6 %collective-permute-start.7 = (bf16[16,512]{1,0:T(8,128)(2,1)S(1)}, bf16[16,512]{1,0:T(8,128)(2,1)S(1)}, u32[]{:S(2)}, u32[]{:S(2)}) collective-permute-start(bf16[16,512]{1,0:T(8,128)(2,1)S(1)} %get-tuple-element.31.refs_0_), channel_id=1, source_target_pairs={{0,8},{4,12},{8,0},{12,4},{16,24},{20,28},{24,16},{28,20},{1,9},{5... | collective-permute-start | bytes 49160 | tf_op jit(solution)/shard_map/ppermute | solution.py:37
  32.8 4.2 %collective-permute-start.11 = (bf16[64,512]{1,0:T(8,128)(2,1)S(1)}, bf16[64,512]{1,0:T(8,128)(2,1)S(1)}, u32[]{:S(2)}, u32[]{:S(2)}) collective-permute-start(bf16[64,512]{1,0:T(8,128)(2,1)S(1)} %shard_map.160.refs_0_), channel_id=1, source_target_pairs={{0,1},{1,0},{2,3},{3,2},{4,5},{5,4},{6,7},{7,6},{8,9},{9,8},{10,11... | collective-permute-start | bytes 196616 | tf_op jit(solution)/shard_map/ppermute | solution.py:37
  32.9 36.2 %collective-permute-start.16 = (bf16[256,768]{1,0:T(8,128)(2,1)S(1)}, bf16[256,768]{1,0:T(8,128)(2,1)S(1)}, u32[]{:S(2)}, u32[]{:S(2)}) collective-permute-start(bf16[256,768]{1,0:T(8,128)(2,1)S(1)} %get-tuple-element.33), channel_id=1, source_target_pairs={{0,4},{4,0},{8,12},{12,8},{16,20},{20,16},{24,28},{28,24},{1,5},{5... | collective-permute-start | bytes 1179656 | tf_op jit(solution)/shard_map/ppermute | solution.py:37
  33.3 35.8 %collective-permute-start.17 = (bf16[256,768]{1,0:T(8,128)(2,1)S(1)}, bf16[256,768]{1,0:T(8,128)(2,1)S(1)}, u32[]{:S(2)}, u32[]{:S(2)}) collective-permute-start(bf16[256,768]{1,0:T(8,128)(2,1)S(1)} %get-tuple-element.34), channel_id=1, source_target_pairs={{0,4},{4,0},{8,12},{12,8},{16,20},{20,16},{24,28},{28,24},{1,5},{5... | collective-permute-start | bytes 1179656 | tf_op jit(solution)/shard_map/ppermute | solution.py:37
  35.0 20.0 %collective-permute-start.15 = (bf16[144,256]{1,0:T(8,128)(2,1)S(1)}, bf16[144,256]{1,0:T(8,128)(2,1)S(1)}, u32[]{:S(2)}, u32[]{:S(2)}) collective-permute-start(bf16[144,256]{1,0:T(8,128)(2,1)S(1)} %get-tuple-element.32), channel_id=1, source_target_pairs={{0,4},{4,0},{8,12},{12,8},{16,20},{20,16},{24,28},{28,24},{1,5},{5... | collective-permute-start | bytes 221192 | tf_op jit(solution)/shard_map/ppermute | solution.py:37
  35.3 49.4 %collective-permute-start.24 = (bf16[768,256]{1,0:T(8,128)(2,1)S(1)}, bf16[768,256]{1,0:T(8,128)(2,1)S(1)}, u32[]{:S(2)}, u32[]{:S(2)}) collective-permute-start(bf16[768,256]{1,0:T(8,128)(2,1)S(1)} %get-tuple-element.40), channel_id=1, source_target_pairs={{0,4},{4,0},{8,12},{12,8},{16,20},{20,16},{24,28},{28,24},{1,5},{5... | collective-permute-start | bytes 1179656 | tf_op jit(solution)/shard_map/ppermute | solution.py:37
  37.1 27.7 %collective-permute-start.14 = (bf16[64,512]{1,0:T(8,128)(2,1)S(1)}, bf16[64,512]{1,0:T(8,128)(2,1)S(1)}, u32[]{:S(2)}, u32[]{:S(2)}) collective-permute-start(bf16[64,512]{1,0:T(8,128)(2,1)S(1)} %add_convert_fusion), channel_id=1, source_target_pairs={{0,4},{1,5},{2,6},{3,7},{4,0},{5,1},{6,2},{7,3},{8,12},{9,13},{10,... | collective-permute-start | bytes 196616 | tf_op jit(solution)/shard_map/ppermute | solution.py:44
  55.0 11.7 %collective-permute-start.13 = (bf16[64,512]{1,0:T(8,128)(2,1)S(1)}, bf16[64,512]{1,0:T(8,128)(2,1)S(1)}, u32[]{:S(2)}, u32[]{:S(2)}) collective-permute-start(bf16[64,512]{1,0:T(8,128)(2,1)S(1)} %add_convert_fusion), channel_id=1, source_target_pairs={{0,6},{1,7},{2,4},{3,5},{4,2},{5,3},{6,0},{7,1},{8,14},{9,15},{10,... | collective-permute-start | bytes 196616 | tf_op jit(solution)/shard_map/ppermute | solution.py:44
  64.8 4.3 %collective-permute-start.12 = (bf16[64,512]{1,0:T(8,128)(2,1)S(1)}, bf16[64,512]{1,0:T(8,128)(2,1)S(1)}, u32[]{:S(2)}, u32[]{:S(2)}) collective-permute-start(bf16[64,512]{1,0:T(8,128)(2,1)S(1)} %add_convert_fusion), channel_id=1, source_target_pairs={{0,2},{1,3},{2,0},{3,1},{4,6},{5,7},{6,4},{7,5},{8,10},{9,11},{10,... | collective-permute-start | bytes 196616 | tf_op jit(solution)/shard_map/ppermute | solution.py:44
  69.5 7.2 %collective-permute-start.18 = (bf16[32,1664]{1,0:T(8,128)(2,1)S(1)}, bf16[32,1664]{1,0:T(8,128)(2,1)S(1)}, u32[]{:S(2)}, u32[]{:S(2)}) collective-permute-start(bf16[32,1664]{1,0:T(8,128)(2,1)S(1)} %get-tuple-element.37), channel_id=1, source_target_pairs={{0,24},{4,28},{8,16},{12,20},{16,8},{20,12},{24,0},{28,4},{1,25},{... | collective-permute-start | bytes 319496 | tf_op jit(solution)/shard_map/ppermute | solution.py:37
  71.0 9.0 %collective-permute-start.19 = (bf16[32,1664]{1,0:T(8,128)(2,1)S(1)}, bf16[32,1664]{1,0:T(8,128)(2,1)S(1)}, u32[]{:S(2)}, u32[]{:S(2)}) collective-permute-start(bf16[32,1664]{1,0:T(8,128)(2,1)S(1)} %get-tuple-element.38), channel_id=1, source_target_pairs={{0,16},{4,20},{8,24},{12,28},{16,0},{20,4},{24,8},{28,12},{1,17},{... | collective-permute-start | bytes 319496 | tf_op jit(solution)/shard_map/ppermute | solution.py:37
  71.7 8.4 %collective-permute-start.20 = (bf16[32,1664]{1,0:T(8,128)(2,1)S(1)}, bf16[32,1664]{1,0:T(8,128)(2,1)S(1)}, u32[]{:S(2)}, u32[]{:S(2)}) collective-permute-start(bf16[32,1664]{1,0:T(8,128)(2,1)S(1)} %get-tuple-element.39), channel_id=1, source_target_pairs={{0,8},{4,12},{8,0},{12,4},{16,24},{20,28},{24,16},{28,20},{1,9},{5... | collective-permute-start | bytes 319496 | tf_op jit(solution)/shard_map/ppermute | solution.py:37
  80.2 6.1 %collective-permute-start.23 = (bf16[32,768]{1,0:T(8,128)(2,1)S(1)}, bf16[32,768]{1,0:T(8,128)(2,1)S(1)}, u32[]{:S(2)}, u32[]{:S(2)}) collective-permute-start(bf16[32,768]{1,0:T(8,128)(2,1)S(1)} %shard_map.162.refs_0_), channel_id=1, source_target_pairs={{0,24},{4,28},{8,16},{12,20},{16,8},{20,12},{24,0},{28,4},{1,25},{... | collective-permute-start | bytes 147464 | tf_op jit(solution)/shard_map/ppermute | solution.py:37
  82.5 5.0 %collective-permute-start.22 = (bf16[32,768]{1,0:T(8,128)(2,1)S(1)}, bf16[32,768]{1,0:T(8,128)(2,1)S(1)}, u32[]{:S(2)}, u32[]{:S(2)}) collective-permute-start(bf16[32,768]{1,0:T(8,128)(2,1)S(1)} %shard_map.162.refs_0_), channel_id=1, source_target_pairs={{0,16},{4,20},{8,24},{12,28},{16,0},{20,4},{24,8},{28,12},{1,17},{... | collective-permute-start | bytes 147464 | tf_op jit(solution)/shard_map/ppermute | solution.py:37
  82.6 5.0 %collective-permute-start.21 = (bf16[32,768]{1,0:T(8,128)(2,1)S(1)}, bf16[32,768]{1,0:T(8,128)(2,1)S(1)}, u32[]{:S(2)}, u32[]{:S(2)}) collective-permute-start(bf16[32,768]{1,0:T(8,128)(2,1)S(1)} %shard_map.162.refs_0_), channel_id=1, source_target_pairs={{0,8},{4,12},{8,0},{12,4},{16,24},{20,28},{24,16},{28,20},{1,9},{5... | collective-permute-start | bytes 147464 | tf_op jit(solution)/shard_map/ppermute | solution.py:37
  87.8 1.4 %collective-permute-start.25 = (bf16[128,512]{1,0:T(8,128)(2,1)S(1)}, bf16[128,512]{1,0:T(8,128)(2,1)S(1)}, u32[]{:S(2)}, u32[]{:S(2)}) collective-permute-start(bf16[128,512]{1,0:T(8,128)(2,1)S(1)} %shard_map.163), channel_id=1, source_target_pairs={{0,1},{1,0},{2,3},{3,2},{4,5},{5,4},{6,7},{7,6},{8,9},{9,8},{10,11... | collective-permute-start | bytes 393224 | tf_op jit(solution)/shard_map/ppermute | solution.py:37
  89.3 7.8 %collective-permute-start.27 = (bf16[128,256]{1,0:T(8,128)(2,1)S(1)}, bf16[128,256]{1,0:T(8,128)(2,1)S(1)}, u32[]{:S(2)}, u32[]{:S(2)}) collective-permute-start(bf16[128,256]{1,0:T(8,128)(2,1)S(1)} %get-tuple-element.45), channel_id=1, source_target_pairs={{0,6},{1,7},{2,4},{3,5},{4,2},{5,3},{6,0},{7,1},{8,14},{9,15},{10,... | collective-permute-start | bytes 196616 | tf_op jit(solution)/shard_map/ppermute | solution.py:44
  91.1 6.0 %collective-permute-start.28 = (bf16[128,256]{1,0:T(8,128)(2,1)S(1)}, bf16[128,256]{1,0:T(8,128)(2,1)S(1)}, u32[]{:S(2)}, u32[]{:S(2)}) collective-permute-start(bf16[128,256]{1,0:T(8,128)(2,1)S(1)} %get-tuple-element.45), channel_id=1, source_target_pairs={{0,4},{1,5},{2,6},{3,7},{4,0},{5,1},{6,2},{7,3},{8,12},{9,13},{10,... | collective-permute-start | bytes 196616 | tf_op jit(solution)/shard_map/ppermute | solution.py:44
  96.4 4.3 %collective-permute-start.26 = (bf16[128,256]{1,0:T(8,128)(2,1)S(1)}, bf16[128,256]{1,0:T(8,128)(2,1)S(1)}, u32[]{:S(2)}, u32[]{:S(2)}) collective-permute-start(bf16[128,256]{1,0:T(8,128)(2,1)S(1)} %get-tuple-element.44), channel_id=1, source_target_pairs={{0,2},{1,3},{2,0},{3,1},{4,6},{5,7},{6,4},{7,5},{8,10},{9,11},{10,... | collective-permute-start | bytes 196616 | tf_op jit(solution)/shard_map/ppermute | solution.py:44

commit v2 on v1

--- a/solution.py
+++ b/solution.py
@@ -13,6 +13,12 @@
 DV = 256
 LANES = 128
 STEPS = 8
+SCATTER = (1, 4, 5, 3, 6, 2)
+NEAR = (6, 4, 2)
+FF_GATE = (6, 4, 2)
+FF_UP = (6, 4, 2)
+LATE = 4
+HIDDEN = (6, 4, 2)
 
 
 eps = 1e-06
@@ -94,31 +100,44 @@
     return ref[pl.ds(pl.multiple_of((me ^ m) * rows, rows), rows), :]
 
 
+def place_of(m, count, rows):
+    return (1, slice(rows, 2 * rows)) if m == count - 1 else (m, slice(0, rows))
+
+
+def relay_kernel(piece, came, out):
+    rows = piece.shape[0]
+    terms = wide(piece[...]) + wide(came[rows:])
+    out[:, :-LANES] = terms[:, :-LANES].astype(jnp.bfloat16)
+    out[:, -LANES:] = split_squares(joined_squares(terms[:, -LANES:]))
+
+
 def project_kernel(count, rows, *refs):
     loaded, (ffgate, ffup, down) = refs[:8], refs[8:11]
-    pieces, (gate_out, up_out, down_out, pair_out) = refs[11 : 11 + count], refs[11 + count : 15 + count]
-    staged, sems = refs[15 + count : 23 + count], refs[23 + count]
+    pieces, (early_out, late_out, down_out, pair_out) = refs[11 : 10 + count], refs[10 + count : 14 + count]
+    staged, sems = refs[14 + count : 22 + count], refs[22 + count]
     me = lax.axis_index("kv")
     other = 1 - lax.rem(me, 2)
     half = ffgate.shape[1] // 2
-    start = pl.multiple_of(other * half, half)
+    start = pl.multiple_of(other * half, LANES)
+    first = half - late_out.shape[1]
     loads = [pltpu.make_async_copy(w, s, sems.at[j]) for j, (w, s) in enumerate(zip(loaded, staged))]
     for load in loads:
         load.start()
     moves = [
-        pltpu.make_async_copy(ffgate.at[:, pl.ds(start, half)], gate_out, sems.at[8]),
-        pltpu.make_async_copy(ffup.at[:, pl.ds(start, half)], up_out, sems.at[9]),
-        pltpu.make_async_copy(down.at[pl.ds(start, half)], down_out, sems.at[10]),
+        pltpu.make_async_copy(ffgate.at[:, pl.ds(start, half)], early_out.at[:, :half], sems.at[8]),
+        pltpu.make_async_copy(ffup.at[:, pl.ds(start, first)], early_out.at[:, half:], sems.at[9]),
+        pltpu.make_async_copy(ffup.at[:, pl.ds(start + first, half - first)], late_out, sems.at[10]),
+        pltpu.make_async_copy(down.at[pl.ds(start, half)], down_out, sems.at[11]),
     ]
     for move in moves:
         move.start()
     tokens, norm_gain, mixer_gain = staged[:3]
     for load in loads[:3]:
         load.wait()
-    total = tokens.shape[0]
-    pair_out[:total] = tokens[...]
-    pair_out[total:] = jnp.broadcast_to(row(mixer_gain), (rows, tokens.shape[1])).astype(jnp.bfloat16)
     mine = jnp.concatenate([block_of(tokens, me, m, rows) for m in range(count)], axis=0)
+    total, model = tokens.shape
+    pair_out[:total] = mine
+    pair_out[total:] = jnp.broadcast_to(row(mixer_gain), (rows, model)).astype(jnp.bfloat16)
     mine = wide(mine)
     scaled = (mine * row(norm_gain)).astype(jnp.bfloat16)
     squares = split_squares(jnp.sum(mine * mine, axis=1, keepdims=True))
@@ -128,34 +147,51 @@
         width = weight.shape[1]
         terms = dot(scaled, weight[...]).astype(jnp.bfloat16)
         for m in range(count):
-            pieces[m][:, at : at + width] = terms[m * rows : (m + 1) * rows]
+            block, top = place_of(m, count, rows)
+            pieces[block][top, at : at + width] = terms[m * rows : (m + 1) * rows]
         at += width
     for m in range(count):
-        pieces[m][:, at:] = squares[m * rows : (m + 1) * rows]
+        block, top = place_of(m, count, rows)
+        pieces[block][top, at:] = squares[m * rows : (m + 1) * rows]
     for move in moves:
         move.wait()
 
 
-def attend_kernel(count, key_width, steps, *refs):
-    pieces, (log_decay_in, state_in, out_gain_in) = refs[:count], refs[count : count + 3]
-    mixed_out, keep_out, key_out, value_out = refs[count + 3 : count + 7]
-    log_decay, state, out_gain, attended, sems = refs[count + 7 :]
+def load_kernel(*refs):
+    loads = [pltpu.make_async_copy(refs[j], refs[3 + j], refs[6].at[j]) for j in range(3)]
+    for load in loads:
+        load.start()
+    for load in loads:
+        load.wait()
+
+
+def update_kernel(steps, state, keep, keys, values, out, fresh, sems):
     rows, heads = state.shape[:2]
     some = rows // steps
-    loads = [
-        pltpu.make_async_copy(log_decay_in, log_decay, sems.at[0]),
-        pltpu.make_async_copy(out_gain_in, out_gain, sems.at[1]),
-    ] + [
-        pltpu.make_async_copy(
-            state_in.at[pl.ds(i * some, some)], state.at[pl.ds(i * some, some)], sems.at[2 + i]
-        )
-        for i in range(steps)
-    ]
-    for load in loads:
-        load.start()
+    keep_columns = [keep[:, h * DK : (h + 1) * DK].T for h in range(heads)]
+    key_columns = [keys[:, h * DK : (h + 1) * DK].T for h in range(heads)]
+    stores = []
+    for i in range(steps):
+        for b in range(i * some, (i + 1) * some):
+            for h in range(heads):
+                fresh[b, h] = (
+                    keep_columns[h][:, b : b + 1] * state[b, h]
+                    + key_columns[h][:, b : b + 1] * values[b : b + 1, h * DV : (h + 1) * DV]
+                )
+        part = pl.ds(i * some, some)
+        stores.append(pltpu.make_async_copy(fresh.at[part], out.at[part], sems.at[i]))
+        stores[-1].start()
+    for store in stores:
+        store.wait()
+
+
+def attend_kernel(count, key_width, *refs):
+    pieces, (log_decay, state, out_gain) = refs[:count], refs[count : count + 3]
+    mixed_out, keep_out, key_out, value_out, attended = refs[count + 3 :]
+    rows, heads = state.shape[:2]
     terms = wide(pieces[0][...])
     for piece in pieces[1:]:
-        terms = terms + wide(piece[...])
+        terms = terms + wide(piece[:rows])
     inv = lax.rsqrt(joined_squares(terms[:, -LANES:]) / D + eps)
     terms = terms * inv
     value_width = heads * DV
@@ -167,19 +203,15 @@
     log_sigmoid = jnp.minimum(decay_pre, 0.0) - jnp.log1p(jnp.exp(-jnp.abs(decay_pre)))
     key_out[...] = keys
     value_out[...] = values
-    for load in loads[:2]:
-        load.wait()
     keep = jnp.exp(log_sigmoid / gate_norm + log_decay[...])
     keep_out[...] = keep
     kept = query * keep
     columns = [kept[:, h * DK : (h + 1) * DK].T for h in range(heads)]
-    for i in range(steps):
-        loads[2 + i].wait()
-        for b in range(i * some, (i + 1) * some):
-            for h in range(heads):
-                attended[b : b + 1, h * DV : (h + 1) * DV] = jnp.sum(
-                    columns[h][:, b : b + 1] * state[b, h], axis=0, keepdims=True
-                )
+    for b in range(rows):
+        for h in range(heads):
+            attended[b : b + 1, h * DV : (h + 1) * DV] = jnp.sum(
+                columns[h][:, b : b + 1] * state[b, h], axis=0, keepdims=True
+            )
     for h in range(heads):
         lanes = slice(h * DK, (h + 1) * DK)
         outs = slice(h * DV, (h + 1) * DV)
@@ -202,48 +234,62 @@
 
 def middle_kernel(n_even, n_odd, *refs):
     evens, odds = refs[:n_even], refs[n_even : n_even + n_odd]
-    tokens, pair, mixer_gain, ffgate, ffup, gate_pair, up_pair = refs[n_even + n_odd :][:7]
-    middle_out, *pieces = refs[n_even + n_odd + 7 :]
+    tokens, pair, mixer_gain, ffgate, sent = refs[n_even + n_odd :][:5]
+    middle_out, own_out, other_out, *pieces = refs[n_even + n_odd + 5 :]
     me = lax.axis_index("kv")
     batch, model = tokens.shape
-    half = gate_pair.shape[1]
+    half = ffgate.shape[1] // 2
     count = 2 * len(pieces)
     rows = batch // count
     even = sum(wide(ref[...]) for ref in evens)
     odd = sum(wide(ref[...]) for ref in odds)
 
+    def pair_block(m):
+        return pair[(m ^ 1) * rows : ((m ^ 1) + 1) * rows]
+
     def stream(stay, first, second):
         blocks = []
         for m in range(count):
             source = first if m % 2 == 0 else second
-            blocks.append(
-                wide(block_of(stay, me, m, rows)) + source[m // 2 * rows : (m // 2 + 1) * rows]
-            )
+            blocks.append(wide(stay(m)) + source[m // 2 * rows : (m // 2 + 1) * rows])
         return wide(jnp.concatenate(blocks, axis=0).astype(jnp.bfloat16))
 
-    own = stream(tokens, even[:, :model], odd[:, model:])
-    other = stream(pair, even[:, model:], odd[:, :model])
+    own = stream(lambda m: block_of(tokens, me, m, rows), even[:, :model], odd[:, model:])
+    other = stream(pair_block, even[:, model:], odd[:, :model])
     middle_out[...] = own.astype(jnp.bfloat16)
     own2 = (own * row(mixer_gain)).astype(jnp.bfloat16)
     other2 = (other * wide(pair[batch : batch + 1])).astype(jnp.bfloat16)
+    own_out[...] = own2
+    other_out[...] = other2
     squares = jnp.sum(own * own, axis=1, keepdims=True) + jnp.sum(other * other, axis=1, keepdims=True)
     squares = split_squares(squares)
     kept = pl.ds(pl.multiple_of(lax.rem(me, 2) * half, half), half)
-    gate = (dot(own2, ffgate[:, kept]) + dot(other2, gate_pair[...])).astype(jnp.bfloat16)
-    upper = (dot(own2, ffup[:, kept]) + dot(other2, up_pair[...])).astype(jnp.bfloat16)
+    gate = (dot(own2, ffgate[:, kept]) + dot(other2, sent[:, :half])).astype(jnp.bfloat16)
     for i, piece in enumerate(pieces):
         part = slice(2 * i * rows, 2 * (i + 1) * rows)
         piece[:, :half] = gate[part]
-        piece[:, half : 2 * half] = upper[part]
-        piece[:, 2 * half :] = squares[part]
+        piece[:, half:] = squares[part]
+
+
+def upper_kernel(own2, other2, ffup, early, late, *pieces):
+    half = ffup.shape[1] // 2
+    first = half - late.shape[1]
+    rows = own2.shape[0] // len(pieces)
+    kept = pl.ds(pl.multiple_of(lax.rem(lax.axis_index("kv"), 2) * half, half), half)
+    upper = dot(own2[...], ffup[:, kept])
+    for columns, weight in ((slice(0, first), early[:, half:]), (slice(first, half), late[...])):
+        part = (upper[:, columns] + dot(other2[...], weight)).astype(jnp.bfloat16)
+        for i, piece in enumerate(pieces):
+            piece[:, columns] = part[i * rows : (i + 1) * rows]
 
 
 def hidden_kernel(count, *refs):
-    pieces, out = refs[:count], refs[count]
+    gates, uppers, out = refs[:count], refs[count : 2 * count], refs[2 * count]
     half = out.shape[1]
-    terms = sum(wide(piece[...]) for piece in pieces)
-    inv = lax.rsqrt(joined_squares(terms[:, 2 * half :]) / D + eps)
-    hidden = jax.nn.silu(terms[:, :half] * inv) * (terms[:, half : 2 * half] * inv)
+    gate = sum(wide(piece[...]) for piece in gates)
+    upper = sum(wide(piece[...]) for piece in uppers)
+    inv = lax.rsqrt(joined_squares(gate[:, half:]) / D + eps)
+    hidden = jax.nn.silu(gate[:, :half] * inv) * (upper * inv)
     out[...] = hidden.astype(jnp.bfloat16)
 
 
@@ -269,7 +315,6 @@
     kv, tp, both = {"kv": n_kv}, {"tp": n_tp}, {"kv": n_kv, "tp": n_tp}
     me = lax.axis_index("kv")
     rows = state.shape[0]
-    heads = state.shape[1]
     key_width = w_query.shape[1]
     value_width = w_value.shape[1]
     model = tokens.shape[1]
@@ -278,55 +323,67 @@
     batch = tokens.shape[0]
     attn_weights = (w_query, w_key, w_value, w_gate, w_decay)
     total_width = sum(w.shape[1] for w in attn_weights) + LANES
+    late = half * LATE // (6 * LANES) * LANES
     loaded = (tokens, norm_gain, mixer_gain) + attn_weights
     made = call(
         functools.partial(project_kernel, n_kv, rows),
-        [shape((rows, total_width))] * n_kv
-        + [shape((model, half))] * 2
+        [shape((rows + (m == 1) * rows, total_width)) for m in range(n_kv - 1)]
+        + [shape((model, half + half - late)), shape((model, late))]
         + [shape((half, model)), shape((batch + rows, model))],
         *in_hbm(*loaded, w_ffgate, w_ffup, w_down),
         specs=[HBM] * 11,
-        out_specs=[VMEM] * (n_kv + 4),
+        out_specs=[VMEM] * (n_kv + 3),
         scratch=[pltpu.VMEM(w.shape, w.dtype) for w in loaded]
-        + [pltpu.SemaphoreType.DMA((11,))],
-    )
-    pieces, (gate_sent, up_sent, down_sent, pair_sent) = made[:n_kv], made[n_kv:]
-    gate_pair = send_xor(gate_sent, kv, (1,))
-    order = [m for m in range(2, n_kv, 2)][::-1] + [m for m in range(1, n_kv, 2)][::-1]
+        + [pltpu.SemaphoreType.DMA((12,))],
+    )
+    pieces, (early_sent, late_sent, down_sent, pair_sent) = made[: n_kv - 1], made[n_kv - 1 :]
+    order = order_of(SCATTER, range(1, n_kv - 1))
     came = {}
-    for m in order:
-        came[m] = send_xor(pieces[m], kv, (m,))
+    came[1] = send_xor(pieces[1], kv, (1,))
+    relayed = call(relay_kernel, shape((rows, total_width)), pieces[n_kv - 2], came[1])
+    for m in order[1:]:
+        came[m] = send_xor(relayed if m == n_kv - 2 else pieces[m], kv, (m,))
     out_pair = send_xor(w_out, kv, (1,))
-    up_pair = send_xor(up_sent, kv, (1,))
+    early_pair = send_xor(early_sent, kv, (1,))
     pair = send_xor(pair_sent, kv, (1,))
+    late_pair = send_xor(late_sent, kv, (1,))
     down_pair = send_xor(down_sent, kv, (1,))
+    state_near, log_decay_near, out_gain_near = call(
+        load_kernel,
+        [pltpu.VMEM(x.shape, x.dtype) for x in (state, log_decay, out_gain)],
+        *in_hbm(state, log_decay, out_gain),
+        specs=[HBM] * 3,
+        scratch=[pltpu.SemaphoreType.DMA((3,))],
+    )
 
     mixed, keep, keys, values = call(
-        functools.partial(attend_kernel, n_kv, key_width, STEPS),
+        functools.partial(attend_kernel, n_kv - 1, key_width),
         [shape((rows, value_width))]
         + [shape((rows, w), jnp.float32) for w in (key_width, key_width, value_width)],
         pieces[0],
         *[came[m] for m in order],
-        *in_hbm(log_decay, state, out_gain),
-        specs=[VMEM] * n_kv + [HBM] * 3,
-        scratch=[
-            pltpu.VMEM(log_decay.shape, jnp.float32),
-            pltpu.VMEM(state.shape, jnp.float32),
-            pltpu.VMEM(out_gain.shape, jnp.float32),
-            pltpu.VMEM((rows, value_width), jnp.float32),
-            pltpu.SemaphoreType.DMA((2 + STEPS,)),
-        ],
-        grant=12 << 20,
+        log_decay_near,
+        state_near,
+        out_gain_near,
+        scratch=[pltpu.VMEM((rows, value_width), jnp.float32)],
     )
 
     evens = list(range(2, n_kv, 2))
     blocks = {}
-    for m in evens[::-1]:
+    for m in order_of(NEAR, evens):
         blocks[m] = send_xor(mixed, kv, (m,))
-    new_state = (
-        state * keep.reshape(rows, heads, DK)[..., None]
-        + keys.reshape(rows, heads, DK)[..., None]
-        * values.reshape(rows, heads, DV)[:, :, None, :]
+    new_state = call(
+        functools.partial(update_kernel, STEPS),
+        shape(state.shape, jnp.float32),
+        state_near,
+        keep,
+        keys,
+        values,
+        out_specs=HBM,
+        scratch=[
+            pltpu.VMEM(state.shape, jnp.float32),
+            pltpu.SemaphoreType.DMA((STEPS,)),
+        ],
     )
     chip = call(
         functools.partial(rows_kernel, n_kv // 2),
@@ -344,26 +401,36 @@
         if m:
             even.append(send_xor(sent, both, (0, m)))
 
-    middle, *parts = call(
+    middle, own2, other2, *gates = call(
         functools.partial(middle_kernel, len(even), len(odd)),
-        [shape((batch, model))] + [shape((2 * rows, 2 * half + LANES))] * (n_kv // 2),
+        [shape((batch, model))] * 3 + [shape((2 * rows, half + LANES))] * (n_kv // 2),
         *even,
         *odd,
         tokens,
         pair,
         mixer_gain,
         w_ffgate,
+        early_pair,
+    )
+    terms2 = [gates[0]]
+    for m in order_of(FF_GATE, evens):
+        terms2.append(send_xor(gates[m // 2], kv, (m,)))
+    uppers = call(
+        upper_kernel,
+        [shape((2 * rows, half))] * (n_kv // 2),
+        own2,
+        other2,
         w_ffup,
-        gate_pair,
-        up_pair,
-    )
-    terms2 = [parts[0]]
-    for m in evens[::-1]:
-        terms2.append(send_xor(parts[m // 2], kv, (m,)))
+        early_pair,
+        late_pair,
+    )
+    terms2.append(uppers[0])
+    for m in order_of(FF_UP, evens):
+        terms2.append(send_xor(uppers[m // 2], kv, (m,)))
     hidden = call(functools.partial(hidden_kernel, n_kv // 2), shape((2 * rows, half)), *terms2)
 
     blocks = {}
-    for m in evens[::-1]:
+    for m in order_of(HIDDEN, evens):
         blocks[m] = send_xor(hidden, kv, (m,))
     down = call(
         functools.partial(rows_kernel, n_kv // 2),
@@ -387,6 +454,12 @@
     return (swap_blocks(result, me, n_kv), new_state)
 
 
+def order_of(wanted, masks):
+    if sorted(wanted) == sorted(masks):
+        return list(wanted)
+    return [m for m in masks if m == 1] + [m for m in masks if m != 1][::-1]
+
+
 def solution(mesh):
     return jax.shard_map(
         body,

time: 102 us -> 94.2 us (0.924)
  waiting for transfers between devices: 51 us -> 39.9 us
  other arithmetic: 5.04 us -> 0.83 us
  Pallas kernels: 5.66 us -> 9.08 us
  starting transfers between devices: 38.7 us -> 41 us
  local copies, waits for them, and re-layouts: 0.12 us -> 2.27 us
    ppermute x23 -> x25, waiting for transfers between devices: 36.1 us -> 22.7 us  [send_xor(): return lax.ppermute(array, axis, pairs)]
    add x1 -> x0, other arithmetic: 4.21 us -> none  [body(): state * keep.reshape(rows, heads, DK)[..., None]]
    pallas_call x6 -> x10, Pallas kernels: 5.66 us -> 9.08 us  [call(): pl.pallas_call(kernel, out_shape=outs, in_specs=specs or [VMEM] * len(arg...]
    ppermute x6, waiting for transfers between devices: 14.9 us -> 17.2 us  [send_xor(): return lax.ppermute(array, (first, second), pairs)]
    unnamed x12 -> x16, local copies, waits for them, and re-layouts: 0.02 us -> 2.22 us
    ppermute x6, starting transfers between devices: 6.69 us -> 8.01 us  [send_xor(): return lax.ppermute(array, (first, second), pairs)]
    ppermute x23 -> x25, starting transfers between devices: 32 us -> 33 us  [send_xor(): return lax.ppermute(array, axis, pairs)]
  transfers between devices with their start and end apart: 29 -> 31, of which waited for: 16 -> 15; matrix products, arithmetic and copies ran while one was open for 4% -> 0% of each run, Pallas kernels for 5% -> 9%
where the time goes in v2:
time: 94.2 us; the launch traced here: 94.1 us
  starting transfers between devices  41 us (44%)
  waiting for transfers between devices  39.9 us (42%)
  Pallas kernels  9.08 us (10%)
  local copies, waits for them, and re-layouts  2.27 us (2%)
  between operations  0.95 us (1%)
    ppermute x25, starting transfers between devices, send_xor(): return lax.ppermute(array, axis, pairs)  33 us
    ppermute x25, waiting for transfers between devices, send_xor(): return lax.ppermute(array, axis, pairs)  22.7 us
    ppermute x6, waiting for transfers between devices, send_xor(): return lax.ppermute(array, (first, second), pairs)  17.2 us
    pallas_call x10, Pallas kernels, call(): pl.pallas_call(kernel, out_shape=outs, in_specs=specs or [VMEM] * len(arg...  9.08 us
    ppermute x6, starting transfers between devices, send_xor(): return lax.ppermute(array, (first, second), pairs)  8.01 us
    unnamed x16, local copies, waits for them, and re-layouts  2.22 us
  transfers between devices with their start and end apart: 31, of which 15 were waited for; matrix products, arithmetic and copies ran while one was open for 0% of the time, Pallas kernels for 9%

profile of v2, /device:TPU:0, one launch (start us, length us, event | category | flops | bytes accessed | tf_op | source)
XLA Modules:
  0.0 94.1 jit_solution(8934934722418284371)
XLA Ops:
  0.6 3.0 %collective-permute-start.9 = (bf16[512,256]{1,0:T(8,128)(2,1)}, bf16[512,256]{1,0:T(8,128)(2,1)S(1)}, u32[]{:S(2)}, u32[]{:S(2)}) collective-permute-start(bf16[512,256]{1,0:T(8,128)(2,1)} %refs_4_.4), channel_id=1, source_target_pairs={{0,4},{4,0},{8,12},{12,8},{16,20},{20,16},{24,28},{28,24},{1,5},{5... | collective-permute-start | bytes 786440 | tf_op jit(solution)/shard_map/ppermute | solution.py:43
  3.7 2.0 %shard_map.158 = (bf16[16,1920]{1,0:T(8,128)(2,1)S(1)}, bf16[32,1920]{1,0:T(8,128)(2,1)S(1)}, bf16[16,1920]{1,0:T(8,128)(2,1)S(1)}, bf16[16,1920]{1,0:T(8,128)(2...) custom-call(bf16[128,256]{1,0:T(8,128)(2,1)} %refs_5_.3, ...), custom_call_target="tpu_custom_call" | custom-call | tf_op jit(solution)/shard_map/pallas_call | solution.py:77
  5.7 0.1 collective-permute-start
  5.8 3.1 %collective-permute-start.1 = (bf16[16,1920]{1,0:T(8,128)(2,1)S(1)}, bf16[16,1920]{1,0:T(8,128)(2,1)S(1)}, u32[]{:S(2)}, u32[]{:S(2)}) collective-permute-start(bf16[16,1920]{1,0:T(8,128)(2,1)S(1)} %get-tuple-element.33), channel_id=1, source_target_pairs={{0,16},{4,20},{8,24},{12,28},{16,0},{20,4},{24,8},{28,12},{1,17},{... | collective-permute-start | bytes 184328 | tf_op jit(solution)/shard_map/ppermute | solution.py:43
  8.9 1.3 %collective-permute-start.2 = (bf16[16,1920]{1,0:T(8,128)(2,1)S(1)}, bf16[16,1920]{1,0:T(8,128)(2,1)S(1)}, u32[]{:S(2)}, u32[]{:S(2)}) collective-permute-start(bf16[16,1920]{1,0:T(8,128)(2,1)S(1)} %get-tuple-element.34), channel_id=1, source_target_pairs={{0,20},{4,16},{8,28},{12,24},{16,4},{20,0},{24,12},{28,8},{1,21},{... | collective-permute-start | bytes 184328 | tf_op jit(solution)/shard_map/ppermute | solution.py:43
  10.1 0.2 collective-permute-start.15
  10.4 4.0 %collective-permute-done.came.refs_1_ = bf16[32,1920]{1,0:T(8,128)(2,1)S(1)} collective-permute-done((bf16[32,1920]{1,0:T(8,128)(2,1)S(1)}, bf16[32,1920]{1,0:T(8,128)(2,1)S(1)}, u32[]{:S(2)}, u32[]{:S(2)}) %collective-permute-start) | collective-permute-done | bytes 122912 | tf_op jit(solution)/shard_map/ppermute | solution.py:43
  14.4 3.6 %collective-permute-start.3 = (bf16[16,1920]{1,0:T(8,128)(2,1)S(1)}, bf16[16,1920]{1,0:T(8,128)(2,1)S(1)}, u32[]{:S(2)}, u32[]{:S(2)}) collective-permute-start(bf16[16,1920]{1,0:T(8,128)(2,1)S(1)} %get-tuple-element.35), channel_id=1, source_target_pairs={{0,12},{4,8},{8,4},{12,0},{16,28},{20,24},{24,20},{28,16},{1,13},{... | collective-permute-start | bytes 184328 | tf_op jit(solution)/shard_map/ppermute | solution.py:43
  18.0 0.2 shard_map.159
  18.2 0.0 copy-start.6
  18.2 0.0 copy-start.7
  18.2 0.5 collective-permute-start.5
  18.7 3.6 %collective-permute-start.4 = (bf16[16,1920]{1,0:T(8,128)(2,1)S(1)}, bf16[16,1920]{1,0:T(8,128)(2,1)S(1)}, u32[]{:S(2)}, u32[]{:S(2)}) collective-permute-start(bf16[16,1920]{1,0:T(8,128)(2,1)S(1)} %shard_map.159), channel_id=1, source_target_pairs={{0,24},{4,28},{8,16},{12,20},{16,8},{20,12},{24,0},{28,4},{1,25},{... | collective-permute-start | bytes 184328 | tf_op jit(solution)/shard_map/ppermute | solution.py:43
  22.3 2.2 %shard_map.160 = (f32[16,2,128,256]{3,2,1,0:T(8,128)S(1)}, f32[16,256]{1,0:T(8,128)S(1)}, f32[256]{0:T(256)S(1)}) custom-call(f32[16,2,128,256]{3,2,1,0:T(8,128)} %refs_0_.3, f32[16,256]{1,0:T(8,128)} %refs_1_.3, f32[256]{0:T(256)} %refs_2_.3), custom_call_target="tpu_custom_call" | custom-call | tf_op jit(solution)/shard_map/pallas_call | solution.py:77
  24.5 0.0 copy-start
  24.6 0.0 copy-start.4
  24.6 0.0 collective-permute-done.3.refs_4_
  24.6 0.0 collective-permute-done.5.refs_6_
  24.6 0.7 collective-permute-done.4.refs_5_
  25.2 1.1 %shard_map.161 = (bf16[16,512]{1,0:T(8,128)(2,1)S(1)}, f32[16,256]{1,0:T(8,128)S(1)}, f32[16,256]{1,0:T(8,128)S(1)}, f32[16,512]{1,0:T(8,128)S(1)}) custom-call(bf16[16,1920]{1,0:T(8,128)(2,1)S(1)} %get-tuple-element.31.refs_0_, bf16[32,1920]{1,0:T(8,128)(2,1)S(1)} %collective-permute-done.came.refs_1_, bf16[16,1920]{1,0:T(8,128)(2,1)S(1)} %collective-permute-done.1.refs_2_, ...), custom_call_target="tpu_custom_call" | custom-call | tf_op jit(solution)/shard_map/pallas_call | solution.py:77
  26.3 0.1 collective-permute-start.6
  26.4 3.7 %collective-permute-start.7 = (bf16[16,512]{1,0:T(8,128)(2,1)S(1)}, bf16[16,512]{1,0:T(8,128)(2,1)S(1)}, u32[]{:S(2)}, u32[]{:S(2)}) collective-permute-start(bf16[16,512]{1,0:T(8,128)(2,1)S(1)} %get-tuple-element.41.refs_0_), channel_id=1, source_target_pairs={{0,16},{4,20},{8,24},{12,28},{16,0},{20,4},{24,8},{28,12},{1,17},{... | collective-permute-start | bytes 49160 | tf_op jit(solution)/shard_map/ppermute | solution.py:43
  30.0 0.7 collective-permute-start.8
  30.8 1.0 %collective-permute-done.7.refs_2_ = bf16[16,512]{1,0:T(8,128)(2,1)S(1)} collective-permute-done((bf16[16,512]{1,0:T(8,128)(2,1)S(1)}, bf16[16,512]{1,0:T(8,128)(2,1)S(1)}, u32[]{:S(2)}, u32[]{:S(2)}) %collective-permute-start.7) | collective-permute-done | bytes 16416 | tf_op jit(solution)/shard_map/ppermute | solution.py:43
  31.8 3.8 %collective-permute-done.8.refs_3_ = bf16[16,512]{1,0:T(8,128)(2,1)S(1)} collective-permute-done((bf16[16,512]{1,0:T(8,128)(2,1)S(1)}, bf16[16,512]{1,0:T(8,128)(2,1)S(1)}, u32[]{:S(2)}, u32[]{:S(2)}) %collective-permute-start.8) | collective-permute-done | bytes 16416 | tf_op jit(solution)/shard_map/ppermute | solution.py:43
  35.6 0.2 shard_map.162.refs_0_
  35.8 0.1 collective-permute-start.10
  35.9 0.6 collective-permute-start.14
  36.5 1.5 %collective-permute-start.19 = (bf16[256,512]{1,0:T(8,128)(2,1)S(1)}, bf16[256,512]{1,0:T(8,128)(2,1)S(1)}, u32[]{:S(2)}, u32[]{:S(2)}) collective-permute-start(bf16[256,512]{1,0:T(8,128)(2,1)S(1)} %get-tuple-element.51), channel_id=1, source_target_pairs={{0,4},{4,0},{8,12},{12,8},{16,20},{20,16},{24,28},{28,24},{1,5},{5... | collective-permute-start | bytes 786440 | tf_op jit(solution)/shard_map/ppermute | solution.py:43
  38.0 0.5 collective-permute-start.26
  38.5 1.6 %collective-permute-start.11 = (bf16[64,512]{1,0:T(8,128)(2,1)S(1)}, bf16[64,512]{1,0:T(8,128)(2,1)S(1)}, u32[]{:S(2)}, u32[]{:S(2)}) collective-permute-start(bf16[64,512]{1,0:T(8,128)(2,1)S(1)} %add_convert_fusion), channel_id=1, source_target_pairs={{0,2},{1,3},{2,0},{3,1},{4,6},{5,7},{6,4},{7,5},{8,10},{9,11},{10,... | collective-permute-start | bytes 196616 | tf_op jit(solution)/shard_map/ppermute | solution.py:50
  40.1 1.0 %collective-permute-done.14.refs_6_ = bf16[144,256]{1,0:T(8,128)(2,1)S(1)} collective-permute-done((bf16[144,256]{1,0:T(8,128)(2,1)S(1)}, bf16[144,256]{1,0:T(8,128)(2,1)S(1)}, u32[]{:S(2)}, u32[]{:S(2)}) %collective-permute-start.14) | collective-permute-done | bytes 73760 | tf_op jit(solution)/shard_map/ppermute | solution.py:43
  41.1 1.3 %collective-permute-start.12 = (bf16[64,512]{1,0:T(8,128)(2,1)S(1)}, bf16[64,512]{1,0:T(8,128)(2,1)S(1)}, u32[]{:S(2)}, u32[]{:S(2)}) collective-permute-start(bf16[64,512]{1,0:T(8,128)(2,1)S(1)} %add_convert_fusion), channel_id=1, source_target_pairs={{0,6},{1,7},{2,4},{3,5},{4,2},{5,3},{6,0},{7,1},{8,14},{9,15},{10,... | collective-permute-start | bytes 196616 | tf_op jit(solution)/shard_map/ppermute | solution.py:50
  42.4 0.5 collective-permute-done.11.refs_2_
  42.9 1.5 %collective-permute-start.13 = (bf16[64,512]{1,0:T(8,128)(2,1)S(1)}, bf16[64,512]{1,0:T(8,128)(2,1)S(1)}, u32[]{:S(2)}, u32[]{:S(2)}) collective-permute-start(bf16[64,512]{1,0:T(8,128)(2,1)S(1)} %add_convert_fusion), channel_id=1, source_target_pairs={{0,4},{1,5},{2,6},{3,7},{4,0},{5,1},{6,2},{7,3},{8,12},{9,13},{10,... | collective-permute-start | bytes 196616 | tf_op jit(solution)/shard_map/ppermute | solution.py:50
  44.4 13.1 %collective-permute-done.12.refs_3_ = bf16[64,512]{1,0:T(8,128)(2,1)S(1)} collective-permute-done((bf16[64,512]{1,0:T(8,128)(2,1)S(1)}, bf16[64,512]{1,0:T(8,128)(2,1)S(1)}, u32[]{:S(2)}, u32[]{:S(2)}) %collective-permute-start.12) | collective-permute-done | bytes 65568 | tf_op jit(solution)/shard_map/ppermute | solution.py:50
  57.5 0.0 collective-permute-done.13.refs_4_
  57.5 0.3 shard_map.163
  57.8 0.0 collective-permute-done.19.late
  57.9 0.3 shard_map.164
  58.2 0.8 collective-permute-start.20
  58.9 0.0 collective-permute-start.21
  58.9 3.1 %collective-permute-start.16 = (bf16[32,896]{1,0:T(8,128)(2,1)S(1)}, bf16[32,896]{1,0:T(8,128)(2,1)S(1)}, u32[]{:S(2)}, u32[]{:S(2)}) collective-permute-start(bf16[32,896]{1,0:T(8,128)(2,1)S(1)} %get-tuple-element.46), channel_id=1, source_target_pairs={{0,24},{4,28},{8,16},{12,20},{16,8},{20,12},{24,0},{28,4},{1,25},{... | collective-permute-start | bytes 172040 | tf_op jit(solution)/shard_map/ppermute | solution.py:43
  62.1 2.0 %collective-permute-start.17 = (bf16[32,896]{1,0:T(8,128)(2,1)S(1)}, bf16[32,896]{1,0:T(8,128)(2,1)S(1)}, u32[]{:S(2)}, u32[]{:S(2)}) collective-permute-start(bf16[32,896]{1,0:T(8,128)(2,1)S(1)} %get-tuple-element.47), channel_id=1, source_target_pairs={{0,16},{4,20},{8,24},{12,28},{16,0},{20,4},{24,8},{28,12},{1,17},{... | collective-permute-start | bytes 172040 | tf_op jit(solution)/shard_map/ppermute | solution.py:43
  64.1 0.3 collective-permute-done.20.refs_5_
  64.4 3.4 %collective-permute-done.21.refs_6_ = bf16[32,768]{1,0:T(8,128)(2,1)S(1)} collective-permute-done((bf16[32,768]{1,0:T(8,128)(2,1)S(1)}, bf16[32,768]{1,0:T(8,128)(2,1)S(1)}, u32[]{:S(2)}, u32[]{:S(2)}) %collective-permute-start.21) | collective-permute-done | bytes 49184 | tf_op jit(solution)/shard_map/ppermute | solution.py:43
  67.8 4.1 %collective-permute-done.22.refs_7_ = bf16[32,768]{1,0:T(8,128)(2,1)S(1)} collective-permute-done((bf16[32,768]{1,0:T(8,128)(2,1)S(1)}, bf16[32,768]{1,0:T(8,128)(2,1)S(1)}, u32[]{:S(2)}, u32[]{:S(2)}) %collective-permute-start.22) | collective-permute-done | bytes 49184 | tf_op jit(solution)/shard_map/ppermute | solution.py:43
  71.9 0.2 shard_map.165.refs_0_
  72.0 0.1 collective-permute-start.23
  72.1 1.6 %collective-permute-start.24 = (bf16[32,768]{1,0:T(8,128)(2,1)S(1)}, bf16[32,768]{1,0:T(8,128)(2,1)S(1)}, u32[]{:S(2)}, u32[]{:S(2)}) collective-permute-start(bf16[32,768]{1,0:T(8,128)(2,1)S(1)} %shard_map.165.refs_0_), channel_id=1, source_target_pairs={{0,16},{4,20},{8,24},{12,28},{16,0},{20,4},{24,8},{28,12},{1,17},{... | collective-permute-start | bytes 147464 | tf_op jit(solution)/shard_map/ppermute | solution.py:43
  73.7 2.8 %collective-permute-start.25 = (bf16[32,768]{1,0:T(8,128)(2,1)S(1)}, bf16[32,768]{1,0:T(8,128)(2,1)S(1)}, u32[]{:S(2)}, u32[]{:S(2)}) collective-permute-start(bf16[32,768]{1,0:T(8,128)(2,1)S(1)} %shard_map.165.refs_0_), channel_id=1, source_target_pairs={{0,24},{4,28},{8,16},{12,20},{16,8},{20,12},{24,0},{28,4},{1,25},{... | collective-permute-start | bytes 147464 | tf_op jit(solution)/shard_map/ppermute | solution.py:43
  76.5 0.1 collective-permute-done.23.refs_1_
  76.6 0.6 collective-permute-done.24.refs_2_
  77.2 2.4 %collective-permute-done.25.refs_3_ = bf16[32,768]{1,0:T(8,128)(2,1)S(1)} collective-permute-done((bf16[32,768]{1,0:T(8,128)(2,1)S(1)}, bf16[32,768]{1,0:T(8,128)(2,1)S(1)}, u32[]{:S(2)}, u32[]{:S(2)}) %collective-permute-start.25) | collective-permute-done | bytes 49184 | tf_op jit(solution)/shard_map/ppermute | solution.py:43
  79.6 0.3 shard_map.166
  79.9 0.1 collective-permute-start.27
  80.0 1.3 %collective-permute-done.27 = bf16[128,512]{1,0:T(8,128)(2,1)S(1)} collective-permute-done((bf16[128,512]{1,0:T(8,128)(2,1)S(1)}, bf16[128,512]{1,0:T(8,128)(2,1)S(1)}, u32[]{:S(2)}, u32[]{:S(2)}) %collective-permute-start.27) | collective-permute-done | bytes 131104 | tf_op jit(solution)/shard_map/ppermute | solution.py:43
  81.3 0.5 collective-permute-start.30
  81.9 2.4 %collective-permute-start.29 = (bf16[128,256]{1,0:T(8,128)(2,1)S(1)}, bf16[128,256]{1,0:T(8,128)(2,1)S(1)}, u32[]{:S(2)}, u32[]{:S(2)}) collective-permute-start(bf16[128,256]{1,0:T(8,128)(2,1)S(1)} %get-tuple-element.61), channel_id=1, source_target_pairs={{0,6},{1,7},{2,4},{3,5},{4,2},{5,3},{6,0},{7,1},{8,14},{9,15},{10,... | collective-permute-start | bytes 196616 | tf_op jit(solution)/shard_map/ppermute | solution.py:50
  84.3 2.2 %copy-done.1 = f32[16,2,128,256]{3,2,1,0:T(8,128)S(1)} copy-done((f32[16,2,128,256]{3,2,1,0:T(8,128)S(1)}, f32[16,2,128,256]{3,2,1,0:T(8,128)}, u32[]{:S(2)}) %copy-start.1) | copy-done | bytes 4194328
  86.5 2.4 %shard_map.167 = f32[16,2,128,256]{3,2,1,0:T(8,128)} custom-call(f32[16,2,128,256]{3,2,1,0:T(8,128)S(1)} %copy-done.1, f32[16,256]{1,0:T(8,128)S(1)} %get-tuple-element.57.keep, f32[16,256]{1,0:T(8,128)S(1)} %get-tuple-element.58.keys, f32[16,512]{1,0:T(8,128)S(1)} %get-tuple-element.59.values), custom_call_target="tpu_custom_call" | custom-call | tf_op jit(solution)/shard_map/pallas_call | solution.py:77
  88.9 0.7 collective-permute-start.28
  89.6 3.6 %collective-permute-done.28 = bf16[128,256]{1,0:T(8,128)(2,1)S(1)} collective-permute-done((bf16[128,256]{1,0:T(8,128)(2,1)S(1)}, bf16[128,256]{1,0:T(8,128)(2,1)S(1)}, u32[]{:S(2)}, u32[]{:S(2)}) %collective-permute-start.28) | collective-permute-done | bytes 65568 | tf_op jit(solution)/shard_map/ppermute | solution.py:50
  93.4 0.7 fusion.2
  (40 shorter events, 0.3 us)
Async XLA Ops:
  0.6 35.0 %collective-permute-start.9 = (bf16[512,256]{1,0:T(8,128)(2,1)}, bf16[512,256]{1,0:T(8,128)(2,1)S(1)}, u32[]{:S(2)}, u32[]{:S(2)}) collective-permute-start(bf16[512,256]{1,0:T(8,128)(2,1)} %refs_4_.4), channel_id=1, source_target_pairs={{0,4},{4,0},{8,12},{12,8},{16,20},{20,16},{24,28},{28,24},{1,5},{5... | collective-permute-start | bytes 786440 | tf_op jit(solution)/shard_map/ppermute | solution.py:43
  5.7 8.7 %collective-permute-start = (bf16[32,1920]{1,0:T(8,128)(2,1)S(1)}, bf16[32,1920]{1,0:T(8,128)(2,1)S(1)}, u32[]{:S(2)}, u32[]{:S(2)}) collective-permute-start(bf16[32,1920]{1,0:T(8,128)(2,1)S(1)} %get-tuple-element.32), channel_id=1, source_target_pairs={{0,4},{4,0},{8,12},{12,8},{16,20},{20,16},{24,28},{28,24},{1,5},{5... | collective-permute-start | bytes 368648 | tf_op jit(solution)/shard_map/ppermute | solution.py:43
  5.8 12.4 %collective-permute-start.1 = (bf16[16,1920]{1,0:T(8,128)(2,1)S(1)}, bf16[16,1920]{1,0:T(8,128)(2,1)S(1)}, u32[]{:S(2)}, u32[]{:S(2)}) collective-permute-start(bf16[16,1920]{1,0:T(8,128)(2,1)S(1)} %get-tuple-element.33), channel_id=1, source_target_pairs={{0,16},{4,20},{8,24},{12,28},{16,0},{20,4},{24,8},{28,12},{1,17},{... | collective-permute-start | bytes 184328 | tf_op jit(solution)/shard_map/ppermute | solution.py:43
  8.9 9.9 %collective-permute-start.2 = (bf16[16,1920]{1,0:T(8,128)(2,1)S(1)}, bf16[16,1920]{1,0:T(8,128)(2,1)S(1)}, u32[]{:S(2)}, u32[]{:S(2)}) collective-permute-start(bf16[16,1920]{1,0:T(8,128)(2,1)S(1)} %get-tuple-element.34), channel_id=1, source_target_pairs={{0,20},{4,16},{8,28},{12,24},{16,4},{20,0},{24,12},{28,8},{1,21},{... | collective-permute-start | bytes 184328 | tf_op jit(solution)/shard_map/ppermute | solution.py:43
  10.1 47.4 %collective-permute-start.15 = (bf16[256,1024]{1,0:T(8,128)(2,1)S(1)}, bf16[256,1024]{1,0:T(8,128)(2,1)S(1)}, u32[]{:S(2)}, u32[]{:S(2)}) collective-permute-start(bf16[256,1024]{1,0:T(8,128)(2,1)S(1)} %get-tuple-element.43), channel_id=1, source_target_pairs={{0,4},{4,0},{8,12},{12,8},{16,20},{20,16},{24,28},{28,24},{1,5},{5... | collective-permute-start | bytes 1572872 | tf_op jit(solution)/shard_map/ppermute | solution.py:43
  14.4 10.2 %collective-permute-start.3 = (bf16[16,1920]{1,0:T(8,128)(2,1)S(1)}, bf16[16,1920]{1,0:T(8,128)(2,1)S(1)}, u32[]{:S(2)}, u32[]{:S(2)}) collective-permute-start(bf16[16,1920]{1,0:T(8,128)(2,1)S(1)} %get-tuple-element.35), channel_id=1, source_target_pairs={{0,12},{4,8},{8,4},{12,0},{16,28},{20,24},{24,20},{28,16},{1,13},{... | collective-permute-start | bytes 184328 | tf_op jit(solution)/shard_map/ppermute | solution.py:43
  18.2 17.4 %copy-start.5 = (bf16[512,256]{1,0:T(8,128)(2,1)S(1)}, bf16[512,256]{1,0:T(8,128)(2,1)}, u32[]{:S(2)}) copy-start(bf16[512,256]{1,0:T(8,128)(2,1)} %refs_4_.4) | copy-start | bytes 786436
  18.2 39.3 %copy-start.3 = (bf16[256,1536]{1,0:T(8,128)(2,1)S(1)}, bf16[256,1536]{1,0:T(8,128)(2,1)}, u32[]{:S(2)}) copy-start(bf16[256,1536]{1,0:T(8,128)(2,1)} %refs_8_.3) | copy-start | bytes 2359300
  18.2 39.3 %copy-start.6 = (bf16[128,256]{1,0:T(8,128)(2,1)S(1)}, bf16[128,256]{1,0:T(8,128)(2,1)}, u32[]{:S(2)}) copy-start(bf16[128,256]{1,0:T(8,128)(2,1)} %refs_5_.3) | copy-start | bytes 196612
  18.2 39.3 %copy-start.7 = (bf16[256]{0:T(256)(128)(2,1)S(1)}, bf16[256]{0:T(256)(128)(2,1)}, u32[]{:S(2)}) copy-start(bf16[256]{0:T(256)(128)(2,1)} %refs_7_.3) | copy-start | bytes 1540
  18.2 6.4 %collective-permute-start.5 = (bf16[16,1920]{1,0:T(8,128)(2,1)S(1)}, bf16[16,1920]{1,0:T(8,128)(2,1)S(1)}, u32[]{:S(2)}, u32[]{:S(2)}) collective-permute-start(bf16[16,1920]{1,0:T(8,128)(2,1)S(1)} %get-tuple-element.37), channel_id=1, source_target_pairs={{0,8},{4,12},{8,0},{12,4},{16,24},{20,28},{24,16},{28,20},{1,9},{5... | collective-permute-start | bytes 184328 | tf_op jit(solution)/shard_map/ppermute | solution.py:43
  18.7 6.5 %collective-permute-start.4 = (bf16[16,1920]{1,0:T(8,128)(2,1)S(1)}, bf16[16,1920]{1,0:T(8,128)(2,1)S(1)}, u32[]{:S(2)}, u32[]{:S(2)}) collective-permute-start(bf16[16,1920]{1,0:T(8,128)(2,1)S(1)} %shard_map.159), channel_id=1, source_target_pairs={{0,24},{4,28},{8,16},{12,20},{16,8},{20,12},{24,0},{28,4},{1,25},{... | collective-permute-start | bytes 184328 | tf_op jit(solution)/shard_map/ppermute | solution.py:43
  24.5 33.6 %copy-start = (f32[16,2,128,256]{3,2,1,0:T(8,128)}, f32[16,2,128,256]{3,2,1,0:T(8,128)S(1)}, u32[]{:S(2)}) copy-start(f32[16,2,128,256]{3,2,1,0:T(8,128)S(1)} %get-tuple-element.39.refs_8_.state) | copy-start | bytes 12582916
  24.6 33.3 %copy-start.4 = (bf16[256,1536]{1,0:T(8,128)(2,1)S(1)}, bf16[256,1536]{1,0:T(8,128)(2,1)}, u32[]{:S(2)}) copy-start(bf16[256,1536]{1,0:T(8,128)(2,1)} %ffup.1) | copy-start | bytes 2359300
  25.2 54.4 %copy-start.2 = (bf16[1536,256]{1,0:T(8,128)(2,1)S(1)}, bf16[1536,256]{1,0:T(8,128)(2,1)}, u32[]{:S(2)}) copy-start(bf16[1536,256]{1,0:T(8,128)(2,1)} %refs_4_.5) | copy-start | bytes 2359300
  26.3 4.4 %collective-permute-start.6 = (bf16[16,512]{1,0:T(8,128)(2,1)S(1)}, bf16[16,512]{1,0:T(8,128)(2,1)S(1)}, u32[]{:S(2)}, u32[]{:S(2)}) collective-permute-start(bf16[16,512]{1,0:T(8,128)(2,1)S(1)} %get-tuple-element.41.refs_0_), channel_id=1, source_target_pairs={{0,8},{4,12},{8,0},{12,4},{16,24},{20,28},{24,16},{28,20},{1,9},{5... | collective-permute-start | bytes 49160 | tf_op jit(solution)/shard_map/ppermute | solution.py:43
  26.4 5.4 %collective-permute-start.7 = (bf16[16,512]{1,0:T(8,128)(2,1)S(1)}, bf16[16,512]{1,0:T(8,128)(2,1)S(1)}, u32[]{:S(2)}, u32[]{:S(2)}) collective-permute-start(bf16[16,512]{1,0:T(8,128)(2,1)S(1)} %get-tuple-element.41.refs_0_), channel_id=1, source_target_pairs={{0,16},{4,20},{8,24},{12,28},{16,0},{20,4},{24,8},{28,12},{1,17},{... | collective-permute-start | bytes 49160 | tf_op jit(solution)/shard_map/ppermute | solution.py:43
  30.0 5.5 %collective-permute-start.8 = (bf16[16,512]{1,0:T(8,128)(2,1)S(1)}, bf16[16,512]{1,0:T(8,128)(2,1)S(1)}, u32[]{:S(2)}, u32[]{:S(2)}) collective-permute-start(bf16[16,512]{1,0:T(8,128)(2,1)S(1)} %get-tuple-element.41.refs_0_), channel_id=1, source_target_pairs={{0,24},{4,28},{8,16},{12,20},{16,8},{20,12},{24,0},{28,4},{1,25},{... | collective-permute-start | bytes 49160 | tf_op jit(solution)/shard_map/ppermute | solution.py:43
  35.8 2.7 %collective-permute-start.10 = (bf16[64,512]{1,0:T(8,128)(2,1)S(1)}, bf16[64,512]{1,0:T(8,128)(2,1)S(1)}, u32[]{:S(2)}, u32[]{:S(2)}) collective-permute-start(bf16[64,512]{1,0:T(8,128)(2,1)S(1)} %shard_map.162.refs_0_), channel_id=1, source_target_pairs={{0,1},{1,0},{2,3},{3,2},{4,5},{5,4},{6,7},{7,6},{8,9},{9,8},{10,11... | collective-permute-start | bytes 196616 | tf_op jit(solution)/shard_map/ppermute | solution.py:43
  35.9 5.2 %collective-permute-start.14 = (bf16[144,256]{1,0:T(8,128)(2,1)S(1)}, bf16[144,256]{1,0:T(8,128)(2,1)S(1)}, u32[]{:S(2)}, u32[]{:S(2)}) collective-permute-start(bf16[144,256]{1,0:T(8,128)(2,1)S(1)} %get-tuple-element.42), channel_id=1, source_target_pairs={{0,4},{4,0},{8,12},{12,8},{16,20},{20,16},{24,28},{28,24},{1,5},{5... | collective-permute-start | bytes 221192 | tf_op jit(solution)/shard_map/ppermute | solution.py:43
  36.5 21.4 %collective-permute-start.19 = (bf16[256,512]{1,0:T(8,128)(2,1)S(1)}, bf16[256,512]{1,0:T(8,128)(2,1)S(1)}, u32[]{:S(2)}, u32[]{:S(2)}) collective-permute-start(bf16[256,512]{1,0:T(8,128)(2,1)S(1)} %get-tuple-element.51), channel_id=1, source_target_pairs={{0,4},{4,0},{8,12},{12,8},{16,20},{20,16},{24,28},{28,24},{1,5},{5... | collective-permute-start | bytes 786440 | tf_op jit(solution)/shard_map/ppermute | solution.py:43
  38.0 38.5 %collective-permute-start.26 = (bf16[768,256]{1,0:T(8,128)(2,1)S(1)}, bf16[768,256]{1,0:T(8,128)(2,1)S(1)}, u32[]{:S(2)}, u32[]{:S(2)}) collective-permute-start(bf16[768,256]{1,0:T(8,128)(2,1)S(1)} %get-tuple-element.56), channel_id=1, source_target_pairs={{0,4},{4,0},{8,12},{12,8},{16,20},{20,16},{24,28},{28,24},{1,5},{5... | collective-permute-start | bytes 1179656 | tf_op jit(solution)/shard_map/ppermute | solution.py:43
  38.5 4.3 %collective-permute-start.11 = (bf16[64,512]{1,0:T(8,128)(2,1)S(1)}, bf16[64,512]{1,0:T(8,128)(2,1)S(1)}, u32[]{:S(2)}, u32[]{:S(2)}) collective-permute-start(bf16[64,512]{1,0:T(8,128)(2,1)S(1)} %add_convert_fusion), channel_id=1, source_target_pairs={{0,2},{1,3},{2,0},{3,1},{4,6},{5,7},{6,4},{7,5},{8,10},{9,11},{10,... | collective-permute-start | bytes 196616 | tf_op jit(solution)/shard_map/ppermute | solution.py:50
  41.1 16.4 %collective-permute-start.12 = (bf16[64,512]{1,0:T(8,128)(2,1)S(1)}, bf16[64,512]{1,0:T(8,128)(2,1)S(1)}, u32[]{:S(2)}, u32[]{:S(2)}) collective-permute-start(bf16[64,512]{1,0:T(8,128)(2,1)S(1)} %add_convert_fusion), channel_id=1, source_target_pairs={{0,6},{1,7},{2,4},{3,5},{4,2},{5,3},{6,0},{7,1},{8,14},{9,15},{10,... | collective-permute-start | bytes 196616 | tf_op jit(solution)/shard_map/ppermute | solution.py:50
  42.9 14.6 %collective-permute-start.13 = (bf16[64,512]{1,0:T(8,128)(2,1)S(1)}, bf16[64,512]{1,0:T(8,128)(2,1)S(1)}, u32[]{:S(2)}, u32[]{:S(2)}) collective-permute-start(bf16[64,512]{1,0:T(8,128)(2,1)S(1)} %add_convert_fusion), channel_id=1, source_target_pairs={{0,4},{1,5},{2,6},{3,7},{4,0},{5,1},{6,2},{7,3},{8,12},{9,13},{10,... | collective-permute-start | bytes 196616 | tf_op jit(solution)/shard_map/ppermute | solution.py:50
  58.2 6.2 %collective-permute-start.20 = (bf16[32,768]{1,0:T(8,128)(2,1)S(1)}, bf16[32,768]{1,0:T(8,128)(2,1)S(1)}, u32[]{:S(2)}, u32[]{:S(2)}) collective-permute-start(bf16[32,768]{1,0:T(8,128)(2,1)S(1)} %get-tuple-element.53), channel_id=1, source_target_pairs={{0,24},{4,28},{8,16},{12,20},{16,8},{20,12},{24,0},{28,4},{1,25},{... | collective-permute-start | bytes 147464 | tf_op jit(solution)/shard_map/ppermute | solution.py:43
  58.9 8.8 %collective-permute-start.21 = (bf16[32,768]{1,0:T(8,128)(2,1)S(1)}, bf16[32,768]{1,0:T(8,128)(2,1)S(1)}, u32[]{:S(2)}, u32[]{:S(2)}) collective-permute-start(bf16[32,768]{1,0:T(8,128)(2,1)S(1)} %get-tuple-element.54), channel_id=1, source_target_pairs={{0,16},{4,20},{8,24},{12,28},{16,0},{20,4},{24,8},{28,12},{1,17},{... | collective-permute-start | bytes 147464 | tf_op jit(solution)/shard_map/ppermute | solution.py:43
  58.9 12.9 %collective-permute-start.16 = (bf16[32,896]{1,0:T(8,128)(2,1)S(1)}, bf16[32,896]{1,0:T(8,128)(2,1)S(1)}, u32[]{:S(2)}, u32[]{:S(2)}) collective-permute-start(bf16[32,896]{1,0:T(8,128)(2,1)S(1)} %get-tuple-element.46), channel_id=1, source_target_pairs={{0,24},{4,28},{8,16},{12,20},{16,8},{20,12},{24,0},{28,4},{1,25},{... | collective-permute-start | bytes 172040 | tf_op jit(solution)/shard_map/ppermute | solution.py:43
  62.1 9.8 %collective-permute-start.17 = (bf16[32,896]{1,0:T(8,128)(2,1)S(1)}, bf16[32,896]{1,0:T(8,128)(2,1)S(1)}, u32[]{:S(2)}, u32[]{:S(2)}) collective-permute-start(bf16[32,896]{1,0:T(8,128)(2,1)S(1)} %get-tuple-element.47), channel_id=1, source_target_pairs={{0,16},{4,20},{8,24},{12,28},{16,0},{20,4},{24,8},{28,12},{1,17},{... | collective-permute-start | bytes 172040 | tf_op jit(solution)/shard_map/ppermute | solution.py:43
  64.4 7.5 %collective-permute-start.18 = (bf16[32,896]{1,0:T(8,128)(2,1)S(1)}, bf16[32,896]{1,0:T(8,128)(2,1)S(1)}, u32[]{:S(2)}, u32[]{:S(2)}) collective-permute-start(bf16[32,896]{1,0:T(8,128)(2,1)S(1)} %get-tuple-element.48), channel_id=1, source_target_pairs={{0,8},{4,12},{8,0},{12,4},{16,24},{20,28},{24,16},{28,20},{1,9},{5... | collective-permute-start | bytes 172040 | tf_op jit(solution)/shard_map/ppermute | solution.py:43
  67.7 4.1 %collective-permute-start.22 = (bf16[32,768]{1,0:T(8,128)(2,1)S(1)}, bf16[32,768]{1,0:T(8,128)(2,1)S(1)}, u32[]{:S(2)}, u32[]{:S(2)}) collective-permute-start(bf16[32,768]{1,0:T(8,128)(2,1)S(1)} %get-tuple-element.55), channel_id=1, source_target_pairs={{0,8},{4,12},{8,0},{12,4},{16,24},{20,28},{24,16},{28,20},{1,9},{5... | collective-permute-start | bytes 147464 | tf_op jit(solution)/shard_map/ppermute | solution.py:43
  72.0 4.5 %collective-permute-start.23 = (bf16[32,768]{1,0:T(8,128)(2,1)S(1)}, bf16[32,768]{1,0:T(8,128)(2,1)S(1)}, u32[]{:S(2)}, u32[]{:S(2)}) collective-permute-start(bf16[32,768]{1,0:T(8,128)(2,1)S(1)} %shard_map.165.refs_0_), channel_id=1, source_target_pairs={{0,8},{4,12},{8,0},{12,4},{16,24},{20,28},{24,16},{28,20},{1,9},{5... | collective-permute-start | bytes 147464 | tf_op jit(solution)/shard_map/ppermute | solution.py:43
  72.1 5.1 %collective-permute-start.24 = (bf16[32,768]{1,0:T(8,128)(2,1)S(1)}, bf16[32,768]{1,0:T(8,128)(2,1)S(1)}, u32[]{:S(2)}, u32[]{:S(2)}) collective-permute-start(bf16[32,768]{1,0:T(8,128)(2,1)S(1)} %shard_map.165.refs_0_), channel_id=1, source_target_pairs={{0,16},{4,20},{8,24},{12,28},{16,0},{20,4},{24,8},{28,12},{1,17},{... | collective-permute-start | bytes 147464 | tf_op jit(solution)/shard_map/ppermute | solution.py:43
  73.7 5.9 %collective-permute-start.25 = (bf16[32,768]{1,0:T(8,128)(2,1)S(1)}, bf16[32,768]{1,0:T(8,128)(2,1)S(1)}, u32[]{:S(2)}, u32[]{:S(2)}) collective-permute-start(bf16[32,768]{1,0:T(8,128)(2,1)S(1)} %shard_map.165.refs_0_), channel_id=1, source_target_pairs={{0,24},{4,28},{8,16},{12,20},{16,8},{20,12},{24,0},{28,4},{1,25},{... | collective-permute-start | bytes 147464 | tf_op jit(solution)/shard_map/ppermute | solution.py:43
  79.9 1.4 %collective-permute-start.27 = (bf16[128,512]{1,0:T(8,128)(2,1)S(1)}, bf16[128,512]{1,0:T(8,128)(2,1)S(1)}, u32[]{:S(2)}, u32[]{:S(2)}) collective-permute-start(bf16[128,512]{1,0:T(8,128)(2,1)S(1)} %shard_map.166), channel_id=1, source_target_pairs={{0,1},{1,0},{2,3},{3,2},{4,5},{5,4},{6,7},{7,6},{8,9},{9,8},{10,11... | collective-permute-start | bytes 393224 | tf_op jit(solution)/shard_map/ppermute | solution.py:43
  81.3 8.2 %collective-permute-start.30 = (bf16[128,256]{1,0:T(8,128)(2,1)S(1)}, bf16[128,256]{1,0:T(8,128)(2,1)S(1)}, u32[]{:S(2)}, u32[]{:S(2)}) collective-permute-start(bf16[128,256]{1,0:T(8,128)(2,1)S(1)} %get-tuple-element.61), channel_id=1, source_target_pairs={{0,4},{1,5},{2,6},{3,7},{4,0},{5,1},{6,2},{7,3},{8,12},{9,13},{10,... | collective-permute-start | bytes 196616 | tf_op jit(solution)/shard_map/ppermute | solution.py:50
  81.9 7.7 %collective-permute-start.29 = (bf16[128,256]{1,0:T(8,128)(2,1)S(1)}, bf16[128,256]{1,0:T(8,128)(2,1)S(1)}, u32[]{:S(2)}, u32[]{:S(2)}) collective-permute-start(bf16[128,256]{1,0:T(8,128)(2,1)S(1)} %get-tuple-element.61), channel_id=1, source_target_pairs={{0,6},{1,7},{2,4},{3,5},{4,2},{5,3},{6,0},{7,1},{8,14},{9,15},{10,... | collective-permute-start | bytes 196616 | tf_op jit(solution)/shard_map/ppermute | solution.py:50
  84.3 2.2 %copy-start.1 = (f32[16,2,128,256]{3,2,1,0:T(8,128)S(1)}, f32[16,2,128,256]{3,2,1,0:T(8,128)}, u32[]{:S(2)}) copy-start(f32[16,2,128,256]{3,2,1,0:T(8,128)} %copy-done) | copy-start | bytes 12582916
  88.9 4.3 %collective-permute-start.28 = (bf16[128,256]{1,0:T(8,128)(2,1)S(1)}, bf16[128,256]{1,0:T(8,128)(2,1)S(1)}, u32[]{:S(2)}, u32[]{:S(2)}) collective-permute-start(bf16[128,256]{1,0:T(8,128)(2,1)S(1)} %get-tuple-element.60), channel_id=1, source_target_pairs={{0,2},{1,3},{2,0},{3,1},{4,6},{5,7},{6,4},{7,5},{8,10},{9,11},{10,... | collective-permute-start | bytes 196616 | tf_op jit(solution)/shard_map/ppermute | solution.py:50

commit v3 on v2

--- a/solution.py
+++ b/solution.py
@@ -12,8 +12,9 @@
 DK = 128
 DV = 256
 LANES = 128
+TILE = 8
 STEPS = 8
-SCATTER = (1, 4, 5, 3, 6, 2)
+SCATTER = (1, 3, 4, 5, 6, 2)
 NEAR = (6, 4, 2)
 FF_GATE = (6, 4, 2)
 FF_UP = (6, 4, 2)
@@ -262,13 +263,19 @@
     own_out[...] = own2
     other_out[...] = other2
     squares = jnp.sum(own * own, axis=1, keepdims=True) + jnp.sum(other * other, axis=1, keepdims=True)
-    squares = split_squares(squares)
     kept = pl.ds(pl.multiple_of(lax.rem(me, 2) * half, half), half)
     gate = (dot(own2, ffgate[:, kept]) + dot(other2, sent[:, :half])).astype(jnp.bfloat16)
+    size = 2 * rows
     for i, piece in enumerate(pieces):
-        part = slice(2 * i * rows, 2 * (i + 1) * rows)
-        piece[:, :half] = gate[part]
-        piece[:, half:] = squares[part]
+        part = slice(i * size, (i + 1) * size)
+        for j in range(half // LANES):
+            piece[j * size : (j + 1) * size] = gate[part, j * LANES : (j + 1) * LANES]
+        flat = jnp.broadcast_to(squares[part], (size, LANES)).T[:TILE]
+        head = flat.astype(jnp.bfloat16)
+        rest = (flat - wide(head)).astype(jnp.bfloat16)
+        line = lax.broadcasted_iota(jnp.int32, flat.shape, 0)
+        piece[-TILE:] = jnp.zeros((TILE, LANES), jnp.bfloat16)
+        piece[-TILE:, :size] = jnp.where(line < TILE // 2, head, rest)
 
 
 def upper_kernel(own2, other2, ffup, early, late, *pieces):
@@ -286,10 +293,14 @@
 def hidden_kernel(count, *refs):
     gates, uppers, out = refs[:count], refs[count : 2 * count], refs[2 * count]
     half = out.shape[1]
-    gate = sum(wide(piece[...]) for piece in gates)
+    size = out.shape[0]
+    terms = sum(wide(piece[...]) for piece in gates)
     upper = sum(wide(piece[...]) for piece in uppers)
-    inv = lax.rsqrt(joined_squares(gate[:, half:]) / D + eps)
-    hidden = jax.nn.silu(gate[:, :half] * inv) * (upper * inv)
+    squares = terms[-TILE:, :size]
+    squares = squares[:1] + squares[TILE // 2 : TILE // 2 + 1]
+    inv = lax.rsqrt(jnp.broadcast_to(squares, (LANES, size)).T[:, :1] / D + eps)
+    gate = [terms[j * size : (j + 1) * size] for j in range(half // LANES)]
+    hidden = jax.nn.silu(jnp.concatenate(gate, axis=1) * inv) * (upper * inv)
     out[...] = hidden.astype(jnp.bfloat16)
 
 
@@ -341,7 +352,7 @@
     came = {}
     came[1] = send_xor(pieces[1], kv, (1,))
     relayed = call(relay_kernel, shape((rows, total_width)), pieces[n_kv - 2], came[1])
-    for m in order[1:]:
+    for m in [m for m in order if m != 1]:
         came[m] = send_xor(relayed if m == n_kv - 2 else pieces[m], kv, (m,))
     out_pair = send_xor(w_out, kv, (1,))
     early_pair = send_xor(early_sent, kv, (1,))
@@ -403,7 +414,7 @@
 
     middle, own2, other2, *gates = call(
         functools.partial(middle_kernel, len(even), len(odd)),
-        [shape((batch, model))] * 3 + [shape((2 * rows, half + LANES))] * (n_kv // 2),
+        [shape((batch, model))] * 3 + [shape((half // LANES * 2 * rows + TILE, LANES))] * (n_kv // 2),
         *even,
         *odd,
         tokens,

time: 94.2 us -> 95.4 us (1.013)
  starting transfers between devices: 41 us -> 42.4 us
    ppermute x25, starting transfers between devices: 33 us -> 34.4 us  [send_xor(): return lax.ppermute(array, axis, pairs)]
  transfers between devices with their start and end apart: 31 -> 31, of which waited for: 15 -> 14; matrix products, arithmetic and copies ran while one was open for 0% -> 0% of each run, Pallas kernels for 9% -> 9%
where the time goes in v3:
time: 95.4 us; the launch traced here: 95.2 us
  starting transfers between devices  42.4 us (44%)
  waiting for transfers between devices  39.6 us (42%)
  Pallas kernels  9.14 us (10%)
  local copies, waits for them, and re-layouts  2.27 us (2%)
    ppermute x25, starting transfers between devices, send_xor(): return lax.ppermute(array, axis, pairs)  34.4 us
    ppermute x25, waiting for transfers between devices, send_xor(): return lax.ppermute(array, axis, pairs)  22.3 us
    ppermute x6, waiting for transfers between devices, send_xor(): return lax.ppermute(array, (first, second), pairs)  17.3 us
    pallas_call x10, Pallas kernels, call(): pl.pallas_call(kernel, out_shape=outs, in_specs=specs or [VMEM] * len(arg...  9.14 us
    ppermute x6, starting transfers between devices, send_xor(): return lax.ppermute(array, (first, second), pairs)  8.01 us
    unnamed x16, local copies, waits for them, and re-layouts  2.22 us
  transfers between devices with their start and end apart: 31, of which 14 were waited for; matrix products, arithmetic and copies ran while one was open for 0% of the time, Pallas kernels for 9%

profile of v3, /device:TPU:0, one launch (start us, length us, event | category | flops | bytes accessed | tf_op | source)
XLA Modules:
  0.0 95.2 jit_solution(5382536180892666234)
XLA Ops:
  0.6 3.0 %collective-permute-start.9 = (bf16[512,256]{1,0:T(8,128)(2,1)}, bf16[512,256]{1,0:T(8,128)(2,1)S(1)}, u32[]{:S(2)}, u32[]{:S(2)}) collective-permute-start(bf16[512,256]{1,0:T(8,128)(2,1)} %refs_4_.4), channel_id=1, source_target_pairs={{0,4},{4,0},{8,12},{12,8},{16,20},{20,16},{24,28},{28,24},{1,5},{5... | collective-permute-start | bytes 786440 | tf_op jit(solution)/shard_map/ppermute | solution.py:44
  3.7 2.0 %shard_map.158 = (bf16[16,1920]{1,0:T(8,128)(2,1)S(1)}, bf16[32,1920]{1,0:T(8,128)(2,1)S(1)}, bf16[16,1920]{1,0:T(8,128)(2,1)S(1)}, bf16[16,1920]{1,0:T(8,128)(2...) custom-call(bf16[128,256]{1,0:T(8,128)(2,1)} %refs_5_.3, ...), custom_call_target="tpu_custom_call" | custom-call | tf_op jit(solution)/shard_map/pallas_call | solution.py:78
  5.7 0.1 collective-permute-start
  5.8 3.0 %collective-permute-start.1 = (bf16[16,1920]{1,0:T(8,128)(2,1)S(1)}, bf16[16,1920]{1,0:T(8,128)(2,1)S(1)}, u32[]{:S(2)}, u32[]{:S(2)}) collective-permute-start(bf16[16,1920]{1,0:T(8,128)(2,1)S(1)} %get-tuple-element.33), channel_id=1, source_target_pairs={{0,12},{4,8},{8,4},{12,0},{16,28},{20,24},{24,20},{28,16},{1,13},{... | collective-permute-start | bytes 184328 | tf_op jit(solution)/shard_map/ppermute | solution.py:44
  8.8 2.6 %collective-permute-start.2 = (bf16[16,1920]{1,0:T(8,128)(2,1)S(1)}, bf16[16,1920]{1,0:T(8,128)(2,1)S(1)}, u32[]{:S(2)}, u32[]{:S(2)}) collective-permute-start(bf16[16,1920]{1,0:T(8,128)(2,1)S(1)} %get-tuple-element.34), channel_id=1, source_target_pairs={{0,16},{4,20},{8,24},{12,28},{16,0},{20,4},{24,8},{28,12},{1,17},{... | collective-permute-start | bytes 184328 | tf_op jit(solution)/shard_map/ppermute | solution.py:44
  11.4 0.5 collective-permute-start.15
  11.9 3.1 %collective-permute-done.came.refs_1_ = bf16[32,1920]{1,0:T(8,128)(2,1)S(1)} collective-permute-done((bf16[32,1920]{1,0:T(8,128)(2,1)S(1)}, bf16[32,1920]{1,0:T(8,128)(2,1)S(1)}, u32[]{:S(2)}, u32[]{:S(2)}) %collective-permute-start) | collective-permute-done | bytes 122912 | tf_op jit(solution)/shard_map/ppermute | solution.py:44
  15.0 4.0 %collective-permute-start.3 = (bf16[16,1920]{1,0:T(8,128)(2,1)S(1)}, bf16[16,1920]{1,0:T(8,128)(2,1)S(1)}, u32[]{:S(2)}, u32[]{:S(2)}) collective-permute-start(bf16[16,1920]{1,0:T(8,128)(2,1)S(1)} %get-tuple-element.35), channel_id=1, source_target_pairs={{0,20},{4,16},{8,28},{12,24},{16,4},{20,0},{24,12},{28,8},{1,21},{... | collective-permute-start | bytes 184328 | tf_op jit(solution)/shard_map/ppermute | solution.py:44
  19.0 0.2 shard_map.159
  19.2 0.0 collective-permute-done.1.refs_2_
  19.2 0.0 copy-start.6
  19.2 0.0 copy-start.7
  19.2 1.6 %collective-permute-start.5 = (bf16[16,1920]{1,0:T(8,128)(2,1)S(1)}, bf16[16,1920]{1,0:T(8,128)(2,1)S(1)}, u32[]{:S(2)}, u32[]{:S(2)}) collective-permute-start(bf16[16,1920]{1,0:T(8,128)(2,1)S(1)} %get-tuple-element.37), channel_id=1, source_target_pairs={{0,8},{4,12},{8,0},{12,4},{16,24},{20,28},{24,16},{28,20},{1,9},{5... | collective-permute-start | bytes 184328 | tf_op jit(solution)/shard_map/ppermute | solution.py:44
  20.9 0.0 collective-permute-done.2.refs_3_
  20.9 0.2 collective-permute-start.4
  21.1 2.2 %shard_map.160 = (f32[16,2,128,256]{3,2,1,0:T(8,128)S(1)}, f32[16,256]{1,0:T(8,128)S(1)}, f32[256]{0:T(256)S(1)}) custom-call(f32[16,2,128,256]{3,2,1,0:T(8,128)} %refs_0_.3, f32[16,256]{1,0:T(8,128)} %refs_1_.3, f32[256]{0:T(256)} %refs_2_.3), custom_call_target="tpu_custom_call" | custom-call | tf_op jit(solution)/shard_map/pallas_call | solution.py:78
  23.3 0.0 copy-start
  23.3 0.0 copy-start.4
  23.3 0.7 collective-permute-done.5.refs_6_
  24.0 2.9 %collective-permute-done.4.refs_5_ = bf16[16,1920]{1,0:T(8,128)(2,1)S(1)} collective-permute-done((bf16[16,1920]{1,0:T(8,128)(2,1)S(1)}, bf16[16,1920]{1,0:T(8,128)(2,1)S(1)}, u32[]{:S(2)}, u32[]{:S(2)}) %collective-permute-start.4) | collective-permute-done | bytes 61472 | tf_op jit(solution)/shard_map/ppermute | solution.py:44
  26.9 1.1 %shard_map.161 = (bf16[16,512]{1,0:T(8,128)(2,1)S(1)}, f32[16,256]{1,0:T(8,128)S(1)}, f32[16,256]{1,0:T(8,128)S(1)}, f32[16,512]{1,0:T(8,128)S(1)}) custom-call(bf16[16,1920]{1,0:T(8,128)(2,1)S(1)} %get-tuple-element.31.refs_0_, bf16[32,1920]{1,0:T(8,128)(2,1)S(1)} %collective-permute-done.came.refs_1_, bf16[16,1920]{1,0:T(8,128)(2,1)S(1)} %collective-permute-done.1.refs_2_, ...), custom_call_target="tpu_custom_call" | custom-call | tf_op jit(solution)/shard_map/pallas_call | solution.py:78
  27.9 0.1 collective-permute-start.6
  28.0 1.2 %collective-permute-start.7 = (bf16[16,512]{1,0:T(8,128)(2,1)S(1)}, bf16[16,512]{1,0:T(8,128)(2,1)S(1)}, u32[]{:S(2)}, u32[]{:S(2)}) collective-permute-start(bf16[16,512]{1,0:T(8,128)(2,1)S(1)} %get-tuple-element.41.refs_0_), channel_id=1, source_target_pairs={{0,16},{4,20},{8,24},{12,28},{16,0},{20,4},{24,8},{28,12},{1,17},{... | collective-permute-start | bytes 49160 | tf_op jit(solution)/shard_map/ppermute | solution.py:44
  29.2 3.2 %collective-permute-start.8 = (bf16[16,512]{1,0:T(8,128)(2,1)S(1)}, bf16[16,512]{1,0:T(8,128)(2,1)S(1)}, u32[]{:S(2)}, u32[]{:S(2)}) collective-permute-start(bf16[16,512]{1,0:T(8,128)(2,1)S(1)} %get-tuple-element.41.refs_0_), channel_id=1, source_target_pairs={{0,24},{4,28},{8,16},{12,20},{16,8},{20,12},{24,0},{28,4},{1,25},{... | collective-permute-start | bytes 49160 | tf_op jit(solution)/shard_map/ppermute | solution.py:44
  32.4 0.0 collective-permute-done.6.refs_1_
  32.4 0.3 collective-permute-done.7.refs_2_
  32.7 2.0 %collective-permute-done.8.refs_3_ = bf16[16,512]{1,0:T(8,128)(2,1)S(1)} collective-permute-done((bf16[16,512]{1,0:T(8,128)(2,1)S(1)}, bf16[16,512]{1,0:T(8,128)(2,1)S(1)}, u32[]{:S(2)}, u32[]{:S(2)}) %collective-permute-start.8) | collective-permute-done | bytes 16416 | tf_op jit(solution)/shard_map/ppermute | solution.py:44
  34.8 0.0 collective-permute-done.9.refs_5_
  34.8 0.2 shard_map.162.refs_0_
  35.0 0.1 collective-permute-start.10
  35.1 0.6 collective-permute-start.14
  35.7 1.5 %collective-permute-start.19 = (bf16[256,512]{1,0:T(8,128)(2,1)S(1)}, bf16[256,512]{1,0:T(8,128)(2,1)S(1)}, u32[]{:S(2)}, u32[]{:S(2)}) collective-permute-start(bf16[256,512]{1,0:T(8,128)(2,1)S(1)} %get-tuple-element.51), channel_id=1, source_target_pairs={{0,4},{4,0},{8,12},{12,8},{16,20},{20,16},{24,28},{28,24},{1,5},{5... | collective-permute-start | bytes 786440 | tf_op jit(solution)/shard_map/ppermute | solution.py:44
  37.2 0.5 collective-permute-start.26
  37.7 0.0 collective-permute-done.10.refs_1_
  37.7 1.6 %collective-permute-start.11 = (bf16[64,512]{1,0:T(8,128)(2,1)S(1)}, bf16[64,512]{1,0:T(8,128)(2,1)S(1)}, u32[]{:S(2)}, u32[]{:S(2)}) collective-permute-start(bf16[64,512]{1,0:T(8,128)(2,1)S(1)} %add_convert_fusion), channel_id=1, source_target_pairs={{0,2},{1,3},{2,0},{3,1},{4,6},{5,7},{6,4},{7,5},{8,10},{9,11},{10,... | collective-permute-start | bytes 196616 | tf_op jit(solution)/shard_map/ppermute | solution.py:51
  39.3 1.0 %collective-permute-done.14.refs_6_ = bf16[144,256]{1,0:T(8,128)(2,1)S(1)} collective-permute-done((bf16[144,256]{1,0:T(8,128)(2,1)S(1)}, bf16[144,256]{1,0:T(8,128)(2,1)S(1)}, u32[]{:S(2)}, u32[]{:S(2)}) %collective-permute-start.14) | collective-permute-done | bytes 73760 | tf_op jit(solution)/shard_map/ppermute | solution.py:44
  40.3 1.3 %collective-permute-start.12 = (bf16[64,512]{1,0:T(8,128)(2,1)S(1)}, bf16[64,512]{1,0:T(8,128)(2,1)S(1)}, u32[]{:S(2)}, u32[]{:S(2)}) collective-permute-start(bf16[64,512]{1,0:T(8,128)(2,1)S(1)} %add_convert_fusion), channel_id=1, source_target_pairs={{0,6},{1,7},{2,4},{3,5},{4,2},{5,3},{6,0},{7,1},{8,14},{9,15},{10,... | collective-permute-start | bytes 196616 | tf_op jit(solution)/shard_map/ppermute | solution.py:51
  41.6 0.5 collective-permute-done.11.refs_2_
  42.0 1.5 %collective-permute-start.13 = (bf16[64,512]{1,0:T(8,128)(2,1)S(1)}, bf16[64,512]{1,0:T(8,128)(2,1)S(1)}, u32[]{:S(2)}, u32[]{:S(2)}) collective-permute-start(bf16[64,512]{1,0:T(8,128)(2,1)S(1)} %add_convert_fusion), channel_id=1, source_target_pairs={{0,4},{1,5},{2,6},{3,7},{4,0},{5,1},{6,2},{7,3},{8,12},{9,13},{10,... | collective-permute-start | bytes 196616 | tf_op jit(solution)/shard_map/ppermute | solution.py:51
  43.5 13.1 %collective-permute-done.12.refs_3_ = bf16[64,512]{1,0:T(8,128)(2,1)S(1)} collective-permute-done((bf16[64,512]{1,0:T(8,128)(2,1)S(1)}, bf16[64,512]{1,0:T(8,128)(2,1)S(1)}, u32[]{:S(2)}, u32[]{:S(2)}) %collective-permute-start.12) | collective-permute-done | bytes 65568 | tf_op jit(solution)/shard_map/ppermute | solution.py:51
  56.7 0.4 shard_map.163
  57.1 0.3 shard_map.164
  57.4 3.2 %collective-permute-start.20 = (bf16[32,768]{1,0:T(8,128)(2,1)S(1)}, bf16[32,768]{1,0:T(8,128)(2,1)S(1)}, u32[]{:S(2)}, u32[]{:S(2)}) collective-permute-start(bf16[32,768]{1,0:T(8,128)(2,1)S(1)} %get-tuple-element.53), channel_id=1, source_target_pairs={{0,24},{4,28},{8,16},{12,20},{16,8},{20,12},{24,0},{28,4},{1,25},{... | collective-permute-start | bytes 147464 | tf_op jit(solution)/shard_map/ppermute | solution.py:44
  60.6 0.7 collective-permute-start.16
  61.3 2.3 %collective-permute-start.17 = (bf16[200,128]{1,0:T(8,128)(2,1)S(1)}, bf16[200,128]{1,0:T(8,128)(2,1)S(1)}, u32[]{:S(2)}, u32[]{:S(2)}) collective-permute-start(bf16[200,128]{1,0:T(8,128)(2,1)S(1)} %get-tuple-element.47), channel_id=1, source_target_pairs={{0,16},{4,20},{8,24},{12,28},{16,0},{20,4},{24,8},{28,12},{1,17},{... | collective-permute-start | bytes 153608 | tf_op jit(solution)/shard_map/ppermute | solution.py:44
  63.6 1.5 %collective-permute-start.18 = (bf16[200,128]{1,0:T(8,128)(2,1)S(1)}, bf16[200,128]{1,0:T(8,128)(2,1)S(1)}, u32[]{:S(2)}, u32[]{:S(2)}) collective-permute-start(bf16[200,128]{1,0:T(8,128)(2,1)S(1)} %get-tuple-element.48), channel_id=1, source_target_pairs={{0,8},{4,12},{8,0},{12,4},{16,24},{20,28},{24,16},{28,20},{1,9},{5... | collective-permute-start | bytes 153608 | tf_op jit(solution)/shard_map/ppermute | solution.py:44
  65.0 2.2 %collective-permute-done.21.refs_6_ = bf16[32,768]{1,0:T(8,128)(2,1)S(1)} collective-permute-done((bf16[32,768]{1,0:T(8,128)(2,1)S(1)}, bf16[32,768]{1,0:T(8,128)(2,1)S(1)}, u32[]{:S(2)}, u32[]{:S(2)}) %collective-permute-start.21) | collective-permute-done | bytes 49184 | tf_op jit(solution)/shard_map/ppermute | solution.py:44
  67.2 4.1 %collective-permute-done.22.refs_7_ = bf16[32,768]{1,0:T(8,128)(2,1)S(1)} collective-permute-done((bf16[32,768]{1,0:T(8,128)(2,1)S(1)}, bf16[32,768]{1,0:T(8,128)(2,1)S(1)}, u32[]{:S(2)}, u32[]{:S(2)}) %collective-permute-start.22) | collective-permute-done | bytes 49184 | tf_op jit(solution)/shard_map/ppermute | solution.py:44
  71.3 0.2 shard_map.165.refs_0_
  71.5 0.1 collective-permute-start.23
  71.6 3.1 %collective-permute-start.24 = (bf16[32,768]{1,0:T(8,128)(2,1)S(1)}, bf16[32,768]{1,0:T(8,128)(2,1)S(1)}, u32[]{:S(2)}, u32[]{:S(2)}) collective-permute-start(bf16[32,768]{1,0:T(8,128)(2,1)S(1)} %shard_map.165.refs_0_), channel_id=1, source_target_pairs={{0,16},{4,20},{8,24},{12,28},{16,0},{20,4},{24,8},{28,12},{1,17},{... | collective-permute-start | bytes 147464 | tf_op jit(solution)/shard_map/ppermute | solution.py:44
  74.8 1.2 %collective-permute-start.25 = (bf16[32,768]{1,0:T(8,128)(2,1)S(1)}, bf16[32,768]{1,0:T(8,128)(2,1)S(1)}, u32[]{:S(2)}, u32[]{:S(2)}) collective-permute-start(bf16[32,768]{1,0:T(8,128)(2,1)S(1)} %shard_map.165.refs_0_), channel_id=1, source_target_pairs={{0,24},{4,28},{8,16},{12,20},{16,8},{20,12},{24,0},{28,4},{1,25},{... | collective-permute-start | bytes 147464 | tf_op jit(solution)/shard_map/ppermute | solution.py:44
  76.0 1.1 %collective-permute-done.24.refs_2_ = bf16[32,768]{1,0:T(8,128)(2,1)S(1)} collective-permute-done((bf16[32,768]{1,0:T(8,128)(2,1)S(1)}, bf16[32,768]{1,0:T(8,128)(2,1)S(1)}, u32[]{:S(2)}, u32[]{:S(2)}) %collective-permute-start.24) | collective-permute-done | bytes 49184 | tf_op jit(solution)/shard_map/ppermute | solution.py:44
  77.1 3.6 %collective-permute-done.25.refs_3_ = bf16[32,768]{1,0:T(8,128)(2,1)S(1)} collective-permute-done((bf16[32,768]{1,0:T(8,128)(2,1)S(1)}, bf16[32,768]{1,0:T(8,128)(2,1)S(1)}, u32[]{:S(2)}, u32[]{:S(2)}) %collective-permute-start.25) | collective-permute-done | bytes 49184 | tf_op jit(solution)/shard_map/ppermute | solution.py:44
  80.6 0.3 shard_map.166
  80.9 0.1 collective-permute-start.27
  81.0 1.3 %collective-permute-done.27 = bf16[128,512]{1,0:T(8,128)(2,1)S(1)} collective-permute-done((bf16[128,512]{1,0:T(8,128)(2,1)S(1)}, bf16[128,512]{1,0:T(8,128)(2,1)S(1)}, u32[]{:S(2)}, u32[]{:S(2)}) %collective-permute-start.27) | collective-permute-done | bytes 131104 | tf_op jit(solution)/shard_map/ppermute | solution.py:44
  82.4 0.6 collective-permute-start.30
  83.0 2.4 %collective-permute-start.29 = (bf16[128,256]{1,0:T(8,128)(2,1)S(1)}, bf16[128,256]{1,0:T(8,128)(2,1)S(1)}, u32[]{:S(2)}, u32[]{:S(2)}) collective-permute-start(bf16[128,256]{1,0:T(8,128)(2,1)S(1)} %get-tuple-element.61), channel_id=1, source_target_pairs={{0,6},{1,7},{2,4},{3,5},{4,2},{5,3},{6,0},{7,1},{8,14},{9,15},{10,... | collective-permute-start | bytes 196616 | tf_op jit(solution)/shard_map/ppermute | solution.py:51
  85.4 2.2 %copy-done.1 = f32[16,2,128,256]{3,2,1,0:T(8,128)S(1)} copy-done((f32[16,2,128,256]{3,2,1,0:T(8,128)S(1)}, f32[16,2,128,256]{3,2,1,0:T(8,128)}, u32[]{:S(2)}) %copy-start.1) | copy-done | bytes 4194328
  87.6 2.4 %shard_map.167 = f32[16,2,128,256]{3,2,1,0:T(8,128)} custom-call(f32[16,2,128,256]{3,2,1,0:T(8,128)S(1)} %copy-done.1, f32[16,256]{1,0:T(8,128)S(1)} %get-tuple-element.57.keep, f32[16,256]{1,0:T(8,128)S(1)} %get-tuple-element.58.keys, f32[16,512]{1,0:T(8,128)S(1)} %get-tuple-element.59.values), custom_call_target="tpu_custom_call" | custom-call | tf_op jit(solution)/shard_map/pallas_call | solution.py:78
  90.0 0.6 collective-permute-start.28
  90.7 3.7 %collective-permute-done.28 = bf16[128,256]{1,0:T(8,128)(2,1)S(1)} collective-permute-done((bf16[128,256]{1,0:T(8,128)(2,1)S(1)}, bf16[128,256]{1,0:T(8,128)(2,1)S(1)}, u32[]{:S(2)}, u32[]{:S(2)}) %collective-permute-start.28) | collective-permute-done | bytes 65568 | tf_op jit(solution)/shard_map/ppermute | solution.py:51
  94.5 0.7 fusion.2
  (40 shorter events, 0.3 us)
Async XLA Ops:
  0.6 34.1 %collective-permute-start.9 = (bf16[512,256]{1,0:T(8,128)(2,1)}, bf16[512,256]{1,0:T(8,128)(2,1)S(1)}, u32[]{:S(2)}, u32[]{:S(2)}) collective-permute-start(bf16[512,256]{1,0:T(8,128)(2,1)} %refs_4_.4), channel_id=1, source_target_pairs={{0,4},{4,0},{8,12},{12,8},{16,20},{20,16},{24,28},{28,24},{1,5},{5... | collective-permute-start | bytes 786440 | tf_op jit(solution)/shard_map/ppermute | solution.py:44
  5.7 9.3 %collective-permute-start = (bf16[32,1920]{1,0:T(8,128)(2,1)S(1)}, bf16[32,1920]{1,0:T(8,128)(2,1)S(1)}, u32[]{:S(2)}, u32[]{:S(2)}) collective-permute-start(bf16[32,1920]{1,0:T(8,128)(2,1)S(1)} %get-tuple-element.32), channel_id=1, source_target_pairs={{0,4},{4,0},{8,12},{12,8},{16,20},{20,16},{24,28},{28,24},{1,5},{5... | collective-permute-start | bytes 368648 | tf_op jit(solution)/shard_map/ppermute | solution.py:44
  5.8 13.4 %collective-permute-start.1 = (bf16[16,1920]{1,0:T(8,128)(2,1)S(1)}, bf16[16,1920]{1,0:T(8,128)(2,1)S(1)}, u32[]{:S(2)}, u32[]{:S(2)}) collective-permute-start(bf16[16,1920]{1,0:T(8,128)(2,1)S(1)} %get-tuple-element.33), channel_id=1, source_target_pairs={{0,12},{4,8},{8,4},{12,0},{16,28},{20,24},{24,20},{28,16},{1,13},{... | collective-permute-start | bytes 184328 | tf_op jit(solution)/shard_map/ppermute | solution.py:44
  8.8 12.1 %collective-permute-start.2 = (bf16[16,1920]{1,0:T(8,128)(2,1)S(1)}, bf16[16,1920]{1,0:T(8,128)(2,1)S(1)}, u32[]{:S(2)}, u32[]{:S(2)}) collective-permute-start(bf16[16,1920]{1,0:T(8,128)(2,1)S(1)} %get-tuple-element.34), channel_id=1, source_target_pairs={{0,16},{4,20},{8,24},{12,28},{16,0},{20,4},{24,8},{28,12},{1,17},{... | collective-permute-start | bytes 184328 | tf_op jit(solution)/shard_map/ppermute | solution.py:44
  11.4 45.3 %collective-permute-start.15 = (bf16[256,1024]{1,0:T(8,128)(2,1)S(1)}, bf16[256,1024]{1,0:T(8,128)(2,1)S(1)}, u32[]{:S(2)}, u32[]{:S(2)}) collective-permute-start(bf16[256,1024]{1,0:T(8,128)(2,1)S(1)} %get-tuple-element.43), channel_id=1, source_target_pairs={{0,4},{4,0},{8,12},{12,8},{16,20},{20,16},{24,28},{28,24},{1,5},{5... | collective-permute-start | bytes 1572872 | tf_op jit(solution)/shard_map/ppermute | solution.py:44
  15.0 8.4 %collective-permute-start.3 = (bf16[16,1920]{1,0:T(8,128)(2,1)S(1)}, bf16[16,1920]{1,0:T(8,128)(2,1)S(1)}, u32[]{:S(2)}, u32[]{:S(2)}) collective-permute-start(bf16[16,1920]{1,0:T(8,128)(2,1)S(1)} %get-tuple-element.35), channel_id=1, source_target_pairs={{0,20},{4,16},{8,28},{12,24},{16,4},{20,0},{24,12},{28,8},{1,21},{... | collective-permute-start | bytes 184328 | tf_op jit(solution)/shard_map/ppermute | solution.py:44
  19.2 15.6 %copy-start.5 = (bf16[512,256]{1,0:T(8,128)(2,1)S(1)}, bf16[512,256]{1,0:T(8,128)(2,1)}, u32[]{:S(2)}) copy-start(bf16[512,256]{1,0:T(8,128)(2,1)} %refs_4_.4) | copy-start | bytes 786436
  19.2 37.5 %copy-start.3 = (bf16[256,1536]{1,0:T(8,128)(2,1)S(1)}, bf16[256,1536]{1,0:T(8,128)(2,1)}, u32[]{:S(2)}) copy-start(bf16[256,1536]{1,0:T(8,128)(2,1)} %refs_8_.3) | copy-start | bytes 2359300
  19.2 37.5 %copy-start.6 = (bf16[128,256]{1,0:T(8,128)(2,1)S(1)}, bf16[128,256]{1,0:T(8,128)(2,1)}, u32[]{:S(2)}) copy-start(bf16[128,256]{1,0:T(8,128)(2,1)} %refs_5_.3) | copy-start | bytes 196612
  19.2 37.5 %copy-start.7 = (bf16[256]{0:T(256)(128)(2,1)S(1)}, bf16[256]{0:T(256)(128)(2,1)}, u32[]{:S(2)}) copy-start(bf16[256]{0:T(256)(128)(2,1)} %refs_7_.3) | copy-start | bytes 1540
  19.2 4.8 %collective-permute-start.5 = (bf16[16,1920]{1,0:T(8,128)(2,1)S(1)}, bf16[16,1920]{1,0:T(8,128)(2,1)S(1)}, u32[]{:S(2)}, u32[]{:S(2)}) collective-permute-start(bf16[16,1920]{1,0:T(8,128)(2,1)S(1)} %get-tuple-element.37), channel_id=1, source_target_pairs={{0,8},{4,12},{8,0},{12,4},{16,24},{20,28},{24,16},{28,20},{1,9},{5... | collective-permute-start | bytes 184328 | tf_op jit(solution)/shard_map/ppermute | solution.py:44
  20.9 6.0 %collective-permute-start.4 = (bf16[16,1920]{1,0:T(8,128)(2,1)S(1)}, bf16[16,1920]{1,0:T(8,128)(2,1)S(1)}, u32[]{:S(2)}, u32[]{:S(2)}) collective-permute-start(bf16[16,1920]{1,0:T(8,128)(2,1)S(1)} %shard_map.159), channel_id=1, source_target_pairs={{0,24},{4,28},{8,16},{12,20},{16,8},{20,12},{24,0},{28,4},{1,25},{... | collective-permute-start | bytes 184328 | tf_op jit(solution)/shard_map/ppermute | solution.py:44
  23.3 34.1 %copy-start = (f32[16,2,128,256]{3,2,1,0:T(8,128)}, f32[16,2,128,256]{3,2,1,0:T(8,128)S(1)}, u32[]{:S(2)}) copy-start(f32[16,2,128,256]{3,2,1,0:T(8,128)S(1)} %get-tuple-element.39.refs_8_.state) | copy-start | bytes 12582916
  23.3 33.8 %copy-start.4 = (bf16[256,1536]{1,0:T(8,128)(2,1)S(1)}, bf16[256,1536]{1,0:T(8,128)(2,1)}, u32[]{:S(2)}) copy-start(bf16[256,1536]{1,0:T(8,128)(2,1)} %ffup.1) | copy-start | bytes 2359300
  26.9 53.8 %copy-start.2 = (bf16[1536,256]{1,0:T(8,128)(2,1)S(1)}, bf16[1536,256]{1,0:T(8,128)(2,1)}, u32[]{:S(2)}) copy-start(bf16[1536,256]{1,0:T(8,128)(2,1)} %refs_4_.5) | copy-start | bytes 2359300
  27.9 4.4 %collective-permute-start.6 = (bf16[16,512]{1,0:T(8,128)(2,1)S(1)}, bf16[16,512]{1,0:T(8,128)(2,1)S(1)}, u32[]{:S(2)}, u32[]{:S(2)}) collective-permute-start(bf16[16,512]{1,0:T(8,128)(2,1)S(1)} %get-tuple-element.41.refs_0_), channel_id=1, source_target_pairs={{0,8},{4,12},{8,0},{12,4},{16,24},{20,28},{24,16},{28,20},{1,9},{5... | collective-permute-start | bytes 49160 | tf_op jit(solution)/shard_map/ppermute | solution.py:44
  28.0 4.7 %collective-permute-start.7 = (bf16[16,512]{1,0:T(8,128)(2,1)S(1)}, bf16[16,512]{1,0:T(8,128)(2,1)S(1)}, u32[]{:S(2)}, u32[]{:S(2)}) collective-permute-start(bf16[16,512]{1,0:T(8,128)(2,1)S(1)} %get-tuple-element.41.refs_0_), channel_id=1, source_target_pairs={{0,16},{4,20},{8,24},{12,28},{16,0},{20,4},{24,8},{28,12},{1,17},{... | collective-permute-start | bytes 49160 | tf_op jit(solution)/shard_map/ppermute | solution.py:44
  29.2 5.5 %collective-permute-start.8 = (bf16[16,512]{1,0:T(8,128)(2,1)S(1)}, bf16[16,512]{1,0:T(8,128)(2,1)S(1)}, u32[]{:S(2)}, u32[]{:S(2)}) collective-permute-start(bf16[16,512]{1,0:T(8,128)(2,1)S(1)} %get-tuple-element.41.refs_0_), channel_id=1, source_target_pairs={{0,24},{4,28},{8,16},{12,20},{16,8},{20,12},{24,0},{28,4},{1,25},{... | collective-permute-start | bytes 49160 | tf_op jit(solution)/shard_map/ppermute | solution.py:44
  35.0 2.7 %collective-permute-start.10 = (bf16[64,512]{1,0:T(8,128)(2,1)S(1)}, bf16[64,512]{1,0:T(8,128)(2,1)S(1)}, u32[]{:S(2)}, u32[]{:S(2)}) collective-permute-start(bf16[64,512]{1,0:T(8,128)(2,1)S(1)} %shard_map.162.refs_0_), channel_id=1, source_target_pairs={{0,1},{1,0},{2,3},{3,2},{4,5},{5,4},{6,7},{7,6},{8,9},{9,8},{10,11... | collective-permute-start | bytes 196616 | tf_op jit(solution)/shard_map/ppermute | solution.py:44
  35.1 5.2 %collective-permute-start.14 = (bf16[144,256]{1,0:T(8,128)(2,1)S(1)}, bf16[144,256]{1,0:T(8,128)(2,1)S(1)}, u32[]{:S(2)}, u32[]{:S(2)}) collective-permute-start(bf16[144,256]{1,0:T(8,128)(2,1)S(1)} %get-tuple-element.42), channel_id=1, source_target_pairs={{0,4},{4,0},{8,12},{12,8},{16,20},{20,16},{24,28},{28,24},{1,5},{5... | collective-permute-start | bytes 221192 | tf_op jit(solution)/shard_map/ppermute | solution.py:44
  35.7 21.4 %collective-permute-start.19 = (bf16[256,512]{1,0:T(8,128)(2,1)S(1)}, bf16[256,512]{1,0:T(8,128)(2,1)S(1)}, u32[]{:S(2)}, u32[]{:S(2)}) collective-permute-start(bf16[256,512]{1,0:T(8,128)(2,1)S(1)} %get-tuple-element.51), channel_id=1, source_target_pairs={{0,4},{4,0},{8,12},{12,8},{16,20},{20,16},{24,28},{28,24},{1,5},{5... | collective-permute-start | bytes 786440 | tf_op jit(solution)/shard_map/ppermute | solution.py:44
  37.2 38.8 %collective-permute-start.26 = (bf16[768,256]{1,0:T(8,128)(2,1)S(1)}, bf16[768,256]{1,0:T(8,128)(2,1)S(1)}, u32[]{:S(2)}, u32[]{:S(2)}) collective-permute-start(bf16[768,256]{1,0:T(8,128)(2,1)S(1)} %get-tuple-element.56), channel_id=1, source_target_pairs={{0,4},{4,0},{8,12},{12,8},{16,20},{20,16},{24,28},{28,24},{1,5},{5... | collective-permute-start | bytes 1179656 | tf_op jit(solution)/shard_map/ppermute | solution.py:44
  37.7 4.3 %collective-permute-start.11 = (bf16[64,512]{1,0:T(8,128)(2,1)S(1)}, bf16[64,512]{1,0:T(8,128)(2,1)S(1)}, u32[]{:S(2)}, u32[]{:S(2)}) collective-permute-start(bf16[64,512]{1,0:T(8,128)(2,1)S(1)} %add_convert_fusion), channel_id=1, source_target_pairs={{0,2},{1,3},{2,0},{3,1},{4,6},{5,7},{6,4},{7,5},{8,10},{9,11},{10,... | collective-permute-start | bytes 196616 | tf_op jit(solution)/shard_map/ppermute | solution.py:51
  40.3 16.4 %collective-permute-start.12 = (bf16[64,512]{1,0:T(8,128)(2,1)S(1)}, bf16[64,512]{1,0:T(8,128)(2,1)S(1)}, u32[]{:S(2)}, u32[]{:S(2)}) collective-permute-start(bf16[64,512]{1,0:T(8,128)(2,1)S(1)} %add_convert_fusion), channel_id=1, source_target_pairs={{0,6},{1,7},{2,4},{3,5},{4,2},{5,3},{6,0},{7,1},{8,14},{9,15},{10,... | collective-permute-start | bytes 196616 | tf_op jit(solution)/shard_map/ppermute | solution.py:51
  42.0 14.6 %collective-permute-start.13 = (bf16[64,512]{1,0:T(8,128)(2,1)S(1)}, bf16[64,512]{1,0:T(8,128)(2,1)S(1)}, u32[]{:S(2)}, u32[]{:S(2)}) collective-permute-start(bf16[64,512]{1,0:T(8,128)(2,1)S(1)} %add_convert_fusion), channel_id=1, source_target_pairs={{0,4},{1,5},{2,6},{3,7},{4,0},{5,1},{6,2},{7,3},{8,12},{9,13},{10,... | collective-permute-start | bytes 196616 | tf_op jit(solution)/shard_map/ppermute | solution.py:51
  57.4 6.2 %collective-permute-start.20 = (bf16[32,768]{1,0:T(8,128)(2,1)S(1)}, bf16[32,768]{1,0:T(8,128)(2,1)S(1)}, u32[]{:S(2)}, u32[]{:S(2)}) collective-permute-start(bf16[32,768]{1,0:T(8,128)(2,1)S(1)} %get-tuple-element.53), channel_id=1, source_target_pairs={{0,24},{4,28},{8,16},{12,20},{16,8},{20,12},{24,0},{28,4},{1,25},{... | collective-permute-start | bytes 147464 | tf_op jit(solution)/shard_map/ppermute | solution.py:44
  60.6 6.6 %collective-permute-start.21 = (bf16[32,768]{1,0:T(8,128)(2,1)S(1)}, bf16[32,768]{1,0:T(8,128)(2,1)S(1)}, u32[]{:S(2)}, u32[]{:S(2)}) collective-permute-start(bf16[32,768]{1,0:T(8,128)(2,1)S(1)} %get-tuple-element.54), channel_id=1, source_target_pairs={{0,16},{4,20},{8,24},{12,28},{16,0},{20,4},{24,8},{28,12},{1,17},{... | collective-permute-start | bytes 147464 | tf_op jit(solution)/shard_map/ppermute | solution.py:44
  60.6 10.7 %collective-permute-start.16 = (bf16[200,128]{1,0:T(8,128)(2,1)S(1)}, bf16[200,128]{1,0:T(8,128)(2,1)S(1)}, u32[]{:S(2)}, u32[]{:S(2)}) collective-permute-start(bf16[200,128]{1,0:T(8,128)(2,1)S(1)} %get-tuple-element.46), channel_id=1, source_target_pairs={{0,24},{4,28},{8,16},{12,20},{16,8},{20,12},{24,0},{28,4},{1,25},{... | collective-permute-start | bytes 153608 | tf_op jit(solution)/shard_map/ppermute | solution.py:44
  61.3 10.0 %collective-permute-start.17 = (bf16[200,128]{1,0:T(8,128)(2,1)S(1)}, bf16[200,128]{1,0:T(8,128)(2,1)S(1)}, u32[]{:S(2)}, u32[]{:S(2)}) collective-permute-start(bf16[200,128]{1,0:T(8,128)(2,1)S(1)} %get-tuple-element.47), channel_id=1, source_target_pairs={{0,16},{4,20},{8,24},{12,28},{16,0},{20,4},{24,8},{28,12},{1,17},{... | collective-permute-start | bytes 153608 | tf_op jit(solution)/shard_map/ppermute | solution.py:44
  63.6 7.8 %collective-permute-start.18 = (bf16[200,128]{1,0:T(8,128)(2,1)S(1)}, bf16[200,128]{1,0:T(8,128)(2,1)S(1)}, u32[]{:S(2)}, u32[]{:S(2)}) collective-permute-start(bf16[200,128]{1,0:T(8,128)(2,1)S(1)} %get-tuple-element.48), channel_id=1, source_target_pairs={{0,8},{4,12},{8,0},{12,4},{16,24},{20,28},{24,16},{28,20},{1,9},{5... | collective-permute-start | bytes 153608 | tf_op jit(solution)/shard_map/ppermute | solution.py:44
  67.2 4.1 %collective-permute-start.22 = (bf16[32,768]{1,0:T(8,128)(2,1)S(1)}, bf16[32,768]{1,0:T(8,128)(2,1)S(1)}, u32[]{:S(2)}, u32[]{:S(2)}) collective-permute-start(bf16[32,768]{1,0:T(8,128)(2,1)S(1)} %get-tuple-element.55), channel_id=1, source_target_pairs={{0,8},{4,12},{8,0},{12,4},{16,24},{20,28},{24,16},{28,20},{1,9},{5... | collective-permute-start | bytes 147464 | tf_op jit(solution)/shard_map/ppermute | solution.py:44
  71.5 4.5 %collective-permute-start.23 = (bf16[32,768]{1,0:T(8,128)(2,1)S(1)}, bf16[32,768]{1,0:T(8,128)(2,1)S(1)}, u32[]{:S(2)}, u32[]{:S(2)}) collective-permute-start(bf16[32,768]{1,0:T(8,128)(2,1)S(1)} %shard_map.165.refs_0_), channel_id=1, source_target_pairs={{0,8},{4,12},{8,0},{12,4},{16,24},{20,28},{24,16},{28,20},{1,9},{5... | collective-permute-start | bytes 147464 | tf_op jit(solution)/shard_map/ppermute | solution.py:44
  71.6 5.5 %collective-permute-start.24 = (bf16[32,768]{1,0:T(8,128)(2,1)S(1)}, bf16[32,768]{1,0:T(8,128)(2,1)S(1)}, u32[]{:S(2)}, u32[]{:S(2)}) collective-permute-start(bf16[32,768]{1,0:T(8,128)(2,1)S(1)} %shard_map.165.refs_0_), channel_id=1, source_target_pairs={{0,16},{4,20},{8,24},{12,28},{16,0},{20,4},{24,8},{28,12},{1,17},{... | collective-permute-start | bytes 147464 | tf_op jit(solution)/shard_map/ppermute | solution.py:44
  74.8 5.9 %collective-permute-start.25 = (bf16[32,768]{1,0:T(8,128)(2,1)S(1)}, bf16[32,768]{1,0:T(8,128)(2,1)S(1)}, u32[]{:S(2)}, u32[]{:S(2)}) collective-permute-start(bf16[32,768]{1,0:T(8,128)(2,1)S(1)} %shard_map.165.refs_0_), channel_id=1, source_target_pairs={{0,24},{4,28},{8,16},{12,20},{16,8},{20,12},{24,0},{28,4},{1,25},{... | collective-permute-start | bytes 147464 | tf_op jit(solution)/shard_map/ppermute | solution.py:44
  80.9 1.4 %collective-permute-start.27 = (bf16[128,512]{1,0:T(8,128)(2,1)S(1)}, bf16[128,512]{1,0:T(8,128)(2,1)S(1)}, u32[]{:S(2)}, u32[]{:S(2)}) collective-permute-start(bf16[128,512]{1,0:T(8,128)(2,1)S(1)} %shard_map.166), channel_id=1, source_target_pairs={{0,1},{1,0},{2,3},{3,2},{4,5},{5,4},{6,7},{7,6},{8,9},{9,8},{10,11... | collective-permute-start | bytes 393224 | tf_op jit(solution)/shard_map/ppermute | solution.py:44
  82.4 8.2 %collective-permute-start.30 = (bf16[128,256]{1,0:T(8,128)(2,1)S(1)}, bf16[128,256]{1,0:T(8,128)(2,1)S(1)}, u32[]{:S(2)}, u32[]{:S(2)}) collective-permute-start(bf16[128,256]{1,0:T(8,128)(2,1)S(1)} %get-tuple-element.61), channel_id=1, source_target_pairs={{0,4},{1,5},{2,6},{3,7},{4,0},{5,1},{6,2},{7,3},{8,12},{9,13},{10,... | collective-permute-start | bytes 196616 | tf_op jit(solution)/shard_map/ppermute | solution.py:51
  83.0 7.6 %collective-permute-start.29 = (bf16[128,256]{1,0:T(8,128)(2,1)S(1)}, bf16[128,256]{1,0:T(8,128)(2,1)S(1)}, u32[]{:S(2)}, u32[]{:S(2)}) collective-permute-start(bf16[128,256]{1,0:T(8,128)(2,1)S(1)} %get-tuple-element.61), channel_id=1, source_target_pairs={{0,6},{1,7},{2,4},{3,5},{4,2},{5,3},{6,0},{7,1},{8,14},{9,15},{10,... | collective-permute-start | bytes 196616 | tf_op jit(solution)/shard_map/ppermute | solution.py:51
  85.4 2.2 %copy-start.1 = (f32[16,2,128,256]{3,2,1,0:T(8,128)S(1)}, f32[16,2,128,256]{3,2,1,0:T(8,128)}, u32[]{:S(2)}) copy-start(f32[16,2,128,256]{3,2,1,0:T(8,128)} %copy-done) | copy-start | bytes 12582916
  90.0 4.3 %collective-permute-start.28 = (bf16[128,256]{1,0:T(8,128)(2,1)S(1)}, bf16[128,256]{1,0:T(8,128)(2,1)S(1)}, u32[]{:S(2)}, u32[]{:S(2)}) collective-permute-start(bf16[128,256]{1,0:T(8,128)(2,1)S(1)} %get-tuple-element.60), channel_id=1, source_target_pairs={{0,2},{1,3},{2,0},{3,1},{4,6},{5,7},{6,4},{7,5},{8,10},{9,11},{10,... | collective-permute-start | bytes 196616 | tf_op jit(solution)/shard_map/ppermute | solution.py:51

commit v4 on v3

--- a/solution.py
+++ b/solution.py
@@ -16,7 +16,7 @@
 STEPS = 8
 SCATTER = (1, 3, 4, 5, 6, 2)
 NEAR = (6, 4, 2)
-FF_GATE = (6, 4, 2)
+FF_GATE = (4, 6, 2)
 FF_UP = (6, 4, 2)
 LATE = 4
 HIDDEN = (6, 4, 2)
@@ -137,8 +137,10 @@
         load.wait()
     mine = jnp.concatenate([block_of(tokens, me, m, rows) for m in range(count)], axis=0)
     total, model = tokens.shape
-    pair_out[:total] = mine
-    pair_out[total:] = jnp.broadcast_to(row(mixer_gain), (rows, model)).astype(jnp.bfloat16)
+    share = total // 2
+    first_rows = lax.rem(lax.axis_index("tp"), 2) == 0
+    pair_out[:share] = jnp.where(first_rows, mine[:share], mine[share:])
+    pair_out[share:] = jnp.broadcast_to(row(mixer_gain), (rows, model)).astype(jnp.bfloat16)
     mine = wide(mine)
     scaled = (mine * row(norm_gain)).astype(jnp.bfloat16)
     squares = split_squares(jnp.sum(mine * mine, axis=1, keepdims=True))
@@ -235,8 +237,8 @@
 
 def middle_kernel(n_even, n_odd, *refs):
     evens, odds = refs[:n_even], refs[n_even : n_even + n_odd]
-    tokens, pair, mixer_gain, ffgate, sent = refs[n_even + n_odd :][:5]
-    middle_out, own_out, other_out, *pieces = refs[n_even + n_odd + 5 :]
+    tokens, pair, pair_core, mixer_gain, ffgate, sent = refs[n_even + n_odd :][:6]
+    middle_out, own_out, other_out, *pieces = refs[n_even + n_odd + 6 :]
     me = lax.axis_index("kv")
     batch, model = tokens.shape
     half = ffgate.shape[1] // 2
@@ -245,8 +247,13 @@
     even = sum(wide(ref[...]) for ref in evens)
     odd = sum(wide(ref[...]) for ref in odds)
 
+    first_rows = lax.rem(lax.axis_index("tp"), 2) == 0
+
     def pair_block(m):
-        return pair[(m ^ 1) * rows : ((m ^ 1) + 1) * rows]
+        at = (m ^ 1) * rows
+        low = at < batch // 2
+        part = slice(at % (batch // 2), at % (batch // 2) + rows)
+        return jnp.where(first_rows == low, pair[part], pair_core[part])
 
     def stream(stay, first, second):
         blocks = []
@@ -259,7 +266,7 @@
     other = stream(pair_block, even[:, model:], odd[:, :model])
     middle_out[...] = own.astype(jnp.bfloat16)
     own2 = (own * row(mixer_gain)).astype(jnp.bfloat16)
-    other2 = (other * wide(pair[batch : batch + 1])).astype(jnp.bfloat16)
+    other2 = (other * wide(pair[batch // 2 : batch // 2 + 1])).astype(jnp.bfloat16)
     own_out[...] = own2
     other_out[...] = other2
     squares = jnp.sum(own * own, axis=1, keepdims=True) + jnp.sum(other * other, axis=1, keepdims=True)
@@ -340,7 +347,7 @@
         functools.partial(project_kernel, n_kv, rows),
         [shape((rows + (m == 1) * rows, total_width)) for m in range(n_kv - 1)]
         + [shape((model, half + half - late)), shape((model, late))]
-        + [shape((half, model)), shape((batch + rows, model))],
+        + [shape((half, model)), shape((batch // 2 + rows, model))],
         *in_hbm(*loaded, w_ffgate, w_ffup, w_down),
         specs=[HBM] * 11,
         out_specs=[VMEM] * (n_kv + 3),
@@ -357,6 +364,7 @@
     out_pair = send_xor(w_out, kv, (1,))
     early_pair = send_xor(early_sent, kv, (1,))
     pair = send_xor(pair_sent, kv, (1,))
+    pair_core = send_xor(pair, tp, (1,))
     late_pair = send_xor(late_sent, kv, (1,))
     down_pair = send_xor(down_sent, kv, (1,))
     state_near, log_decay_near, out_gain_near = call(
@@ -419,6 +427,7 @@
         *odd,
         tokens,
         pair,
+        pair_core,
         mixer_gain,
         w_ffgate,
         early_pair,

time: 95.4 us -> 93.7 us (0.982)
  waiting for transfers between devices: 39.6 us -> 38.6 us
    ppermute x6, waiting for transfers between devices: 17.3 us -> 15.9 us  [send_xor(): return lax.ppermute(array, (first, second), pairs)]
    ppermute x25 -> x26, starting transfers between devices: 34.4 us -> 33.6 us  [send_xor(): return lax.ppermute(array, axis, pairs)]
    ppermute x25 -> x26, waiting for transfers between devices: 22.3 us -> 22.7 us  [send_xor(): return lax.ppermute(array, axis, pairs)]
  transfers between devices with their start and end apart: 31 -> 32, of which waited for: 14 -> 15; matrix products, arithmetic and copies ran while one was open for 0% -> 0% of each run, Pallas kernels for 9% -> 9%
where the time goes in v4:
time: 93.7 us; the launch traced here: 93.5 us
  starting transfers between devices  41.7 us (45%)
  waiting for transfers between devices  38.6 us (41%)
  Pallas kernels  9.11 us (10%)
  local copies, waits for them, and re-layouts  2.27 us (2%)
  between operations  0.95 us (1%)
    ppermute x26, starting transfers between devices, send_xor(): return lax.ppermute(array, axis, pairs)  33.6 us
    ppermute x26, waiting for transfers between devices, send_xor(): return lax.ppermute(array, axis, pairs)  22.7 us
    ppermute x6, waiting for transfers between devices, send_xor(): return lax.ppermute(array, (first, second), pairs)  15.9 us
    pallas_call x10, Pallas kernels, call(): pl.pallas_call(kernel, out_shape=outs, in_specs=specs or [VMEM] * len(arg...  9.11 us
    ppermute x6, starting transfers between devices, send_xor(): return lax.ppermute(array, (first, second), pairs)  8.1 us
    unnamed x16, local copies, waits for them, and re-layouts  2.22 us
  transfers between devices with their start and end apart: 32, of which 15 were waited for; matrix products, arithmetic and copies ran while one was open for 0% of the time, Pallas kernels for 9%

profile of v4, /device:TPU:0, one launch (start us, length us, event | category | flops | bytes accessed | tf_op | source)
XLA Modules:
  0.0 93.5 jit_solution(16687463857463031127)
XLA Ops:
  0.6 3.0 %collective-permute-start.9 = (bf16[512,256]{1,0:T(8,128)(2,1)}, bf16[512,256]{1,0:T(8,128)(2,1)S(1)}, u32[]{:S(2)}, u32[]{:S(2)}) collective-permute-start(bf16[512,256]{1,0:T(8,128)(2,1)} %refs_4_.4), channel_id=1, source_target_pairs={{0,4},{4,0},{8,12},{12,8},{16,20},{20,16},{24,28},{28,24},{1,5},{5... | collective-permute-start | bytes 786440 | tf_op jit(solution)/shard_map/ppermute | solution.py:44
  3.7 2.0 %shard_map.158 = (bf16[16,1920]{1,0:T(8,128)(2,1)S(1)}, bf16[32,1920]{1,0:T(8,128)(2,1)S(1)}, bf16[16,1920]{1,0:T(8,128)(2,1)S(1)}, bf16[16,1920]{1,0:T(8,128)(2...) custom-call(bf16[128,256]{1,0:T(8,128)(2,1)} %refs_5_.3, ...), custom_call_target="tpu_custom_call" | custom-call | tf_op jit(solution)/shard_map/pallas_call | solution.py:78
  5.7 0.1 collective-permute-start
  5.8 3.0 %collective-permute-start.1 = (bf16[16,1920]{1,0:T(8,128)(2,1)S(1)}, bf16[16,1920]{1,0:T(8,128)(2,1)S(1)}, u32[]{:S(2)}, u32[]{:S(2)}) collective-permute-start(bf16[16,1920]{1,0:T(8,128)(2,1)S(1)} %get-tuple-element.33), channel_id=1, source_target_pairs={{0,12},{4,8},{8,4},{12,0},{16,28},{20,24},{24,20},{28,16},{1,13},{... | collective-permute-start | bytes 184328 | tf_op jit(solution)/shard_map/ppermute | solution.py:44
  8.8 2.6 %collective-permute-start.2 = (bf16[16,1920]{1,0:T(8,128)(2,1)S(1)}, bf16[16,1920]{1,0:T(8,128)(2,1)S(1)}, u32[]{:S(2)}, u32[]{:S(2)}) collective-permute-start(bf16[16,1920]{1,0:T(8,128)(2,1)S(1)} %get-tuple-element.34), channel_id=1, source_target_pairs={{0,16},{4,20},{8,24},{12,28},{16,0},{20,4},{24,8},{28,12},{1,17},{... | collective-permute-start | bytes 184328 | tf_op jit(solution)/shard_map/ppermute | solution.py:44
  11.4 0.5 collective-permute-start.16
  11.9 3.1 %collective-permute-done.came.refs_1_ = bf16[32,1920]{1,0:T(8,128)(2,1)S(1)} collective-permute-done((bf16[32,1920]{1,0:T(8,128)(2,1)S(1)}, bf16[32,1920]{1,0:T(8,128)(2,1)S(1)}, u32[]{:S(2)}, u32[]{:S(2)}) %collective-permute-start) | collective-permute-done | bytes 122912 | tf_op jit(solution)/shard_map/ppermute | solution.py:44
  15.0 4.0 %collective-permute-start.3 = (bf16[16,1920]{1,0:T(8,128)(2,1)S(1)}, bf16[16,1920]{1,0:T(8,128)(2,1)S(1)}, u32[]{:S(2)}, u32[]{:S(2)}) collective-permute-start(bf16[16,1920]{1,0:T(8,128)(2,1)S(1)} %get-tuple-element.35), channel_id=1, source_target_pairs={{0,20},{4,16},{8,28},{12,24},{16,4},{20,0},{24,12},{28,8},{1,21},{... | collective-permute-start | bytes 184328 | tf_op jit(solution)/shard_map/ppermute | solution.py:44
  19.0 0.2 shard_map.159
  19.2 0.0 collective-permute-done.1.refs_2_
  19.2 0.0 copy-start.6
  19.2 0.0 copy-start.7
  19.2 1.6 %collective-permute-start.5 = (bf16[16,1920]{1,0:T(8,128)(2,1)S(1)}, bf16[16,1920]{1,0:T(8,128)(2,1)S(1)}, u32[]{:S(2)}, u32[]{:S(2)}) collective-permute-start(bf16[16,1920]{1,0:T(8,128)(2,1)S(1)} %get-tuple-element.37), channel_id=1, source_target_pairs={{0,8},{4,12},{8,0},{12,4},{16,24},{20,28},{24,16},{28,20},{1,9},{5... | collective-permute-start | bytes 184328 | tf_op jit(solution)/shard_map/ppermute | solution.py:44
  20.9 0.0 collective-permute-done.2.refs_3_
  20.9 0.2 collective-permute-start.4
  21.1 2.2 %shard_map.160 = (f32[16,2,128,256]{3,2,1,0:T(8,128)S(1)}, f32[16,256]{1,0:T(8,128)S(1)}, f32[256]{0:T(256)S(1)}) custom-call(f32[16,2,128,256]{3,2,1,0:T(8,128)} %refs_0_.3, f32[16,256]{1,0:T(8,128)} %refs_1_.3, f32[256]{0:T(256)} %refs_2_.3), custom_call_target="tpu_custom_call" | custom-call | tf_op jit(solution)/shard_map/pallas_call | solution.py:78
  23.3 0.0 copy-start
  23.3 0.0 copy-start.4
  23.3 0.7 collective-permute-done.5.refs_6_
  24.0 2.9 %collective-permute-done.4.refs_5_ = bf16[16,1920]{1,0:T(8,128)(2,1)S(1)} collective-permute-done((bf16[16,1920]{1,0:T(8,128)(2,1)S(1)}, bf16[16,1920]{1,0:T(8,128)(2,1)S(1)}, u32[]{:S(2)}, u32[]{:S(2)}) %collective-permute-start.4) | collective-permute-done | bytes 61472 | tf_op jit(solution)/shard_map/ppermute | solution.py:44
  26.9 1.1 %shard_map.161 = (bf16[16,512]{1,0:T(8,128)(2,1)S(1)}, f32[16,256]{1,0:T(8,128)S(1)}, f32[16,256]{1,0:T(8,128)S(1)}, f32[16,512]{1,0:T(8,128)S(1)}) custom-call(bf16[16,1920]{1,0:T(8,128)(2,1)S(1)} %get-tuple-element.31.refs_0_, bf16[32,1920]{1,0:T(8,128)(2,1)S(1)} %collective-permute-done.came.refs_1_, bf16[16,1920]{1,0:T(8,128)(2,1)S(1)} %collective-permute-done.1.refs_2_, ...), custom_call_target="tpu_custom_call" | custom-call | tf_op jit(solution)/shard_map/pallas_call | solution.py:78
  27.9 0.1 collective-permute-start.6
  28.0 1.2 %collective-permute-start.7 = (bf16[16,512]{1,0:T(8,128)(2,1)S(1)}, bf16[16,512]{1,0:T(8,128)(2,1)S(1)}, u32[]{:S(2)}, u32[]{:S(2)}) collective-permute-start(bf16[16,512]{1,0:T(8,128)(2,1)S(1)} %get-tuple-element.41.refs_0_), channel_id=1, source_target_pairs={{0,16},{4,20},{8,24},{12,28},{16,0},{20,4},{24,8},{28,12},{1,17},{... | collective-permute-start | bytes 49160 | tf_op jit(solution)/shard_map/ppermute | solution.py:44
  29.2 3.2 %collective-permute-start.8 = (bf16[16,512]{1,0:T(8,128)(2,1)S(1)}, bf16[16,512]{1,0:T(8,128)(2,1)S(1)}, u32[]{:S(2)}, u32[]{:S(2)}) collective-permute-start(bf16[16,512]{1,0:T(8,128)(2,1)S(1)} %get-tuple-element.41.refs_0_), channel_id=1, source_target_pairs={{0,24},{4,28},{8,16},{12,20},{16,8},{20,12},{24,0},{28,4},{1,25},{... | collective-permute-start | bytes 49160 | tf_op jit(solution)/shard_map/ppermute | solution.py:44
  32.4 0.0 collective-permute-done.6.refs_1_
  32.4 0.3 collective-permute-done.7.refs_2_
  32.7 2.0 %collective-permute-done.8.refs_3_ = bf16[16,512]{1,0:T(8,128)(2,1)S(1)} collective-permute-done((bf16[16,512]{1,0:T(8,128)(2,1)S(1)}, bf16[16,512]{1,0:T(8,128)(2,1)S(1)}, u32[]{:S(2)}, u32[]{:S(2)}) %collective-permute-start.8) | collective-permute-done | bytes 16416 | tf_op jit(solution)/shard_map/ppermute | solution.py:44
  34.8 0.0 collective-permute-done.9.refs_5_
  34.8 0.2 shard_map.162.refs_0_
  35.0 0.1 collective-permute-start.10
  35.1 0.6 collective-permute-start.14
  35.7 1.5 %collective-permute-start.20 = (bf16[256,512]{1,0:T(8,128)(2,1)S(1)}, bf16[256,512]{1,0:T(8,128)(2,1)S(1)}, u32[]{:S(2)}, u32[]{:S(2)}) collective-permute-start(bf16[256,512]{1,0:T(8,128)(2,1)S(1)} %get-tuple-element.51), channel_id=1, source_target_pairs={{0,4},{4,0},{8,12},{12,8},{16,20},{20,16},{24,28},{28,24},{1,5},{5... | collective-permute-start | bytes 786440 | tf_op jit(solution)/shard_map/ppermute | solution.py:44
  37.2 0.5 collective-permute-start.27
  37.7 0.0 collective-permute-done.10.refs_1_
  37.7 1.6 %collective-permute-start.11 = (bf16[64,512]{1,0:T(8,128)(2,1)S(1)}, bf16[64,512]{1,0:T(8,128)(2,1)S(1)}, u32[]{:S(2)}, u32[]{:S(2)}) collective-permute-start(bf16[64,512]{1,0:T(8,128)(2,1)S(1)} %add_convert_fusion), channel_id=1, source_target_pairs={{0,2},{1,3},{2,0},{3,1},{4,6},{5,7},{6,4},{7,5},{8,10},{9,11},{10,... | collective-permute-start | bytes 196616 | tf_op jit(solution)/shard_map/ppermute | solution.py:51
  39.3 0.3 collective-permute-done.14.refs_6_
  39.6 1.2 %collective-permute-done.15.refs_7_ = bf16[80,256]{1,0:T(8,128)(2,1)S(1)} collective-permute-done((bf16[80,256]{1,0:T(8,128)(2,1)S(1)}, bf16[80,256]{1,0:T(8,128)(2,1)S(1)}, u32[]{:S(2)}, u32[]{:S(2)}) %collective-permute-start.15) | collective-permute-done | bytes 40992 | tf_op jit(solution)/shard_map/ppermute | solution.py:44
  40.8 1.2 %collective-permute-start.12 = (bf16[64,512]{1,0:T(8,128)(2,1)S(1)}, bf16[64,512]{1,0:T(8,128)(2,1)S(1)}, u32[]{:S(2)}, u32[]{:S(2)}) collective-permute-start(bf16[64,512]{1,0:T(8,128)(2,1)S(1)} %add_convert_fusion), channel_id=1, source_target_pairs={{0,6},{1,7},{2,4},{3,5},{4,2},{5,3},{6,0},{7,1},{8,14},{9,15},{10,... | collective-permute-start | bytes 196616 | tf_op jit(solution)/shard_map/ppermute | solution.py:51
  42.0 0.1 collective-permute-done.11.refs_2_
  42.0 1.7 %collective-permute-start.13 = (bf16[64,512]{1,0:T(8,128)(2,1)S(1)}, bf16[64,512]{1,0:T(8,128)(2,1)S(1)}, u32[]{:S(2)}, u32[]{:S(2)}) collective-permute-start(bf16[64,512]{1,0:T(8,128)(2,1)S(1)} %add_convert_fusion), channel_id=1, source_target_pairs={{0,4},{1,5},{2,6},{3,7},{4,0},{5,1},{6,2},{7,3},{8,12},{9,13},{10,... | collective-permute-start | bytes 196616 | tf_op jit(solution)/shard_map/ppermute | solution.py:51
  43.8 12.2 %collective-permute-done.12.refs_3_ = bf16[64,512]{1,0:T(8,128)(2,1)S(1)} collective-permute-done((bf16[64,512]{1,0:T(8,128)(2,1)S(1)}, bf16[64,512]{1,0:T(8,128)(2,1)S(1)}, u32[]{:S(2)}, u32[]{:S(2)}) %collective-permute-start.12) | collective-permute-done | bytes 65568 | tf_op jit(solution)/shard_map/ppermute | solution.py:51
  56.0 0.3 shard_map.163
  56.4 0.3 shard_map.164
  56.7 3.2 %collective-permute-start.21 = (bf16[32,768]{1,0:T(8,128)(2,1)S(1)}, bf16[32,768]{1,0:T(8,128)(2,1)S(1)}, u32[]{:S(2)}, u32[]{:S(2)}) collective-permute-start(bf16[32,768]{1,0:T(8,128)(2,1)S(1)} %get-tuple-element.53), channel_id=1, source_target_pairs={{0,24},{4,28},{8,16},{12,20},{16,8},{20,12},{24,0},{28,4},{1,25},{... | collective-permute-start | bytes 147464 | tf_op jit(solution)/shard_map/ppermute | solution.py:44
  59.9 2.9 %collective-permute-start.17 = (bf16[200,128]{1,0:T(8,128)(2,1)S(1)}, bf16[200,128]{1,0:T(8,128)(2,1)S(1)}, u32[]{:S(2)}, u32[]{:S(2)}) collective-permute-start(bf16[200,128]{1,0:T(8,128)(2,1)S(1)} %get-tuple-element.46), channel_id=1, source_target_pairs={{0,16},{4,20},{8,24},{12,28},{16,0},{20,4},{24,8},{28,12},{1,17},{... | collective-permute-start | bytes 153608 | tf_op jit(solution)/shard_map/ppermute | solution.py:44
  62.8 0.7 collective-permute-start.18
  63.5 3.0 %collective-permute-done.22.refs_6_ = bf16[32,768]{1,0:T(8,128)(2,1)S(1)} collective-permute-done((bf16[32,768]{1,0:T(8,128)(2,1)S(1)}, bf16[32,768]{1,0:T(8,128)(2,1)S(1)}, u32[]{:S(2)}, u32[]{:S(2)}) %collective-permute-start.22) | collective-permute-done | bytes 49184 | tf_op jit(solution)/shard_map/ppermute | solution.py:44
  66.5 4.1 %collective-permute-done.23.refs_7_ = bf16[32,768]{1,0:T(8,128)(2,1)S(1)} collective-permute-done((bf16[32,768]{1,0:T(8,128)(2,1)S(1)}, bf16[32,768]{1,0:T(8,128)(2,1)S(1)}, u32[]{:S(2)}, u32[]{:S(2)}) %collective-permute-start.23) | collective-permute-done | bytes 49184 | tf_op jit(solution)/shard_map/ppermute | solution.py:44
  70.6 0.2 shard_map.165.refs_0_
  70.8 0.1 collective-permute-start.24
  70.9 2.3 %collective-permute-start.25 = (bf16[32,768]{1,0:T(8,128)(2,1)S(1)}, bf16[32,768]{1,0:T(8,128)(2,1)S(1)}, u32[]{:S(2)}, u32[]{:S(2)}) collective-permute-start(bf16[32,768]{1,0:T(8,128)(2,1)S(1)} %shard_map.165.refs_0_), channel_id=1, source_target_pairs={{0,16},{4,20},{8,24},{12,28},{16,0},{20,4},{24,8},{28,12},{1,17},{... | collective-permute-start | bytes 147464 | tf_op jit(solution)/shard_map/ppermute | solution.py:44
  73.2 2.1 %collective-permute-start.26 = (bf16[32,768]{1,0:T(8,128)(2,1)S(1)}, bf16[32,768]{1,0:T(8,128)(2,1)S(1)}, u32[]{:S(2)}, u32[]{:S(2)}) collective-permute-start(bf16[32,768]{1,0:T(8,128)(2,1)S(1)} %shard_map.165.refs_0_), channel_id=1, source_target_pairs={{0,24},{4,28},{8,16},{12,20},{16,8},{20,12},{24,0},{28,4},{1,25},{... | collective-permute-start | bytes 147464 | tf_op jit(solution)/shard_map/ppermute | solution.py:44
  75.3 0.9 collective-permute-done.25.refs_2_
  76.2 2.9 %collective-permute-done.26.refs_3_ = bf16[32,768]{1,0:T(8,128)(2,1)S(1)} collective-permute-done((bf16[32,768]{1,0:T(8,128)(2,1)S(1)}, bf16[32,768]{1,0:T(8,128)(2,1)S(1)}, u32[]{:S(2)}, u32[]{:S(2)}) %collective-permute-start.26) | collective-permute-done | bytes 49184 | tf_op jit(solution)/shard_map/ppermute | solution.py:44
  79.0 0.3 shard_map.166
  79.3 0.1 collective-permute-start.28
  79.4 1.3 %collective-permute-done.28 = bf16[128,512]{1,0:T(8,128)(2,1)S(1)} collective-permute-done((bf16[128,512]{1,0:T(8,128)(2,1)S(1)}, bf16[128,512]{1,0:T(8,128)(2,1)S(1)}, u32[]{:S(2)}, u32[]{:S(2)}) %collective-permute-start.28) | collective-permute-done | bytes 131104 | tf_op jit(solution)/shard_map/ppermute | solution.py:44
  80.8 1.0 %collective-permute-start.31 = (bf16[128,256]{1,0:T(8,128)(2,1)S(1)}, bf16[128,256]{1,0:T(8,128)(2,1)S(1)}, u32[]{:S(2)}, u32[]{:S(2)}) collective-permute-start(bf16[128,256]{1,0:T(8,128)(2,1)S(1)} %get-tuple-element.61), channel_id=1, source_target_pairs={{0,4},{1,5},{2,6},{3,7},{4,0},{5,1},{6,2},{7,3},{8,12},{9,13},{10,... | collective-permute-start | bytes 196616 | tf_op jit(solution)/shard_map/ppermute | solution.py:51
  81.8 1.9 %collective-permute-start.30 = (bf16[128,256]{1,0:T(8,128)(2,1)S(1)}, bf16[128,256]{1,0:T(8,128)(2,1)S(1)}, u32[]{:S(2)}, u32[]{:S(2)}) collective-permute-start(bf16[128,256]{1,0:T(8,128)(2,1)S(1)} %get-tuple-element.61), channel_id=1, source_target_pairs={{0,6},{1,7},{2,4},{3,5},{4,2},{5,3},{6,0},{7,1},{8,14},{9,15},{10,... | collective-permute-start | bytes 196616 | tf_op jit(solution)/shard_map/ppermute | solution.py:51
  83.7 2.2 %copy-done.1 = f32[16,2,128,256]{3,2,1,0:T(8,128)S(1)} copy-done((f32[16,2,128,256]{3,2,1,0:T(8,128)S(1)}, f32[16,2,128,256]{3,2,1,0:T(8,128)}, u32[]{:S(2)}) %copy-start.1) | copy-done | bytes 4194328
  85.9 2.4 %shard_map.167 = f32[16,2,128,256]{3,2,1,0:T(8,128)} custom-call(f32[16,2,128,256]{3,2,1,0:T(8,128)S(1)} %copy-done.1, f32[16,256]{1,0:T(8,128)S(1)} %get-tuple-element.57.keep, f32[16,256]{1,0:T(8,128)S(1)} %get-tuple-element.58.keys, f32[16,512]{1,0:T(8,128)S(1)} %get-tuple-element.59.values), custom_call_target="tpu_custom_call" | custom-call | tf_op jit(solution)/shard_map/pallas_call | solution.py:78
  88.3 0.7 collective-permute-start.29
  89.1 3.6 %collective-permute-done.29 = bf16[128,256]{1,0:T(8,128)(2,1)S(1)} collective-permute-done((bf16[128,256]{1,0:T(8,128)(2,1)S(1)}, bf16[128,256]{1,0:T(8,128)(2,1)S(1)}, u32[]{:S(2)}, u32[]{:S(2)}) %collective-permute-start.29) | collective-permute-done | bytes 65568 | tf_op jit(solution)/shard_map/ppermute | solution.py:51
  92.8 0.7 fusion.2
  (42 shorter events, 0.3 us)
Async XLA Ops:
  0.6 34.1 %collective-permute-start.9 = (bf16[512,256]{1,0:T(8,128)(2,1)}, bf16[512,256]{1,0:T(8,128)(2,1)S(1)}, u32[]{:S(2)}, u32[]{:S(2)}) collective-permute-start(bf16[512,256]{1,0:T(8,128)(2,1)} %refs_4_.4), channel_id=1, source_target_pairs={{0,4},{4,0},{8,12},{12,8},{16,20},{20,16},{24,28},{28,24},{1,5},{5... | collective-permute-start | bytes 786440 | tf_op jit(solution)/shard_map/ppermute | solution.py:44
  5.7 9.3 %collective-permute-start = (bf16[32,1920]{1,0:T(8,128)(2,1)S(1)}, bf16[32,1920]{1,0:T(8,128)(2,1)S(1)}, u32[]{:S(2)}, u32[]{:S(2)}) collective-permute-start(bf16[32,1920]{1,0:T(8,128)(2,1)S(1)} %get-tuple-element.32), channel_id=1, source_target_pairs={{0,4},{4,0},{8,12},{12,8},{16,20},{20,16},{24,28},{28,24},{1,5},{5... | collective-permute-start | bytes 368648 | tf_op jit(solution)/shard_map/ppermute | solution.py:44
  5.8 13.4 %collective-permute-start.1 = (bf16[16,1920]{1,0:T(8,128)(2,1)S(1)}, bf16[16,1920]{1,0:T(8,128)(2,1)S(1)}, u32[]{:S(2)}, u32[]{:S(2)}) collective-permute-start(bf16[16,1920]{1,0:T(8,128)(2,1)S(1)} %get-tuple-element.33), channel_id=1, source_target_pairs={{0,12},{4,8},{8,4},{12,0},{16,28},{20,24},{24,20},{28,16},{1,13},{... | collective-permute-start | bytes 184328 | tf_op jit(solution)/shard_map/ppermute | solution.py:44
  8.8 12.1 %collective-permute-start.2 = (bf16[16,1920]{1,0:T(8,128)(2,1)S(1)}, bf16[16,1920]{1,0:T(8,128)(2,1)S(1)}, u32[]{:S(2)}, u32[]{:S(2)}) collective-permute-start(bf16[16,1920]{1,0:T(8,128)(2,1)S(1)} %get-tuple-element.34), channel_id=1, source_target_pairs={{0,16},{4,20},{8,24},{12,28},{16,0},{20,4},{24,8},{28,12},{1,17},{... | collective-permute-start | bytes 184328 | tf_op jit(solution)/shard_map/ppermute | solution.py:44
  11.4 44.6 %collective-permute-start.16 = (bf16[256,1024]{1,0:T(8,128)(2,1)S(1)}, bf16[256,1024]{1,0:T(8,128)(2,1)S(1)}, u32[]{:S(2)}, u32[]{:S(2)}) collective-permute-start(bf16[256,1024]{1,0:T(8,128)(2,1)S(1)} %get-tuple-element.43), channel_id=1, source_target_pairs={{0,4},{4,0},{8,12},{12,8},{16,20},{20,16},{24,28},{28,24},{1,5},{5... | collective-permute-start | bytes 1572872 | tf_op jit(solution)/shard_map/ppermute | solution.py:44
  15.0 8.4 %collective-permute-start.3 = (bf16[16,1920]{1,0:T(8,128)(2,1)S(1)}, bf16[16,1920]{1,0:T(8,128)(2,1)S(1)}, u32[]{:S(2)}, u32[]{:S(2)}) collective-permute-start(bf16[16,1920]{1,0:T(8,128)(2,1)S(1)} %get-tuple-element.35), channel_id=1, source_target_pairs={{0,20},{4,16},{8,28},{12,24},{16,4},{20,0},{24,12},{28,8},{1,21},{... | collective-permute-start | bytes 184328 | tf_op jit(solution)/shard_map/ppermute | solution.py:44
  19.2 15.6 %copy-start.5 = (bf16[512,256]{1,0:T(8,128)(2,1)S(1)}, bf16[512,256]{1,0:T(8,128)(2,1)}, u32[]{:S(2)}) copy-start(bf16[512,256]{1,0:T(8,128)(2,1)} %refs_4_.4) | copy-start | bytes 786436
  19.2 36.8 %copy-start.3 = (bf16[256,1536]{1,0:T(8,128)(2,1)S(1)}, bf16[256,1536]{1,0:T(8,128)(2,1)}, u32[]{:S(2)}) copy-start(bf16[256,1536]{1,0:T(8,128)(2,1)} %refs_9_.3) | copy-start | bytes 2359300
  19.2 36.8 %copy-start.6 = (bf16[128,256]{1,0:T(8,128)(2,1)S(1)}, bf16[128,256]{1,0:T(8,128)(2,1)}, u32[]{:S(2)}) copy-start(bf16[128,256]{1,0:T(8,128)(2,1)} %refs_5_.3) | copy-start | bytes 196612
  19.2 36.8 %copy-start.7 = (bf16[256]{0:T(256)(128)(2,1)S(1)}, bf16[256]{0:T(256)(128)(2,1)}, u32[]{:S(2)}) copy-start(bf16[256]{0:T(256)(128)(2,1)} %refs_8_.3) | copy-start | bytes 1540
  19.2 4.8 %collective-permute-start.5 = (bf16[16,1920]{1,0:T(8,128)(2,1)S(1)}, bf16[16,1920]{1,0:T(8,128)(2,1)S(1)}, u32[]{:S(2)}, u32[]{:S(2)}) collective-permute-start(bf16[16,1920]{1,0:T(8,128)(2,1)S(1)} %get-tuple-element.37), channel_id=1, source_target_pairs={{0,8},{4,12},{8,0},{12,4},{16,24},{20,28},{24,16},{28,20},{1,9},{5... | collective-permute-start | bytes 184328 | tf_op jit(solution)/shard_map/ppermute | solution.py:44
  20.9 6.0 %collective-permute-start.4 = (bf16[16,1920]{1,0:T(8,128)(2,1)S(1)}, bf16[16,1920]{1,0:T(8,128)(2,1)S(1)}, u32[]{:S(2)}, u32[]{:S(2)}) collective-permute-start(bf16[16,1920]{1,0:T(8,128)(2,1)S(1)} %shard_map.159), channel_id=1, source_target_pairs={{0,24},{4,28},{8,16},{12,20},{16,8},{20,12},{24,0},{28,4},{1,25},{... | collective-permute-start | bytes 184328 | tf_op jit(solution)/shard_map/ppermute | solution.py:44
  23.3 33.4 %copy-start = (f32[16,2,128,256]{3,2,1,0:T(8,128)}, f32[16,2,128,256]{3,2,1,0:T(8,128)S(1)}, u32[]{:S(2)}) copy-start(f32[16,2,128,256]{3,2,1,0:T(8,128)S(1)} %get-tuple-element.39.refs_8_.state) | copy-start | bytes 12582916
  23.3 33.0 %copy-start.4 = (bf16[256,1536]{1,0:T(8,128)(2,1)S(1)}, bf16[256,1536]{1,0:T(8,128)(2,1)}, u32[]{:S(2)}) copy-start(bf16[256,1536]{1,0:T(8,128)(2,1)} %ffup.1) | copy-start | bytes 2359300
  26.9 52.2 %copy-start.2 = (bf16[1536,256]{1,0:T(8,128)(2,1)S(1)}, bf16[1536,256]{1,0:T(8,128)(2,1)}, u32[]{:S(2)}) copy-start(bf16[1536,256]{1,0:T(8,128)(2,1)} %refs_4_.5) | copy-start | bytes 2359300
  27.9 4.4 %collective-permute-start.6 = (bf16[16,512]{1,0:T(8,128)(2,1)S(1)}, bf16[16,512]{1,0:T(8,128)(2,1)S(1)}, u32[]{:S(2)}, u32[]{:S(2)}) collective-permute-start(bf16[16,512]{1,0:T(8,128)(2,1)S(1)} %get-tuple-element.41.refs_0_), channel_id=1, source_target_pairs={{0,8},{4,12},{8,0},{12,4},{16,24},{20,28},{24,16},{28,20},{1,9},{5... | collective-permute-start | bytes 49160 | tf_op jit(solution)/shard_map/ppermute | solution.py:44
  28.0 4.7 %collective-permute-start.7 = (bf16[16,512]{1,0:T(8,128)(2,1)S(1)}, bf16[16,512]{1,0:T(8,128)(2,1)S(1)}, u32[]{:S(2)}, u32[]{:S(2)}) collective-permute-start(bf16[16,512]{1,0:T(8,128)(2,1)S(1)} %get-tuple-element.41.refs_0_), channel_id=1, source_target_pairs={{0,16},{4,20},{8,24},{12,28},{16,0},{20,4},{24,8},{28,12},{1,17},{... | collective-permute-start | bytes 49160 | tf_op jit(solution)/shard_map/ppermute | solution.py:44
  29.2 5.5 %collective-permute-start.8 = (bf16[16,512]{1,0:T(8,128)(2,1)S(1)}, bf16[16,512]{1,0:T(8,128)(2,1)S(1)}, u32[]{:S(2)}, u32[]{:S(2)}) collective-permute-start(bf16[16,512]{1,0:T(8,128)(2,1)S(1)} %get-tuple-element.41.refs_0_), channel_id=1, source_target_pairs={{0,24},{4,28},{8,16},{12,20},{16,8},{20,12},{24,0},{28,4},{1,25},{... | collective-permute-start | bytes 49160 | tf_op jit(solution)/shard_map/ppermute | solution.py:44
  35.0 2.7 %collective-permute-start.10 = (bf16[64,512]{1,0:T(8,128)(2,1)S(1)}, bf16[64,512]{1,0:T(8,128)(2,1)S(1)}, u32[]{:S(2)}, u32[]{:S(2)}) collective-permute-start(bf16[64,512]{1,0:T(8,128)(2,1)S(1)} %shard_map.162.refs_0_), channel_id=1, source_target_pairs={{0,1},{1,0},{2,3},{3,2},{4,5},{5,4},{6,7},{7,6},{8,9},{9,8},{10,11... | collective-permute-start | bytes 196616 | tf_op jit(solution)/shard_map/ppermute | solution.py:44
  35.1 4.5 %collective-permute-start.14 = (bf16[80,256]{1,0:T(8,128)(2,1)S(1)}, bf16[80,256]{1,0:T(8,128)(2,1)S(1)}, u32[]{:S(2)}, u32[]{:S(2)}) collective-permute-start(bf16[80,256]{1,0:T(8,128)(2,1)S(1)} %get-tuple-element.42), channel_id=1, source_target_pairs={{0,4},{4,0},{8,12},{12,8},{16,20},{20,16},{24,28},{28,24},{1,5},{5... | collective-permute-start | bytes 122888 | tf_op jit(solution)/shard_map/ppermute | solution.py:44
  35.7 20.7 %collective-permute-start.20 = (bf16[256,512]{1,0:T(8,128)(2,1)S(1)}, bf16[256,512]{1,0:T(8,128)(2,1)S(1)}, u32[]{:S(2)}, u32[]{:S(2)}) collective-permute-start(bf16[256,512]{1,0:T(8,128)(2,1)S(1)} %get-tuple-element.51), channel_id=1, source_target_pairs={{0,4},{4,0},{8,12},{12,8},{16,20},{20,16},{24,28},{28,24},{1,5},{5... | collective-permute-start | bytes 786440 | tf_op jit(solution)/shard_map/ppermute | solution.py:44
  37.2 38.1 %collective-permute-start.27 = (bf16[768,256]{1,0:T(8,128)(2,1)S(1)}, bf16[768,256]{1,0:T(8,128)(2,1)S(1)}, u32[]{:S(2)}, u32[]{:S(2)}) collective-permute-start(bf16[768,256]{1,0:T(8,128)(2,1)S(1)} %get-tuple-element.56), channel_id=1, source_target_pairs={{0,4},{4,0},{8,12},{12,8},{16,20},{20,16},{24,28},{28,24},{1,5},{5... | collective-permute-start | bytes 1179656 | tf_op jit(solution)/shard_map/ppermute | solution.py:44
  37.7 4.3 %collective-permute-start.11 = (bf16[64,512]{1,0:T(8,128)(2,1)S(1)}, bf16[64,512]{1,0:T(8,128)(2,1)S(1)}, u32[]{:S(2)}, u32[]{:S(2)}) collective-permute-start(bf16[64,512]{1,0:T(8,128)(2,1)S(1)} %add_convert_fusion), channel_id=1, source_target_pairs={{0,2},{1,3},{2,0},{3,1},{4,6},{5,7},{6,4},{7,5},{8,10},{9,11},{10,... | collective-permute-start | bytes 196616 | tf_op jit(solution)/shard_map/ppermute | solution.py:51
  39.6 1.2 %collective-permute-start.15 = (bf16[80,256]{1,0:T(8,128)(2,1)S(1)}, bf16[80,256]{1,0:T(8,128)(2,1)S(1)}, u32[]{:S(2)}, u32[]{:S(2)}) collective-permute-start(bf16[80,256]{1,0:T(8,128)(2,1)S(1)} %collective-permute-done.14.refs_6_), channel_id=1, source_target_pairs={{0,1},{1,0},{2,3},{3,2},{4,5},{5,4},{6,7},{7,6},{8,9},{9,8},{10,11... | collective-permute-start | bytes 122888 | tf_op jit(solution)/shard_map/ppermute | solution.py:44
  40.8 15.2 %collective-permute-start.12 = (bf16[64,512]{1,0:T(8,128)(2,1)S(1)}, bf16[64,512]{1,0:T(8,128)(2,1)S(1)}, u32[]{:S(2)}, u32[]{:S(2)}) collective-permute-start(bf16[64,512]{1,0:T(8,128)(2,1)S(1)} %add_convert_fusion), channel_id=1, source_target_pairs={{0,6},{1,7},{2,4},{3,5},{4,2},{5,3},{6,0},{7,1},{8,14},{9,15},{10,... | collective-permute-start | bytes 196616 | tf_op jit(solution)/shard_map/ppermute | solution.py:51
  42.0 13.9 %collective-permute-start.13 = (bf16[64,512]{1,0:T(8,128)(2,1)S(1)}, bf16[64,512]{1,0:T(8,128)(2,1)S(1)}, u32[]{:S(2)}, u32[]{:S(2)}) collective-permute-start(bf16[64,512]{1,0:T(8,128)(2,1)S(1)} %add_convert_fusion), channel_id=1, source_target_pairs={{0,4},{1,5},{2,6},{3,7},{4,0},{5,1},{6,2},{7,3},{8,12},{9,13},{10,... | collective-permute-start | bytes 196616 | tf_op jit(solution)/shard_map/ppermute | solution.py:51
  56.7 6.8 %collective-permute-start.21 = (bf16[32,768]{1,0:T(8,128)(2,1)S(1)}, bf16[32,768]{1,0:T(8,128)(2,1)S(1)}, u32[]{:S(2)}, u32[]{:S(2)}) collective-permute-start(bf16[32,768]{1,0:T(8,128)(2,1)S(1)} %get-tuple-element.53), channel_id=1, source_target_pairs={{0,24},{4,28},{8,16},{12,20},{16,8},{20,12},{24,0},{28,4},{1,25},{... | collective-permute-start | bytes 147464 | tf_op jit(solution)/shard_map/ppermute | solution.py:44
  59.9 6.6 %collective-permute-start.22 = (bf16[32,768]{1,0:T(8,128)(2,1)S(1)}, bf16[32,768]{1,0:T(8,128)(2,1)S(1)}, u32[]{:S(2)}, u32[]{:S(2)}) collective-permute-start(bf16[32,768]{1,0:T(8,128)(2,1)S(1)} %get-tuple-element.54), channel_id=1, source_target_pairs={{0,16},{4,20},{8,24},{12,28},{16,0},{20,4},{24,8},{28,12},{1,17},{... | collective-permute-start | bytes 147464 | tf_op jit(solution)/shard_map/ppermute | solution.py:44
  59.9 10.7 %collective-permute-start.17 = (bf16[200,128]{1,0:T(8,128)(2,1)S(1)}, bf16[200,128]{1,0:T(8,128)(2,1)S(1)}, u32[]{:S(2)}, u32[]{:S(2)}) collective-permute-start(bf16[200,128]{1,0:T(8,128)(2,1)S(1)} %get-tuple-element.46), channel_id=1, source_target_pairs={{0,16},{4,20},{8,24},{12,28},{16,0},{20,4},{24,8},{28,12},{1,17},{... | collective-permute-start | bytes 153608 | tf_op jit(solution)/shard_map/ppermute | solution.py:44
  62.8 7.8 %collective-permute-start.18 = (bf16[200,128]{1,0:T(8,128)(2,1)S(1)}, bf16[200,128]{1,0:T(8,128)(2,1)S(1)}, u32[]{:S(2)}, u32[]{:S(2)}) collective-permute-start(bf16[200,128]{1,0:T(8,128)(2,1)S(1)} %get-tuple-element.47), channel_id=1, source_target_pairs={{0,24},{4,28},{8,16},{12,20},{16,8},{20,12},{24,0},{28,4},{1,25},{... | collective-permute-start | bytes 153608 | tf_op jit(solution)/shard_map/ppermute | solution.py:44
  63.5 7.1 %collective-permute-start.19 = (bf16[200,128]{1,0:T(8,128)(2,1)S(1)}, bf16[200,128]{1,0:T(8,128)(2,1)S(1)}, u32[]{:S(2)}, u32[]{:S(2)}) collective-permute-start(bf16[200,128]{1,0:T(8,128)(2,1)S(1)} %get-tuple-element.48), channel_id=1, source_target_pairs={{0,8},{4,12},{8,0},{12,4},{16,24},{20,28},{24,16},{28,20},{1,9},{5... | collective-permute-start | bytes 153608 | tf_op jit(solution)/shard_map/ppermute | solution.py:44
  66.5 4.1 %collective-permute-start.23 = (bf16[32,768]{1,0:T(8,128)(2,1)S(1)}, bf16[32,768]{1,0:T(8,128)(2,1)S(1)}, u32[]{:S(2)}, u32[]{:S(2)}) collective-permute-start(bf16[32,768]{1,0:T(8,128)(2,1)S(1)} %get-tuple-element.55), channel_id=1, source_target_pairs={{0,8},{4,12},{8,0},{12,4},{16,24},{20,28},{24,16},{28,20},{1,9},{5... | collective-permute-start | bytes 147464 | tf_op jit(solution)/shard_map/ppermute | solution.py:44
  70.8 4.5 %collective-permute-start.24 = (bf16[32,768]{1,0:T(8,128)(2,1)S(1)}, bf16[32,768]{1,0:T(8,128)(2,1)S(1)}, u32[]{:S(2)}, u32[]{:S(2)}) collective-permute-start(bf16[32,768]{1,0:T(8,128)(2,1)S(1)} %shard_map.165.refs_0_), channel_id=1, source_target_pairs={{0,8},{4,12},{8,0},{12,4},{16,24},{20,28},{24,16},{28,20},{1,9},{5... | collective-permute-start | bytes 147464 | tf_op jit(solution)/shard_map/ppermute | solution.py:44
  70.9 5.3 %collective-permute-start.25 = (bf16[32,768]{1,0:T(8,128)(2,1)S(1)}, bf16[32,768]{1,0:T(8,128)(2,1)S(1)}, u32[]{:S(2)}, u32[]{:S(2)}) collective-permute-start(bf16[32,768]{1,0:T(8,128)(2,1)S(1)} %shard_map.165.refs_0_), channel_id=1, source_target_pairs={{0,16},{4,20},{8,24},{12,28},{16,0},{20,4},{24,8},{28,12},{1,17},{... | collective-permute-start | bytes 147464 | tf_op jit(solution)/shard_map/ppermute | solution.py:44
  73.2 5.9 %collective-permute-start.26 = (bf16[32,768]{1,0:T(8,128)(2,1)S(1)}, bf16[32,768]{1,0:T(8,128)(2,1)S(1)}, u32[]{:S(2)}, u32[]{:S(2)}) collective-permute-start(bf16[32,768]{1,0:T(8,128)(2,1)S(1)} %shard_map.165.refs_0_), channel_id=1, source_target_pairs={{0,24},{4,28},{8,16},{12,20},{16,8},{20,12},{24,0},{28,4},{1,25},{... | collective-permute-start | bytes 147464 | tf_op jit(solution)/shard_map/ppermute | solution.py:44
  79.3 1.4 %collective-permute-start.28 = (bf16[128,512]{1,0:T(8,128)(2,1)S(1)}, bf16[128,512]{1,0:T(8,128)(2,1)S(1)}, u32[]{:S(2)}, u32[]{:S(2)}) collective-permute-start(bf16[128,512]{1,0:T(8,128)(2,1)S(1)} %shard_map.166), channel_id=1, source_target_pairs={{0,1},{1,0},{2,3},{3,2},{4,5},{5,4},{6,7},{7,6},{8,9},{9,8},{10,11... | collective-permute-start | bytes 393224 | tf_op jit(solution)/shard_map/ppermute | solution.py:44
  80.8 8.2 %collective-permute-start.31 = (bf16[128,256]{1,0:T(8,128)(2,1)S(1)}, bf16[128,256]{1,0:T(8,128)(2,1)S(1)}, u32[]{:S(2)}, u32[]{:S(2)}) collective-permute-start(bf16[128,256]{1,0:T(8,128)(2,1)S(1)} %get-tuple-element.61), channel_id=1, source_target_pairs={{0,4},{1,5},{2,6},{3,7},{4,0},{5,1},{6,2},{7,3},{8,12},{9,13},{10,... | collective-permute-start | bytes 196616 | tf_op jit(solution)/shard_map/ppermute | solution.py:51
  81.8 7.2 %collective-permute-start.30 = (bf16[128,256]{1,0:T(8,128)(2,1)S(1)}, bf16[128,256]{1,0:T(8,128)(2,1)S(1)}, u32[]{:S(2)}, u32[]{:S(2)}) collective-permute-start(bf16[128,256]{1,0:T(8,128)(2,1)S(1)} %get-tuple-element.61), channel_id=1, source_target_pairs={{0,6},{1,7},{2,4},{3,5},{4,2},{5,3},{6,0},{7,1},{8,14},{9,15},{10,... | collective-permute-start | bytes 196616 | tf_op jit(solution)/shard_map/ppermute | solution.py:51
  83.7 2.2 %copy-start.1 = (f32[16,2,128,256]{3,2,1,0:T(8,128)S(1)}, f32[16,2,128,256]{3,2,1,0:T(8,128)}, u32[]{:S(2)}) copy-start(f32[16,2,128,256]{3,2,1,0:T(8,128)} %copy-done) | copy-start | bytes 12582916
  88.3 4.3 %collective-permute-start.29 = (bf16[128,256]{1,0:T(8,128)(2,1)S(1)}, bf16[128,256]{1,0:T(8,128)(2,1)S(1)}, u32[]{:S(2)}, u32[]{:S(2)}) collective-permute-start(bf16[128,256]{1,0:T(8,128)(2,1)S(1)} %get-tuple-element.60), channel_id=1, source_target_pairs={{0,2},{1,3},{2,0},{3,1},{4,6},{5,7},{6,4},{7,5},{8,10},{9,11},{10,... | collective-permute-start | bytes 196616 | tf_op jit(solution)/shard_map/ppermute | solution.py:51
